TPU v7x, 512 devices: a 4x2x32 block of a 4x8x32 slice. The times are simulated.
512 devices in a mesh: grp: 2 (over y), sp: 32 (over z), tp: 8 (over x, core).
Axes of the slice: x: 4, y: 2, z: 32, core: 2. Of those that a mesh axis runs over, the one named last changes fastest.
The devices are a block of a 4x8x32 slice.
Arguments:
- tokens: bfloat16 [32768, 2048], P(('grp', 'sp')), parts along dimension 0, may hold values from -6 to 6
- fresh_token_input: bfloat16 [4096], P('grp'), parts along dimension 0, may hold values from -6 to 6
- value_matrix: bfloat16 [2048, 2048], P(None, 'tp'), may hold values from -0.125 to 0.125
- write_matrix: bfloat16 [2048, 1024], P(None, 'tp'), may hold values from -0.125 to 0.125
- read_matrix: bfloat16 [2048, 1024], P(None, 'tp'), may hold values from -0.125 to 0.125
- gate_matrix: bfloat16 [2048, 2048], P(None, 'tp'), may hold values from -0.125 to 0.125
- step_matrix: bfloat16 [2048, 32], replicated, may hold values from -0.125 to 0.125
- value_filter_taps: bfloat16 [4, 2048], replicated, may hold values from -3 to 3
- write_filter_taps: bfloat16 [4, 1024], replicated, may hold values from -3 to 3
- read_filter_taps: bfloat16 [4, 1024], replicated, may hold values from -3 to 3
- head_log_decay: float32 [32], replicated
- step_offset_bias: float32 [32], replicated, may hold values from -3.5 to -2.5
- decay_spike: float32 [32768, 32], P(('grp', 'sp'), 'tp'), parts along dimension 0, may hold values from -3 to 0, as said below
- bypass_scale: float32 [32], replicated, may hold values from 0.5 to 2
- group_norm_scale: float32 [2048], replicated, may hold values from 0.1 to 1.9
Outputs:
- prompt_out: bfloat16 [32768, 2048], P(('grp', 'sp'), 'tp'), parts along dimension 0
- state_cache: bfloat16 [256, 2048], P(('grp', 'sp'), 'tp'), parts along dimension 0
- step_out: bfloat16 [128, 32], P(('grp', 'tp'), 'sp'), parts along dimension 0
There are 2 independent parts, one for each index of `grp`. A program takes and returns all parts, laid end to end along the dimension named above; an argument that names none is the same for every part. Nothing has to cross between parts.
Inputs may be any that keep to these rules, and one draw needn't show every extreme that they name: `decay_spike`: never positive.
All inputs are finite; a program needn't handle non-finite values.
Results may differ from a plain program's by a relative error of at most 0.023.
Values may be sent and summed in bfloat16 or wider, within the bound.
No kernel may reach another device: no remote copies, remote signals or barrier semaphores. Data moves between devices by JAX's collectives and lax.ppermute only.
A program may use at most 64 MiB of HBM per device.

v0:
```python
import jax
import jax.numpy as jnp
from jax import lax
from jax.sharding import PartitionSpec as P

HEAD = 64
STATE = 128
CONV = 4
BLOCK = 128


epsilon = 1e-06


def passed_along(block, axis, distance):
    devices = range(lax.axis_size(axis))
    route = [(i - distance, i) for i in devices if i - distance in devices]
    return lax.ppermute(block, axis, route)


def from_root(value, axis, source):
    kept = jnp.where(lax.axis_index(axis) == source, value, 0).astype(value.dtype)
    return lax.psum(kept, axis)


def in_order(pieces, dim):
    dims = list(pieces.shape[1:])
    dims[dim] *= pieces.shape[0]
    return jnp.moveaxis(pieces, 0, dim).reshape(dims)


def from_everyone(value, axis):
    peers = lax.axis_size(axis)
    return lax.all_to_all(
        jnp.broadcast_to(value[None], (peers, *value.shape)), axis, 0, 0, tiled=True
    )


def gather_directly(value, axis, dim):
    return in_order(from_everyone(value, axis), dim)


def taken_together(value, axis):
    everything = from_everyone(value, axis)
    return jnp.sum(everything, axis=0)


def project(operand, weights):
    return jnp.dot(operand, weights, preferred_element_type=jnp.float32).astype(jnp.bfloat16)


def apply_taps(previous, current, tap_weights):
    joined = jnp.concatenate([previous, current], axis=0).astype(jnp.float32)
    length = current.shape[0]
    summed = jnp.zeros(current.shape, jnp.float32)
    for offset in range(CONV):
        summed = summed + tap_weights[offset].astype(jnp.float32) * joined[offset : offset + length]
    return summed


def group_norm(gated_rows, groups):
    shaped = gated_rows.reshape(gated_rows.shape[:-1] + (groups, -1))
    normed = shaped * lax.rsqrt(jnp.mean(shaped * shaped, axis=-1, keepdims=True) + epsilon)
    return normed.reshape(gated_rows.shape)


def read_new(cached, stored_portion, read_part, new_decay, step_now, value_now):
    states = cached.astype(jnp.float32).reshape((cached.shape[0],) + value_now.shape)
    updated = (
        new_decay[None, :, :, None] * states
        + step_now[None, :, :, None] * stored_portion.T[:, :, None, None] * value_now[None]
    )
    return jnp.einsum("gn,ngep->gep", read_part, updated)


def on_device(
    tokens,
    fresh_token_input,
    value_matrix,
    write_matrix,
    read_matrix,
    gate_matrix,
    step_matrix,
    value_filter_taps,
    write_filter_taps,
    read_filter_taps,
    head_log_decay,
    step_offset_bias,
    decay_spike,
    bypass_scale,
    group_norm_scale,
):
    head_rank = lax.axis_index("tp")
    sequence_rank = lax.axis_index("sp")
    sequence_count = lax.axis_size("sp")
    channels = value_matrix.shape[1]
    head_count = channels // HEAD
    map_width = write_matrix.shape[1]
    group_count = map_width // STATE
    per_group = head_count // group_count
    row_count = tokens.shape[0]
    head_start = head_rank * head_count
    local_count = STATE // sequence_count
    own_step = lax.dynamic_slice_in_dim(step_matrix, head_start, head_count, 1)
    own_value_taps = lax.dynamic_slice_in_dim(value_filter_taps, head_rank * channels, channels, 1)
    own_write_taps = lax.dynamic_slice_in_dim(
        write_filter_taps, head_rank * map_width, map_width, 1
    )
    own_read_taps = lax.dynamic_slice_in_dim(read_filter_taps, head_rank * map_width, map_width, 1)
    head_decay_rates = jnp.exp(lax.dynamic_slice_in_dim(head_log_decay, head_start, head_count, 0))
    own_bias = lax.dynamic_slice_in_dim(step_offset_bias, head_start, head_count, 0)
    own_skip = lax.dynamic_slice_in_dim(bypass_scale, head_start, head_count, 0)
    own_gain = lax.dynamic_slice_in_dim(group_norm_scale, head_rank * channels, channels, 0)
    value_rows = project(tokens, value_matrix)
    write_rows = project(tokens, write_matrix)
    read_rows = project(tokens, read_matrix)
    gate_rows = project(tokens, gate_matrix)
    step_raw = jnp.dot(tokens, own_step, preferred_element_type=jnp.float32)
    edge = row_count - (CONV - 1)
    tail_rows = (value_rows[edge:], write_rows[edge:], read_rows[edge:])
    before = passed_along((tail_rows[0], tail_rows[1], tail_rows[2]), "sp", 1)
    ending = (
        from_root(tail_rows[0], "sp", sequence_count - 1),
        from_root(tail_rows[1], "sp", sequence_count - 1),
        from_root(tail_rows[2], "sp", sequence_count - 1),
    )
    values = jax.nn.silu(apply_taps(before[0], value_rows, own_value_taps)).astype(jnp.bfloat16)
    writes = jax.nn.silu(apply_taps(before[1], write_rows, own_write_taps)).astype(jnp.bfloat16)
    reads = jax.nn.silu(apply_taps(before[2], read_rows, own_read_taps)).astype(jnp.bfloat16)
    step_length = jax.nn.softplus(step_raw + own_bias)
    log_decay_value = decay_spike - step_length * head_decay_rates
    blocks = row_count // BLOCK
    block_values = values.reshape(blocks, BLOCK, group_count, per_group, HEAD)
    block_writes = writes.reshape(blocks, BLOCK, group_count, STATE)
    block_reads = reads.reshape(blocks, BLOCK, group_count, STATE)
    block_steps = step_length.reshape(blocks, BLOCK, group_count, per_group)
    cumulative = jnp.cumsum(log_decay_value.reshape(blocks, BLOCK, group_count, per_group), axis=1)
    block_end = cumulative[:, -1]
    scaled = (
        (jnp.exp(block_end[:, None] - cumulative) * block_steps)[..., None]
        * block_values.astype(jnp.float32)
    ).astype(jnp.bfloat16)
    block_states = jnp.einsum(
        "bsgn,bsgep->bngep", block_writes, scaled, preferred_element_type=jnp.float32
    )
    running = jnp.zeros((STATE, group_count, per_group, HEAD), jnp.float32)
    inside = []
    for block_index in range(blocks):
        inside.append(running)
        running = (
            jnp.exp(block_end[block_index])[None, :, :, None] * running + block_states[block_index]
        )
    local_states = jnp.stack(inside)
    shard_fading_factor = jnp.sum(block_end, axis=0)
    before_block = jnp.cumsum(block_end, axis=0) - block_end
    decay_table = gather_directly(shard_fading_factor[None], "sp", 0)
    inclusive = jnp.cumsum(decay_table, axis=0)
    exclusive = inclusive - decay_table
    total_decay = inclusive[-1]
    row_pieces = lax.all_to_all(running[None], "sp", split_axis=1, concat_axis=0, tiled=True)
    ranks = jnp.arange(sequence_count)
    below = (ranks[None, :] < ranks[:, None])[:, :, None, None]
    prefix_weight = jnp.exp(jnp.where(below, exclusive[:, None] - inclusive[None, :], -jnp.inf))
    prefix_rows = jnp.einsum("jkge,kngep->jngep", prefix_weight, row_pieces)
    final_weight = jnp.exp(total_decay[None] - inclusive)
    final_rows = jnp.einsum("kge,kngep->ngep", final_weight, row_pieces)
    earlier_state = lax.all_to_all(prefix_rows, "sp", split_axis=0, concat_axis=1, tiled=True)[0]
    scores = jnp.einsum(
        "blgn,bsgn->bgls", block_reads, block_writes, preferred_element_type=jnp.float32
    )
    cum_heads = jnp.transpose(cumulative, (0, 2, 3, 1))
    decay_gaps = cum_heads[..., :, None] - cum_heads[..., None, :]
    step_heads = jnp.transpose(block_steps, (0, 2, 3, 1))
    causal = jnp.tril(jnp.ones((BLOCK, BLOCK), bool))
    mixing = (
        scores[:, :, None]
        * jnp.exp(jnp.where(causal, decay_gaps, -jnp.inf))
        * step_heads[..., None, :]
    ).astype(jnp.bfloat16)
    inner_part = jnp.einsum(
        "bgels,bsgep->blgep", mixing, block_values, preferred_element_type=jnp.float32
    )
    entering = jnp.exp(before_block)[:, None, :, :, None] * earlier_state[None] + local_states
    carried_part = jnp.exp(cumulative)[..., None] * jnp.einsum(
        "blgn,bngep->blgep", block_reads.astype(jnp.float32), entering
    )
    mixed_rows = (inner_part + carried_part).reshape(row_count, head_count, HEAD) + own_skip[
        None, :, None
    ] * values.astype(jnp.float32).reshape(row_count, head_count, HEAD)
    gated_rows = mixed_rows.reshape(row_count, channels) * jax.nn.silu(
        gate_rows.astype(jnp.float32)
    )
    prompt_out = (group_norm(gated_rows, group_count) * own_gain).astype(jnp.bfloat16)
    new_row = fresh_token_input[None]
    new_value = project(new_row, value_matrix)
    new_write = project(new_row, write_matrix)
    new_read = project(new_row, read_matrix)
    new_gate = project(new_row, gate_matrix)
    new_step = jax.nn.softplus(
        jnp.dot(new_row, own_step, preferred_element_type=jnp.float32)[0] + own_bias
    )
    new_values = jax.nn.silu(apply_taps(ending[0], new_value, own_value_taps)).astype(jnp.bfloat16)
    latest_stores = jax.nn.silu(apply_taps(ending[1], new_write, own_write_taps)).astype(
        jnp.bfloat16
    )
    new_reads = jax.nn.silu(apply_taps(ending[2], new_read, own_read_taps)).astype(jnp.bfloat16)
    value_now = new_values.astype(jnp.float32).reshape(group_count, per_group, HEAD)
    write_now = latest_stores.astype(jnp.float32)
    read_now = new_reads.astype(jnp.float32)
    new_decay = jnp.exp(-new_step * head_decay_rates).reshape(group_count, per_group)
    step_now = new_step.reshape(group_count, per_group)
    row_start = sequence_rank * local_count
    cache_rows = final_rows.reshape(local_count, channels).astype(jnp.bfloat16)
    stored_portion = lax.dynamic_slice_in_dim(write_now, row_start, local_count, 1)
    read_part = lax.dynamic_slice_in_dim(read_now, row_start, local_count, 1)
    partial_value = read_new(cache_rows, stored_portion, read_part, new_decay, step_now, value_now)
    reading = taken_together(partial_value, "sp")
    new_mixed = reading + own_skip.reshape(group_count, per_group)[:, :, None] * value_now
    new_gated = new_mixed.reshape(1, channels) * jax.nn.silu(new_gate.astype(jnp.float32))
    step_whole = (group_norm(new_gated, group_count) * own_gain).astype(jnp.bfloat16)[0]
    step_table = step_whole.reshape(channels // sequence_count, sequence_count)
    step_out = lax.dynamic_slice_in_dim(step_table, sequence_rank, 1, 1)
    return (prompt_out, cache_rows, step_out)


def solution(mesh):
    placed = (
        P(("grp", "sp"), None),
        P("grp"),
        P(None, "tp"),
        P(None, "tp"),
        P(None, "tp"),
        P(None, "tp"),
        P(),
        P(),
        P(),
        P(),
        P(),
        P(),
        P(("grp", "sp"), "tp"),
        P(),
        P(),
    )
    return jax.shard_map(
        on_device,
        mesh=mesh,
        in_specs=placed,
        out_specs=(P(("grp", "sp"), "tp"), P(("grp", "sp"), "tp"), P(("grp", "tp"), "sp")),
        check_vma=False,
    )
```

profile of v0, /device:TPU:40, one launch (start us, length us, event | category | flops | bytes accessed | tf_op | source)
XLA Modules:
  0.0 264.0 jit_solution(4816721934194735863)
XLA Ops:
  0.7 1.6 copy-done
  2.2 1.8 convolution_convert_fusion.2
  4.6 5.3 %collective-permute-start.2 = (bf16[3,128]{1,0:T(4,128)(2,1)}, bf16[3,128]{1,0:T(4,128)(2,1)}, u32[]{:S(2)}, u32[]{:S(2)}) collective-permute-start(bf16[3,128]{1,0:T(4,128)(2,1)} %get-tuple-element.46), channel_id=1, source_target_pairs={{0,8},{8,16},{16,24},{24,32},{32,40},{40,48},{48,56},{56,64},{64,7... | collective-permute-start | bytes 2312 | tf_op jit(solution)/shard_map/ppermute | solution.py:18
  11.3 4.7 %collective-permute-start.1 = (bf16[3,128]{1,0:T(4,128)(2,1)}, bf16[3,128]{1,0:T(4,128)(2,1)}, u32[]{:S(2)}, u32[]{:S(2)}) collective-permute-start(bf16[3,128]{1,0:T(4,128)(2,1)} %get-tuple-element.44), channel_id=1, source_target_pairs={{0,8},{8,16},{16,24},{24,32},{32,40},{40,48},{48,56},{56,64},{64,7... | collective-permute-start | bytes 2312 | tf_op jit(solution)/shard_map/ppermute | solution.py:18
  16.1 1.5 multiply_exponential_fusion
  17.5 1.4 multiply_subtract_fusion
  20.6 43.0 %all-to-all-start.1 = ((f32[32,1,1,4]{3,2,1,0:T(1,128)}), f32[32,1,1,4]{3,2,1,0:T(1,128)}, u32[]{:S(2)}, u32[]{:S(2)}) async-start(f32[32,1,1,4]{3,2,1,0:T(1,128)} %broadcast_in_dim.36), calls=%async_computation.1 | async-start | bytes 32768 | tf_op jit(solution)/shard_map/all_to_all | solution.py:34
  63.6 1.9 convolution_convert_fusion.1
  66.8 3.8 %collective-permute-start = (bf16[3,256]{1,0:T(4,128)(2,1)}, bf16[3,256]{1,0:T(4,128)(2,1)}, u32[]{:S(2)}, u32[]{:S(2)}) collective-permute-start(bf16[3,256]{1,0:T(4,128)(2,1)} %get-tuple-element.42), channel_id=1, source_target_pairs={{0,8},{8,16},{16,24},{24,32},{32,40},{40,48},{48,56},{56,64},{64,7... | collective-permute-start | bytes 4616 | tf_op jit(solution)/shard_map/ppermute | solution.py:18
  72.2 1.5 fusion.89
  76.5 2.1 fusion.90
  79.9 56.4 %all-reduce = (bf16[3,256]{1,0:T(4,128)(2,1)S(1)}, bf16[3,128]{1,0:T(4,128)(2,1)S(1)}, bf16[3,128]{1,0:T(4,128)(2,1)S(1)}) all-reduce(bf16[3,256]{1,0:T(4,128)(2,1)S(1)} %copy-done.13, bf16[3,128]{1,0:T(4,128)(2,1)S(1)} %copy-done.18, bf16[3,128]{1,0:T(4,128)(2,1)S(1)} %copy-done.19), channel_id=1, replica_groups=mesh['grp'=2,'sp'=32,'tp'=8] {'sp'}, use_global_device_ids=true, to_apply=%region_7.8 | all-reduce | flops 1536 | bytes 6144 | tf_op jit(solution)/shard_map/psum | solution.py:23
  137.6 2.2 fusion.85
  144.8 0.9 fusion.88
  149.1 19.8 %all-to-all-start = ((bf16[32,2,512]{2,1,0:T(2,128)(2,1)}), bf16[32,2,512]{2,1,0:T(2,128)(2,1)S(1)}, u32[]{:S(2)}, u32[]{:S(2)}) async-start(bf16[32,2,512]{2,1,0:T(2,128)(2,1)} %reshape.495), calls=%async_computation | async-start | bytes 131072 | tf_op jit(solution)/shard_map/all_to_all | solution.py:160
  170.7 22.1 %all-to-all-done = bf16[32,2,512]{2,1,0:T(2,128)(2,1)S(1)} async-done(((bf16[32,2,512]{2,1,0:T(2,128)(2,1)}), bf16[32,2,512]{2,1,0:T(2,128)(2,1)S(1)}, u32[]{:S(2)}, u32[]{:S(2)}) %all-to-all-start) | async-done | bytes 65568 | tf_op jit(solution)/shard_map/all_to_all | solution.py:160
  194.1 5.3 %all-to-all-start.3 = ((f32[32,1,256]{2,1,0:T(1,128)}), f32[32,1,256]{2,1,0:T(1,128)}, u32[]{:S(2)}, u32[]{:S(2)}) async-start(f32[32,1,256]{2,1,0:T(1,128)} %reshape.499), calls=%async_computation.3 | async-start | bytes 65536 | tf_op jit(solution)/shard_map/all_to_all | solution.py:34
  199.9 0.9 reshape.497
  200.8 21.1 %all-to-all-done.3 = f32[32,1,256]{2,1,0:T(1,128)} async-done(((f32[32,1,256]{2,1,0:T(1,128)}), f32[32,1,256]{2,1,0:T(1,128)}, u32[]{:S(2)}, u32[]{:S(2)}) %all-to-all-start.3) | async-done | bytes 32800 | tf_op jit(solution)/shard_map/all_to_all | solution.py:34
  221.8 5.0 %all-to-all-start.2 = ((f32[32,1,1024]{2,1,0:T(1,128)}), f32[32,1,1024]{2,1,0:T(1,128)S(1)}, u32[]{:S(2)}, u32[]{:S(2)}) async-start(f32[32,1,1024]{2,1,0:T(1,128)} %reshape.497), calls=%async_computation.2 | async-start | bytes 262144 | tf_op jit(solution)/shard_map/all_to_all | solution.py:167
  226.8 1.3 fusion.39
  228.1 1.6 fusion.52
  230.9 1.5 reduce.19
  232.6 1.3 multiply_reduce_fusion.1
  234.6 1.3 multiply_convert_fusion.7
  236.7 16.4 %all-to-all-done.2 = f32[32,1,1024]{2,1,0:T(1,128)S(1)} async-done(((f32[32,1,1024]{2,1,0:T(1,128)}), f32[32,1,1024]{2,1,0:T(1,128)S(1)}, u32[]{:S(2)}, u32[]{:S(2)}) %all-to-all-start.2) | async-done | bytes 131104 | tf_op jit(solution)/shard_map/all_to_all | solution.py:167
  253.2 0.9 reduce.18
  254.5 1.4 fusion.1
  255.9 2.1 fusion
  258.0 1.4 copy.186
  259.5 1.4 reshape.479
  260.9 2.2 multiply_reduce_fusion
  (145 shorter events, 26.8 us)
Async XLA Ops:
  0.6 1.6 copy-start
  0.6 9.3 %copy-start.2 = (bf16[2048,128]{1,0:T(8,128)(2,1)S(1)}, bf16[2048,128]{1,0:T(8,128)(2,1)}, u32[]{:S(2)}) copy-start(bf16[2048,128]{1,0:T(8,128)(2,1)} %param.19) | copy-start | bytes 1572868
  2.2 13.7 %copy-start.17 = (bf16[2048]{0:T(1024)(128)(2,1)S(1)}, bf16[2048]{0:T(1024)(128)(2,1)}, u32[]{:S(2)}) copy-start(bf16[2048]{0:T(1024)(128)(2,1)} %param.16) | copy-start | bytes 12292
  2.2 13.7 %copy-start.27 = (f32[32]{0:T(128)S(1)}, f32[32]{0:T(128)}, u32[]{:S(2)}) copy-start(f32[32]{0:T(128)} %param.26) | copy-start | bytes 388
  2.2 13.8 %copy-start.28 = (f32[32]{0:T(128)S(1)}, f32[32]{0:T(128)}, u32[]{:S(2)}) copy-start(f32[32]{0:T(128)} %param.25) | copy-start | bytes 388
  4.0 13.5 %copy-start.12 = (f32[512,4]{0,1:T(4,128)S(1)}, f32[512,4]{0,1:T(4,128)}, u32[]{:S(2)}) copy-start(f32[512,4]{0,1:T(4,128)} %param.27) | copy-start | bytes 24580
  4.6 139.3 %collective-permute-start.2 = (bf16[3,128]{1,0:T(4,128)(2,1)}, bf16[3,128]{1,0:T(4,128)(2,1)}, u32[]{:S(2)}, u32[]{:S(2)}) collective-permute-start(bf16[3,128]{1,0:T(4,128)(2,1)} %get-tuple-element.46), channel_id=1, source_target_pairs={{0,8},{8,16},{16,24},{24,32},{32,40},{40,48},{48,56},{56,64},{64,7... | collective-permute-start | bytes 2312 | tf_op jit(solution)/shard_map/ppermute | solution.py:18
  10.6 8.4 %copy-start.3 = (bf16[512,128]{1,0:T(8,128)(2,1)}, bf16[512,128]{1,0:T(8,128)(2,1)S(1)}, u32[]{:S(2)}) copy-start(bf16[512,128]{1,0:T(8,128)(2,1)S(1)} %convolution_convert_fusion.3) | copy-start | bytes 393220
  11.3 131.8 %collective-permute-start.1 = (bf16[3,128]{1,0:T(4,128)(2,1)}, bf16[3,128]{1,0:T(4,128)(2,1)}, u32[]{:S(2)}, u32[]{:S(2)}) collective-permute-start(bf16[3,128]{1,0:T(4,128)(2,1)} %get-tuple-element.44), channel_id=1, source_target_pairs={{0,8},{8,16},{16,24},{24,32},{32,40},{40,48},{48,56},{56,64},{64,7... | collective-permute-start | bytes 2312 | tf_op jit(solution)/shard_map/ppermute | solution.py:18
  19.3 51.9 %copy-start.1 = (bf16[2048,128]{1,0:T(8,128)(2,1)S(1)}, bf16[2048,128]{1,0:T(8,128)(2,1)}, u32[]{:S(2)}) copy-start(bf16[2048,128]{1,0:T(8,128)(2,1)} %param.18) | copy-start | bytes 1572868
  20.6 128.6 %all-to-all-start.1 = ((f32[32,1,1,4]{3,2,1,0:T(1,128)}), f32[32,1,1,4]{3,2,1,0:T(1,128)}, u32[]{:S(2)}, u32[]{:S(2)}) async-start(f32[32,1,1,4]{3,2,1,0:T(1,128)} %broadcast_in_dim.36), calls=%async_computation.1 | async-start | bytes 32768 | tf_op jit(solution)/shard_map/all_to_all | solution.py:34
  66.8 78.9 %collective-permute-start = (bf16[3,256]{1,0:T(4,128)(2,1)}, bf16[3,256]{1,0:T(4,128)(2,1)}, u32[]{:S(2)}, u32[]{:S(2)}) collective-permute-start(bf16[3,256]{1,0:T(4,128)(2,1)} %get-tuple-element.42), channel_id=1, source_target_pairs={{0,8},{8,16},{16,24},{24,32},{32,40},{40,48},{48,56},{56,64},{64,7... | collective-permute-start | bytes 4616 | tf_op jit(solution)/shard_map/ppermute | solution.py:18
  72.0 6.7 %copy-start.9 = (f32[4,1,1,4]{3,2,1,0:T(1,128)S(1)}, f32[4,1,1,4]{3,2,1,0:T(1,128)}, u32[]{:S(2)}) copy-start(f32[4,1,1,4]{3,2,1,0:T(1,128)} %get-tuple-element.36) | copy-start | bytes 196
  72.0 7.9 %copy-start.13 = (bf16[3,256]{1,0:T(4,128)(2,1)S(1)}, bf16[3,256]{1,0:T(4,128)(2,1)}, u32[]{:S(2)}) copy-start(bf16[3,256]{1,0:T(4,128)(2,1)} %get-tuple-element.41) | copy-start | bytes 4612
  72.0 7.9 %copy-start.18 = (bf16[3,128]{1,0:T(4,128)(2,1)S(1)}, bf16[3,128]{1,0:T(4,128)(2,1)}, u32[]{:S(2)}) copy-start(bf16[3,128]{1,0:T(4,128)(2,1)} %get-tuple-element.45) | copy-start | bytes 2308
  72.0 7.9 %copy-start.19 = (bf16[3,128]{1,0:T(4,128)(2,1)S(1)}, bf16[3,128]{1,0:T(4,128)(2,1)}, u32[]{:S(2)}) copy-start(bf16[3,128]{1,0:T(4,128)(2,1)} %get-tuple-element.43) | copy-start | bytes 2308
  72.0 64.3 %copy-start.20 = (bf16[1,128]{1,0:T(2,128)(2,1)S(1)}, bf16[1,128]{1,0:T(2,128)(2,1)}, u32[]{:S(2)}) copy-start(bf16[1,128]{1,0:T(2,128)(2,1)} %fusion.5) | copy-start | bytes 772
  72.0 65.0 %copy-start.26 = (f32[4]{0:T(128)S(1)}, f32[4]{0:T(128)}, u32[]{:S(2)}) copy-start(f32[4]{0:T(128)} %get-tuple-element.57) | copy-start | bytes 52
  72.0 71.1 %copy-start.4 = (bf16[512,128]{1,0:T(8,128)(2,1)S(1)}, bf16[512,128]{1,0:T(8,128)(2,1)}, u32[]{:S(2)}) copy-start(bf16[512,128]{1,0:T(8,128)(2,1)} %copy-done.3) | copy-start | bytes 393220
  78.6 67.2 %copy-start.7 = (bf16[512,256]{1,0:T(8,128)(2,1)S(1)}, bf16[512,256]{1,0:T(8,128)(2,1)}, u32[]{:S(2)}) copy-start(bf16[512,256]{1,0:T(8,128)(2,1)} %copy-done.6) | copy-start | bytes 786436
  143.9 2.9 %copy-start.5 = (bf16[512,128]{1,0:T(8,128)(2,1)}, bf16[512,128]{1,0:T(8,128)(2,1)S(1)}, u32[]{:S(2)}) copy-start(bf16[512,128]{1,0:T(8,128)(2,1)S(1)} %multiply_convert_fusion.6) | copy-start | bytes 393220
  146.5 1.0 copy-start.14
  146.9 46.2 %copy-start.24 = (f32[4]{0:T(128)S(1)}, f32[4]{0:T(128)}, u32[]{:S(2)}) copy-start(f32[4]{0:T(128)} %get-tuple-element.25) | copy-start | bytes 52
  146.9 46.3 %copy-start.25 = (bf16[1,128]{1,0:T(2,128)(2,1)S(1)}, bf16[1,128]{1,0:T(2,128)(2,1)}, u32[]{:S(2)}) copy-start(bf16[1,128]{1,0:T(2,128)(2,1)} %fusion.80) | copy-start | bytes 772
  147.0 52.4 %copy-start.10 = (pred[32,32]{1,0:T(8,128)(4,1)S(1)}, pred[32,32]{1,0:T(8,128)(4,1)}, u32[]{:S(2)}) copy-start(pred[32,32]{1,0:T(8,128)(4,1)} %iota_compare_fusion.1) | copy-start | bytes 3076
  149.1 43.7 %all-to-all-start = ((bf16[32,2,512]{2,1,0:T(2,128)(2,1)}), bf16[32,2,512]{2,1,0:T(2,128)(2,1)S(1)}, u32[]{:S(2)}, u32[]{:S(2)}) async-start(bf16[32,2,512]{2,1,0:T(2,128)(2,1)} %reshape.495), calls=%async_computation | async-start | bytes 131072 | tf_op jit(solution)/shard_map/all_to_all | solution.py:160
  194.1 27.7 %all-to-all-start.3 = ((f32[32,1,256]{2,1,0:T(1,128)}), f32[32,1,256]{2,1,0:T(1,128)}, u32[]{:S(2)}, u32[]{:S(2)}) async-start(f32[32,1,256]{2,1,0:T(1,128)} %reshape.499), calls=%async_computation.3 | async-start | bytes 65536 | tf_op jit(solution)/shard_map/all_to_all | solution.py:34
  200.8 55.1 %copy-start.8 = (f32[4,128,128]{2,1,0:T(8,128)S(1)}, f32[4,128,128]{2,1,0:T(8,128)}, u32[]{:S(2)}) copy-start(f32[4,128,128]{2,1,0:T(8,128)} %fusion.88) | copy-start | bytes 786436
  221.8 31.3 %all-to-all-start.2 = ((f32[32,1,1024]{2,1,0:T(1,128)}), f32[32,1,1024]{2,1,0:T(1,128)S(1)}, u32[]{:S(2)}, u32[]{:S(2)}) async-start(f32[32,1,1024]{2,1,0:T(1,128)} %reshape.497), calls=%async_computation.2 | async-start | bytes 262144 | tf_op jit(solution)/shard_map/all_to_all | solution.py:167
  229.8 26.1 %copy-start.11 = (pred[128,128]{1,0:T(8,128)(4,1)S(1)}, pred[128,128]{1,0:T(8,128)(4,1)}, u32[]{:S(2)}) copy-start(pred[128,128]{1,0:T(8,128)(4,1)} %iota_compare_fusion) | copy-start | bytes 49156
  258.0 2.9 %copy-start.23 = (f32[256]{0:T(256)S(1)}, f32[256]{0:T(256)}, u32[]{:S(2)}) copy-start(f32[256]{0:T(256)} %mul.534) | copy-start | bytes 3076
  260.9 2.2 copy-start.16
  (4 other events, 3.6 us)
where the time goes:
time: 265 us; the launch traced here: 264 us
  starting transfers between devices  86.9 us (33%)
  waiting for transfers between devices  59.6 us (22%)
  blocking collectives  56.4 us (21%)
  other arithmetic  21.9 us (8%)
  matrix products  19.2 us (7%)
  local copies, waits for them, and re-layouts  18 us (7%)
    psum x1, blocking collectives, from_root(): return lax.psum(kept, axis)  56.4 us
    all_to_all x2, starting transfers between devices, from_everyone(): lax.all_to_all(jnp.broadcast_to(value[None], (peers, *value.shape)), axis...  48.4 us
    all_to_all x1, waiting for transfers between devices, on_device(): lax.all_to_all(running[None], 'sp', split_axis=1, concat_axis=0, tiled=True)  22.1 us
    all_to_all x2, waiting for transfers between devices, from_everyone(): lax.all_to_all(jnp.broadcast_to(value[None], (peers, *value.shape)), axis...  21.1 us
    all_to_all x1, starting transfers between devices, on_device(): lax.all_to_all(running[None], 'sp', split_axis=1, concat_axis=0, tiled=True)  19.8 us
    all_to_all x1, waiting for transfers between devices, on_device(): lax.all_to_all(prefix_rows, 'sp', split_axis=0, concat_axis=1, tiled=True)  16.4 us
    ppermute x3, starting transfers between devices, passed_along(): return lax.ppermute(block, axis, route)  13.8 us
    dot_general x8, matrix products, project(): jnp.dot(operand, weights, preferred_element_type=jnp.float32)  11.1 us
  transfers between devices with their start and end apart: 7, of which 3 were waited for; matrix products, arithmetic and copies ran while one was open for 16% of the time, Pallas kernels for 0%

commit v1 on v0

v1 whole, which is shorter than its diff:
```python
import jax
import jax.numpy as jnp
from jax import lax
from jax.experimental import pallas as pl
from jax.experimental.pallas import tpu as pltpu
from jax.sharding import PartitionSpec as P

HEAD = 64
STATE = 128
CONV = 4
BLOCK = 128
SUB = 8
MISC = 128
HALO = 8

epsilon = 1e-06
f32 = jnp.float32
bf16 = jnp.bfloat16
HIGHEST = lax.Precision.HIGHEST
VMEM_LIMIT = 56 * 1024 * 1024


def dot(a, b, dims=((1,), (0,)), precision=None):
    return lax.dot_general(a, b, (dims, ((), ())), precision=precision, preferred_element_type=f32)


def silu(x):
    return x / (1.0 + jnp.exp(-x))


def softplus(x):
    return jnp.maximum(x, 0.0) + jnp.log1p(jnp.exp(-jnp.abs(x)))


def iota(shape, dim):
    return lax.broadcasted_iota(jnp.int32, shape, dim)


def spread(heads, channels):
    return (iota((heads, channels), 0) == iota((heads, channels), 1) // HEAD).astype(f32)


def own_rows(table, rank, count):
    picked = table[0:count]
    for other in range(1, table.shape[0] // count):
        picked = jnp.where(rank == other, table[other * count : (other + 1) * count], picked)
    return picked


def head_column(ref, first, count, width):
    rows = iota((count, width), 0)
    column = jnp.full((count, width), ref[first], f32)
    for h in range(1, count):
        column = jnp.where(rows == h, ref[first + h], column)
    return column


def project_kernel(
    tok_ref, fresh_ref, wv_ref, ww_ref, wr_ref, ws_ref, rows_ref, step_ref, new_ref, newstep_ref,
    acc, accs, accn, accns,
):
    k = pl.program_id(0)
    last = pl.num_programs(0) - 1
    tok = tok_ref[...]
    fresh = jnp.broadcast_to(fresh_ref[...], (16, fresh_ref.shape[1]))
    weights = jnp.concatenate([wv_ref[...], ww_ref[...], wr_ref[...]], axis=1)
    part = dot(tok, weights)
    parts = dot(ws_ref[...], tok, ((1,), (1,)))
    partn = dot(fresh, weights)
    partns = dot(ws_ref[...], fresh, ((1,), (1,)))

    @pl.when(k == 0)
    def _():
        acc[...] = part
        accs[...] = parts
        accn[...] = partn
        accns[...] = partns

    @pl.when(k > 0)
    def _():
        acc[...] += part
        accs[...] += parts
        accn[...] += partn
        accns[...] += partns

    @pl.when(k == last)
    def _():
        rank = lax.axis_index("tp")
        heads = step_ref.shape[0]
        rows_ref[...] = acc[...].astype(bf16)
        step_ref[...] = own_rows(accs[...], rank, heads)
        new_ref[...] = accn[...][0:8]
        newstep_ref[...] = own_rows(accns[...], rank, heads)


def local_kernel(
    rows_ref, halo_ref, wv_ref, ww_ref, wr_ref, step_ref, new_ref, newstep_ref, spike_ref,
    vtap_ref, wtap_ref, rtap_ref, decay_ref, bias_ref, skip_ref,
    vwr_ref, cum_ref, dt_ref, inside_ref, send_ref, ext,
):
    rank = lax.axis_index("tp")
    length = rows_ref.shape[0]
    heads = step_ref.shape[0]
    channels = wv_ref.shape[1]
    first = rank * heads
    halo = halo_ref[...]
    before = jnp.concatenate(
        [dot(halo, wv_ref[...]), dot(halo, ww_ref[...]), dot(halo, wr_ref[...])], axis=1
    )
    ext[0:HALO] = before.astype(bf16).astype(f32)
    ext[HALO:] = rows_ref[...].astype(f32)
    taps = jnp.concatenate(
        [
            vtap_ref[:, pl.ds(pl.multiple_of(rank * channels, 128), channels)].astype(f32),
            wtap_ref[:, pl.ds(pl.multiple_of(rank * STATE, 128), STATE)].astype(f32),
            rtap_ref[:, pl.ds(pl.multiple_of(rank * STATE, 128), STATE)].astype(f32),
        ],
        axis=1,
    )
    off = HALO - (CONV - 1)
    summed = taps[0:1] * ext[off : off + length]
    for k in range(1, CONV):
        summed = summed + taps[k : k + 1] * ext[off + k : off + k + length]
    vwr = silu(summed).astype(bf16)
    vwr_ref[...] = vwr
    newest = taps[CONV - 1 : CONV] * new_ref[0:1].astype(bf16).astype(f32)
    for k in range(CONV - 1):
        row = length + off + k
        newest = newest + taps[k : k + 1] * ext[row : row + 1]
    newest = silu(newest).astype(bf16).astype(f32)
    new_value = newest[:, 0:channels]
    new_write = newest[:, channels : channels + STATE]
    new_read = newest[:, channels + STATE :]
    bias = head_column(bias_ref, first, heads, 128)
    rate = jnp.exp(head_column(decay_ref, first, heads, 128))
    upper = (iota((BLOCK, BLOCK), 0) <= iota((BLOCK, BLOCK), 1)).astype(f32)
    expand = spread(heads, channels)
    running = jnp.zeros((STATE, channels), f32)
    total = jnp.zeros((heads, 128), f32)
    for b in range(length // BLOCK):
        at = slice(b * BLOCK, (b + 1) * BLOCK)
        dt = softplus(step_ref[:, at] + bias)
        log_decay = spike_ref[:, at] - dt * rate
        cum = dot(log_decay, upper, precision=HIGHEST)
        dt_ref[:, at] = dt
        cum_ref[:, at] = cum
        end = jnp.broadcast_to(cum[:, BLOCK - 1 :], (heads, BLOCK))
        factor = dot(jnp.exp(end - cum) * dt, expand, ((0,), (0,)), HIGHEST)
        scaled = (factor * vwr[at, 0:channels].astype(f32)).astype(bf16)
        states = dot(vwr[at, channels : channels + STATE], scaled, ((0,), (0,)))
        fade = dot(jnp.exp(end), expand, ((0,), (0,)), HIGHEST)
        inside_ref[b] = running.astype(bf16)
        running = fade * running + states
        total = total + end
    fade = jnp.exp(total)
    high = fade.astype(bf16).astype(f32)
    low = fade - high
    shape = (STATE, MISC)
    lanes = iota(shape, 1)
    rows = iota(shape, 0)
    misc = jnp.zeros(shape, f32)
    for h in range(heads):
        misc = jnp.where(lanes == h, high[h : h + 1, 0:1], misc)
        misc = jnp.where(lanes == heads + h, low[h : h + 1, 0:1], misc)
    own = STATE // lax.axis_size("sp")
    stretch = SUB * own
    diagonal = jnp.where(rows == lanes, jnp.broadcast_to(new_read, shape), 0.0)
    read_column = jnp.sum(diagonal, axis=1, keepdims=True)
    new_dt = softplus(newstep_ref[...][:, 0:1] + bias[:, 0:1])
    skip = head_column(skip_ref, first, heads, 128)[:, 0:1]
    weight = new_dt * jnp.sum(new_read * new_write, axis=1, keepdims=True) + skip
    direct = jnp.sum(expand * weight, axis=0, keepdims=True) * new_value
    placed = jnp.where(iota((8, channels), 0) == iota((8, channels), 1) // HEAD, direct, 0.0)
    shift = (iota((channels, MISC), 0) % HEAD + (MISC - HEAD) == iota((channels, MISC), 1)).astype(f32)
    direct_rows = dot(placed, shift, precision=HIGHEST)[0:own]
    for g in range(STATE // stretch):
        at = slice(g * stretch, (g + 1) * stretch)
        piece = running[at].reshape(SUB, own, channels).astype(bf16)
        for copy in range(STATE // stretch):
            send_ref[copy * SUB : (copy + 1) * SUB, :, g * channels : (g + 1) * channels] = piece
    note = misc[0:stretch]
    for g in range(STATE // stretch):
        at = slice(g * stretch, (g + 1) * stretch)
        note = jnp.where(lanes[0:stretch] == 2 * heads + g, read_column[at], note)
    note = note.reshape(SUB, own, MISC)
    note = jnp.where(iota(note.shape, 2) >= MISC - HEAD, direct_rows[None], note).astype(bf16)
    wide = STATE // stretch * channels
    for copy in range(STATE // stretch):
        send_ref[copy * SUB : (copy + 1) * SUB, :, wide:] = note


def inner_kernel(
    tok_ref, wg_ref, fresh_ref, vwr_ref, cum_ref, dt_ref, inside_ref, skip_ref,
    base_ref, lift_ref, newgate_ref, before,
):
    b = pl.program_id(0)
    rank = lax.axis_index("tp")
    heads = cum_ref.shape[0]
    channels = wg_ref.shape[1]

    @pl.when(b == 0)
    def _():
        before[...] = jnp.zeros_like(before)
        fresh = jnp.broadcast_to(fresh_ref[...], (16, fresh_ref.shape[1]))
        gate = dot(fresh, wg_ref[...])[0:8].astype(bf16).astype(f32)
        newgate_ref[...] = silu(gate)

    expand = spread(heads, channels)
    skip = jnp.sum(
        expand * head_column(skip_ref, rank * heads, heads, channels), axis=0, keepdims=True
    )
    cum = cum_ref[...]
    dt = dt_ref[...]
    values = vwr_ref[:, 0:channels]
    writes = vwr_ref[:, channels : channels + STATE]
    reads = vwr_ref[:, channels + STATE :]
    gate = silu(dot(tok_ref[...], wg_ref[...]).astype(bf16).astype(f32))
    scores = dot(reads, writes, ((1,), (1,)))
    causal = iota((BLOCK, BLOCK), 0) >= iota((BLOCK, BLOCK), 1)
    columns = jnp.transpose(jnp.concatenate([cum, cum], axis=0))
    parts = []
    for h in range(heads):
        gap = columns[:, h : h + 1] - cum[h : h + 1]
        mixing = scores * jnp.exp(jnp.where(causal, gap, -jnp.inf)) * dt[h : h + 1]
        parts.append(dot(mixing.astype(bf16), values[:, h * HEAD : (h + 1) * HEAD]))
    inner = jnp.concatenate(parts, axis=1)
    fade = dot(jnp.exp(cum), expand, ((0,), (0,)), HIGHEST)
    carried = fade * dot(reads, inside_ref[0])
    base_ref[...] = (inner + carried + skip * values.astype(f32)) * gate
    far = jnp.exp(cum + before[...])
    lift_ref[...] = dot(far, expand, ((0,), (0,)), HIGHEST) * gate
    before[...] += jnp.broadcast_to(cum[:, BLOCK - 1 :], before.shape)


def prefix_kernel(recv_ref, newstep_ref, decay_ref, bias_ref, send_ref, cache_ref, direct_ref, states):
    rank = lax.axis_index("tp")
    place = lax.axis_index("sp")
    count = recv_ref.shape[0]
    own = recv_ref.shape[1]
    wide = recv_ref.shape[2] - MISC
    pieces = count // SUB
    channels = wide // pieces
    heads = channels // HEAD
    group = place // SUB
    notes = recv_ref[:, 0:1, wide:].astype(f32).reshape(count, MISC)
    lane = iota((MISC, channels), 0)
    owner = iota((MISC, channels), 1) // HEAD
    pick = jnp.where((lane == owner) | (lane == owner + heads), 1.0, 0.0)
    fades = dot(jnp.where(iota(notes.shape, 1) < 2 * heads, notes, 0.0), pick, precision=HIGHEST)
    state = jnp.zeros((own, wide), f32)
    for k in range(count):
        states[k] = state
        fade = jnp.concatenate([fades[k : k + 1]] * pieces, axis=1)
        state = fade * state + recv_ref[k, :, 0:wide].astype(f32)
    kept = state.astype(bf16)
    mine = kept[:, 0:channels]
    for g in range(1, pieces):
        mine = jnp.where(group == g, kept[:, g * channels : (g + 1) * channels], mine)
    cache_ref[...] = mine
    note = recv_ref[count - 1, :, wide:].astype(f32)
    reading = jnp.zeros((own, channels), f32)
    for g in range(pieces):
        column = note[:, 2 * heads + g : 2 * heads + g + 1]
        reading = reading + column * kept[:, g * channels : (g + 1) * channels].astype(f32)
    first = rank * heads
    bias = head_column(bias_ref, first, heads, 1)
    rate = jnp.exp(head_column(decay_ref, first, heads, 1))
    decay = jnp.exp(-softplus(newstep_ref[...][:, 0:1] + bias) * rate)
    decay = jnp.sum(spread(heads, channels) * decay, axis=0, keepdims=True)
    partial = jnp.sum(reading, axis=0, keepdims=True) * decay
    high = partial.astype(bf16).astype(f32)
    low = partial - high
    rows = iota((own, channels), 0)
    share = jnp.where(rows == 0, high, jnp.where(rows == 1, low, 0.0)).astype(bf16)
    chosen = states[pl.ds(group * SUB, SUB)]
    send_ref[:, :, 0:wide] = chosen.astype(bf16)
    send_ref[:, :, wide:] = jnp.broadcast_to(share[None], (SUB, own, channels))
    unshift = (iota((MISC, channels), 0) == iota((MISC, channels), 1) % HEAD + (MISC - HEAD)).astype(f32)
    laid = dot(note, unshift, precision=HIGHEST)
    direct_ref[...] = jnp.sum(jnp.where(rows == iota(rows.shape, 1) // HEAD, laid, 0.0), axis=0, keepdims=True)


def finish_kernel(recv_ref, base_ref, lift_ref, reads_ref, gain_ref, direct_ref, newgate_ref, out_ref, step_ref):
    rank = lax.axis_index("tp")
    place = lax.axis_index("sp")
    channels = base_ref.shape[1]
    wide = recv_ref.shape[2] - channels
    pieces = wide // channels
    own = recv_ref.shape[1]
    earlier = jnp.concatenate(
        [
            recv_ref[:, :, g * channels : (g + 1) * channels].astype(f32).reshape(SUB * own, channels)
            for g in range(pieces)
        ],
        axis=0,
    ).astype(bf16)
    gain = gain_ref[:, pl.ds(pl.multiple_of(rank * channels, 128), channels)]
    gated = base_ref[...] + dot(reads_ref[...], earlier) * lift_ref[...]
    scale = lax.rsqrt(jnp.mean(gated * gated, axis=1, keepdims=True) + epsilon)
    out_ref[...] = (gated * scale * gain).astype(bf16)
    partial = jnp.sum(jnp.sum(recv_ref[:, :, wide:].astype(f32), axis=0), axis=0, keepdims=True)
    new = (partial + direct_ref[...]) * newgate_ref[0:1]
    scale = lax.rsqrt(jnp.mean(new * new, axis=1, keepdims=True) + epsilon)
    step = (new * scale * gain).astype(bf16)
    columns = lax.axis_size("sp")
    channel = iota((channels, 128), 0)
    take = (channel // columns == iota((channels, 128), 1)) & (channel % columns == place)
    picked = dot(jnp.broadcast_to(step, (16, channels)), take.astype(bf16))
    step_ref[...] = picked[0:1, 0 : channels // columns].astype(bf16)


def call(kernel, out_shape, grid=None, in_specs=None, out_specs=None, scratch=(), flops=0, name=None):
    return pl.pallas_call(
        kernel,
        out_shape=out_shape,
        grid_spec=pltpu.PrefetchScalarGridSpec(
            num_scalar_prefetch=0,
            grid=grid or (),
            in_specs=in_specs,
            out_specs=out_specs,
            scratch_shapes=scratch,
        ),
        compiler_params=pltpu.CompilerParams(
            vmem_limit_bytes=VMEM_LIMIT,
            dimension_semantics=("arbitrary",) * len(grid or ()),
        ),
        cost_estimate=pl.CostEstimate(flops=flops, transcendentals=0, bytes_accessed=1 << 20),
        name=name,
    )


def shaped(*shape, dtype=f32):
    return jax.ShapeDtypeStruct(shape, dtype)


def on_device(
    tokens,
    fresh_token_input,
    value_matrix,
    write_matrix,
    read_matrix,
    gate_matrix,
    step_matrix,
    value_filter_taps,
    write_filter_taps,
    read_filter_taps,
    head_log_decay,
    step_offset_bias,
    decay_spike,
    bypass_scale,
    group_norm_scale,
):
    sequence_count = lax.axis_size("sp")
    length, depth = tokens.shape
    channels = value_matrix.shape[1]
    heads = channels // HEAD
    all_heads = step_matrix.shape[1]
    own = STATE // sequence_count
    pieces = sequence_count // SUB
    blocks = length // BLOCK
    width = channels + 2 * STATE
    vm = pl.BlockSpec(memory_space=pltpu.VMEM)
    sm = pl.BlockSpec(memory_space=pltpu.SMEM)

    halo = lax.ppermute(
        tokens[length - HALO :], "sp", [(i, i + 1) for i in range(sequence_count - 1)]
    )
    fresh = fresh_token_input[None]
    spike = decay_spike.T
    chunk = depth // 4
    rows, step_raw, new_rows, new_step = call(
        project_kernel,
        (
            shaped(length, width, dtype=bf16),
            shaped(heads, length),
            shaped(8, width),
            shaped(heads, 16),
        ),
        grid=(depth // chunk,),
        in_specs=[
            pl.BlockSpec((length, chunk), lambda k: (0, k)),
            pl.BlockSpec((1, chunk), lambda k: (0, k)),
            pl.BlockSpec((chunk, channels), lambda k: (k, 0)),
            pl.BlockSpec((chunk, STATE), lambda k: (k, 0)),
            pl.BlockSpec((chunk, STATE), lambda k: (k, 0)),
            pl.BlockSpec((all_heads, chunk), lambda k: (0, k)),
        ],
        out_specs=[
            pl.BlockSpec((length, width), lambda k: (0, 0)),
            pl.BlockSpec((heads, length), lambda k: (0, 0)),
            pl.BlockSpec((8, width), lambda k: (0, 0)),
            pl.BlockSpec((heads, 16), lambda k: (0, 0)),
        ],
        scratch=[
            pltpu.VMEM((length, width), f32),
            pltpu.VMEM((all_heads, length), f32),
            pltpu.VMEM((16, width), f32),
            pltpu.VMEM((all_heads, 16), f32),
        ],
        flops=2 * length * depth * width,
        name="project",
    )(tokens, fresh, value_matrix, write_matrix, read_matrix, step_matrix.T)

    wide = pieces * channels
    vwr, cum, dt, inside, send = call(
        local_kernel,
        (
            shaped(length, width, dtype=bf16),
            shaped(heads, length),
            shaped(heads, length),
            shaped(blocks, STATE, channels, dtype=bf16),
            shaped(sequence_count, own, wide + MISC, dtype=bf16),
        ),
        in_specs=[vm] * 12 + [sm] * 3,
        out_specs=[vm] * 5,
        scratch=[pltpu.VMEM((length + HALO, width), f32)],
        flops=2 * length * STATE * channels,
        name="local",
    )(
        rows, halo, value_matrix, write_matrix, read_matrix, step_raw, new_rows, new_step, spike,
        value_filter_taps, write_filter_taps, read_filter_taps,
        head_log_decay, step_offset_bias, bypass_scale,
    )

    received = lax.all_to_all(send, "sp", 0, 0, tiled=True)

    base, lift, new_gate = call(
        inner_kernel,
        (shaped(length, channels), shaped(length, channels), shaped(8, channels)),
        grid=(blocks,),
        in_specs=[
            pl.BlockSpec((BLOCK, depth), lambda b: (b, 0)),
            pl.BlockSpec((depth, channels), lambda b: (0, 0)),
            pl.BlockSpec((1, depth), lambda b: (0, 0)),
            pl.BlockSpec((BLOCK, width), lambda b: (b, 0)),
            pl.BlockSpec((heads, BLOCK), lambda b: (0, b)),
            pl.BlockSpec((heads, BLOCK), lambda b: (0, b)),
            pl.BlockSpec((1, STATE, channels), lambda b: (b, 0, 0)),
            sm,
        ],
        out_specs=[
            pl.BlockSpec((BLOCK, channels), lambda b: (b, 0)),
            pl.BlockSpec((BLOCK, channels), lambda b: (b, 0)),
            pl.BlockSpec((8, channels), lambda b: (0, 0)),
        ],
        scratch=[pltpu.VMEM((heads, BLOCK), f32)],
        flops=2 * length * depth * channels,
        name="inner",
    )(tokens, gate_matrix, fresh, vwr, cum, dt, inside, bypass_scale)

    send_back, cache_rows, direct = call(
        prefix_kernel,
        (
            shaped(SUB, own, wide + channels, dtype=bf16),
            shaped(own, channels, dtype=bf16),
            shaped(1, channels),
        ),
        in_specs=[vm, vm, sm, sm],
        out_specs=[vm] * 3,
        scratch=[pltpu.VMEM((sequence_count, own, wide), f32)],
        name="prefix",
    )(received, new_step, head_log_decay, step_offset_bias)

    teams = [[SUB * t + i for i in range(SUB)] for t in range(pieces)]
    returned = lax.all_to_all(send_back, "sp", 0, 0, tiled=True, axis_index_groups=teams)

    prompt_out, step_row = call(
        finish_kernel,
        (
            shaped(length, channels, dtype=bf16),
            shaped(1, channels // sequence_count, dtype=bf16),
        ),
        grid=(1,),
        in_specs=[
            pl.BlockSpec(returned.shape, lambda i: (0, 0, 0)),
            pl.BlockSpec((length, channels), lambda i: (0, 0)),
            pl.BlockSpec((length, channels), lambda i: (0, 0)),
            pl.BlockSpec((length, STATE), lambda i: (0, (channels + STATE) // STATE)),
            pl.BlockSpec((1, group_norm_scale.shape[0]), lambda i: (0, 0)),
            pl.BlockSpec((1, channels), lambda i: (0, 0)),
            pl.BlockSpec((8, channels), lambda i: (0, 0)),
        ],
        out_specs=[
            pl.BlockSpec((length, channels), lambda i: (0, 0)),
            pl.BlockSpec((1, channels // sequence_count), lambda i: (0, 0)),
        ],
        name="finish",
    )(returned, base, lift, vwr, group_norm_scale[None], direct, new_gate)
    return (prompt_out, cache_rows, step_row.T)


def solution(mesh):
    placed = (
        P(("grp", "sp"), None),
        P("grp"),
        P(None, "tp"),
        P(None, "tp"),
        P(None, "tp"),
        P(None, "tp"),
        P(),
        P(),
        P(),
        P(),
        P(),
        P(),
        P(("grp", "sp"), "tp"),
        P(),
        P(),
    )
    return jax.shard_map(
        on_device,
        mesh=mesh,
        in_specs=placed,
        out_specs=(P(("grp", "sp"), "tp"), P(("grp", "sp"), "tp"), P(("grp", "tp"), "sp")),
        check_vma=False,
    )
```

time: 265 us -> 129 us (0.49)
  starting transfers between devices: 86.9 us -> 8.26 us
  waiting for transfers between devices: 59.6 us -> 4.17 us
  blocking collectives: 56.4 us -> 89.1 us
  Pallas kernels: 0 us -> 22.6 us
  other arithmetic: 21.9 us -> 0 us
  matrix products: 19.2 us -> 0 us
  local copies, waits for them, and re-layouts: 18 us -> 3.27 us
    all_to_all x0 -> x1, blocking collectives: none -> 89.1 us  [on_device(): received = lax.all_to_all(send, 'sp', 0, 0, tiled=True)]
    all_to_all x4 -> x1, starting transfers between devices: 73.1 us -> 3.56 us  [on_device(): lax.all_to_all(send_back, 'sp', 0, 0, tiled=True, axis_index_groups=teams)]
    psum x1 -> x0, blocking collectives: 56.4 us -> none  [from_root(): return lax.psum(kept, axis)]
    all_to_all x4 -> x1, waiting for transfers between devices: 59.6 us -> 4.17 us  [on_device(): lax.all_to_all(send_back, 'sp', 0, 0, tiled=True, axis_index_groups=teams)]
    pallas_call x0 -> x5, Pallas kernels: none -> 22.6 us  [the longest x1 6.68 us: on_device(): call(inner_kernel, (shaped(length, channels), shaped(length, channels), s...]
    dot_general x17 -> x0, matrix products: 19.2 us -> none  [the longest x8 11.1 us: project(): jnp.dot(operand, weights, preferred_element_type=jnp.float32)]
    ppermute x3 -> x1, starting transfers between devices: 13.8 us -> 4.7 us  [on_device(): lax.ppermute(tokens[length - HALO:], 'sp', [(i, i + 1) for i in range(seq...]
    convert_element_type x16 -> x0, other arithmetic: 7.83 us -> none  [the longest x1 2.17 us: on_device(): new_values.astype(jnp.float32).reshape(group_count, per_group, HEAD)]
  transfers between devices with their start and end apart: 7 -> 2, of which waited for: 3 -> 1; matrix products, arithmetic and copies ran while one was open for 16% -> 1% of each run, Pallas kernels for 0% -> 10%
where the time goes in v1:
time: 129 us; the launch traced here: 128 us
  blocking collectives  89.1 us (69%)
  Pallas kernels  22.6 us (18%)
  starting transfers between devices  8.26 us (6%)
  waiting for transfers between devices  4.17 us (3%)
  local copies, waits for them, and re-layouts  3.27 us (3%)
    all_to_all x1, blocking collectives, on_device(): received = lax.all_to_all(send, 'sp', 0, 0, tiled=True)  89.1 us
    pallas_call x1, Pallas kernels, on_device(): call(inner_kernel, (shaped(length, channels), shaped(length, channels), s...  6.68 us
    pallas_call x1, Pallas kernels, on_device(): call(local_kernel, (shaped(length, width, dtype=bf16), shaped(heads, leng...  6.04 us
    pallas_call x1, Pallas kernels, on_device(): call(project_kernel, (shaped(length, width, dtype=bf16), shaped(heads, le...  5.54 us
    ppermute x1, starting transfers between devices, on_device(): lax.ppermute(tokens[length - HALO:], 'sp', [(i, i + 1) for i in range(seq...  4.7 us
    all_to_all x1, waiting for transfers between devices, on_device(): lax.all_to_all(send_back, 'sp', 0, 0, tiled=True, axis_index_groups=teams)  4.17 us
    all_to_all x1, starting transfers between devices, on_device(): lax.all_to_all(send_back, 'sp', 0, 0, tiled=True, axis_index_groups=teams)  3.56 us
  transfers between devices with their start and end apart: 2, of which 1 were waited for; matrix products, arithmetic and copies ran while one was open for 1% of the time, Pallas kernels for 10%

profile of v1, /device:TPU:40, one launch (start us, length us, event | category | flops | bytes accessed | tf_op | source)
XLA Modules:
  0.0 128.0 jit_solution(7792963586880136698)
XLA Ops:
  0.6 0.8 slice.3
  1.4 4.7 %collective-permute-start = (bf16[8,2048]{1,0:T(8,128)(2,1)S(1)}, bf16[8,2048]{1,0:T(8,128)(2,1)S(1)}, u32[]{:S(2)}, u32[]{:S(2)}) collective-permute-start(bf16[8,2048]{1,0:T(8,128)(2,1)S(1)} %slice.3), channel_id=1, source_target_pairs={{0,8},{8,16},{16,24},{24,32},{32,40},{40,48},{48,56},{56,64},{64,7... | collective-permute-start | bytes 98312 | tf_op jit(solution)/shard_map/ppermute | solution.py:365
  6.1 1.3 %broadcast_in_dim.6.fresh_ref = bf16[1,2048]{1,0:T(2,128)(2,1)} reshape(bf16[2048]{0:T(1024)(128)(2,1)} %param.16) | data formatting | bytes 8192 | tf_op jit(solution)/shard_map/broadcast_in_dim | solution.py:368
  7.4 5.5 %project.1 = (bf16[512,512]{1,0:T(8,128)(2,1)}, f32[4,512]{1,0:T(4,128)}, f32[8,512]{1,0:T(8,128)}, f32[4,16]{1,0:T(4,128)}) custom-call(bf16[512,2048]{1,0:T(8,128)(2,1)} %tok_ref.3, bf16[1,2048]{1,0:T(2,128)(2,1)} %broadcast_in_dim.6.fresh_ref, bf16[2048,256]{1,0:T(8,128)(2,1)} %wv_ref.3, bf16[2048,128]{1,0:T(8,128)(2,1)} %ww_ref.3, ...), custom_call_target="tpu_custom_call" | custom-call | flops 1073741824 | bytes 1048576 | tf_op jit(solution)/shard_map/project/pallas_call | solution.py:371
  12.9 0.0 collective-permute-done.halo_ref
  12.9 0.0 copy-start.1
  12.9 0.6 copy-done.1
  13.5 6.0 %local.1 = (bf16[512,512]{1,0:T(8,128)(2,1)}, f32[4,512]{1,0:T(4,128)}, f32[4,512]{1,0:T(4,128)}, bf16[4,128,256]{2,1,0:T(8,128)(2,1)}, bf16[32,4,1152]{2,1,0:T(4,128)(2,1)}) custom-call(bf16[512,512]{1,0:T(8,128)(2,1)} %get-tuple-element.20.rows_ref, bf16[8,2048]{1,0:T(8,128)(2,1)} %copy-done.1, bf16[2048,256]{1,0:T(8,128)(2,1)} %wv_ref.3, ...), custom_call_target="tpu_custom_call" | custom-call | flops 33554432 | bytes 1048576 | tf_op jit(solution)/shard_map/local/pallas_call | solution.py:405
  19.6 89.1 %all_to_all.10.recv_ref = bf16[32,4,1152]{2,1,0:T(4,128)(2,1)} all-to-all(bf16[32,4,1152]{2,1,0:T(4,128)(2,1)} %get-tuple-element.24), channel_id=1, replica_groups=mesh['grp'=2,'sp'=32,'tp'=8] {'sp'}, dimensions={0} | all-to-all | bytes 589824 | tf_op jit(solution)/shard_map/all_to_all | solution.py:425
  108.6 2.0 %prefix.1 = (bf16[8,4,1280]{2,1,0:T(4,128)(2,1)}, bf16[4,256]{1,0:T(4,128)(2,1)}, f32[1,256]{1,0:T(1,128)}) custom-call(bf16[32,4,1152]{2,1,0:T(4,128)(2,1)} %all_to_all.10.recv_ref, f32[4,16]{1,0:T(4,128)} %get-tuple-element.23.newstep_ref, f32[32]{0:T(128)} %decay_ref.3, f32[32]{0:T(128)} %bias_ref.3), custom_call_target="tpu_custom_call" | custom-call | bytes 1048576 | tf_op jit(solution)/shard_map/prefix/pallas_call | solution.py:451
  110.7 3.6 %all-to-all-start.1 = ((bf16[8,4,1280]{2,1,0:T(4,128)(2,1)}), bf16[8,4,1280]{2,1,0:T(4,128)(2,1)S(1)}, u32[]{:S(2)}, u32[]{:S(2)}) async-start(bf16[8,4,1280]{2,1,0:T(4,128)(2,1)} %get-tuple-element.25), calls=%async_computation.1 | async-start | bytes 163840 | tf_op jit(solution)/shard_map/all_to_all | solution.py:465
  114.2 6.7 %inner.1 = (f32[512,256]{1,0:T(8,128)}, f32[512,256]{1,0:T(8,128)}, f32[8,256]{1,0:T(8,128)}) custom-call(bf16[512,2048]{1,0:T(8,128)(2,1)} %tok_ref.3, bf16[2048,256]{1,0:T(8,128)(2,1)} %wg_ref.1, bf16[1,2048]{1,0:T(2,128)(2,1)} %broadcast_in_dim.6.fresh_ref, bf16[512,512]{1,0:T(8,128)(2,1)} %get-tuple-element.26.vwr_ref.reads_ref, ...), custom_call_target="tpu_custom_call" | custom-call | flops 536870912 | bytes 1048576 | tf_op jit(solution)/shard_map/inner/pallas_call | solution.py:427
  120.9 4.2 %all-to-all-done.1.recv_ref = bf16[8,4,1280]{2,1,0:T(4,128)(2,1)S(1)} async-done(((bf16[8,4,1280]{2,1,0:T(4,128)(2,1)}), bf16[8,4,1280]{2,1,0:T(4,128)(2,1)S(1)}, u32[]{:S(2)}, u32[]{:S(2)}) %all-to-all-start.1) | async-done | bytes 81952 | tf_op jit(solution)/shard_map/all_to_all | solution.py:465
  125.1 0.0 copy-start
  125.1 0.6 copy-done
  125.7 2.3 %finish.1 = (bf16[512,256]{1,0:T(8,128)(2,1)}, bf16[1,8]{1,0:T(2,128)(2,1)}) custom-call(bf16[8,4,1280]{2,1,0:T(4,128)(2,1)} %copy-done, f32[512,256]{1,0:T(8,128)} %get-tuple-element.30.base_ref, f32[512,256]{1,0:T(8,128)} %get-tuple-element.31.lift_ref, bf16[512,512]{1,0:T(8,128)(2,1)} %get-tuple-element.26.vwr_ref.reads_ref, f32[1,2048]{1,0:T(1,128)} %bitcast.6, ...), custom_call_target="tpu_custom_call" | custom-call | bytes 1048576 | tf_op jit(solution)/shard_map/finish/pallas_call | solution.py:467
Async XLA Ops:
  1.4 11.5 %collective-permute-start = (bf16[8,2048]{1,0:T(8,128)(2,1)S(1)}, bf16[8,2048]{1,0:T(8,128)(2,1)S(1)}, u32[]{:S(2)}, u32[]{:S(2)}) collective-permute-start(bf16[8,2048]{1,0:T(8,128)(2,1)S(1)} %slice.3), channel_id=1, source_target_pairs={{0,8},{8,16},{16,24},{24,32},{32,40},{40,48},{48,56},{56,64},{64,7... | collective-permute-start | bytes 98312 | tf_op jit(solution)/shard_map/ppermute | solution.py:365
  12.9 0.6 copy-start.1
  110.7 14.4 %all-to-all-start.1 = ((bf16[8,4,1280]{2,1,0:T(4,128)(2,1)}), bf16[8,4,1280]{2,1,0:T(4,128)(2,1)S(1)}, u32[]{:S(2)}, u32[]{:S(2)}) async-start(bf16[8,4,1280]{2,1,0:T(4,128)(2,1)} %get-tuple-element.25), calls=%async_computation.1 | async-start | bytes 163840 | tf_op jit(solution)/shard_map/all_to_all | solution.py:465
  125.1 0.6 copy-start

commit v2 on v1

--- a/solution.py
+++ b/solution.py
@@ -9,7 +9,7 @@
 STATE = 128
 CONV = 4
 BLOCK = 128
-SUB = 8
+SUB = 32
 MISC = 128
 HALO = 8
 
@@ -462,6 +462,7 @@
     )(received, new_step, head_log_decay, step_offset_bias)
 
     teams = [[SUB * t + i for i in range(SUB)] for t in range(pieces)]
+    teams = teams if pieces > 1 else None
     returned = lax.all_to_all(send_back, "sp", 0, 0, tiled=True, axis_index_groups=teams)
 
     prompt_out, step_row = call(

time: 129 us -> 131 us (1.016)
  waiting for transfers between devices: 4.17 us -> 21.9 us
  blocking collectives: 89.1 us -> 72.4 us
    all_to_all x1, waiting for transfers between devices: 4.17 us -> 21.9 us  [on_device(): lax.all_to_all(send_back, 'sp', 0, 0, tiled=True, axis_index_groups=teams)]
    all_to_all x1, blocking collectives: 89.1 us -> 72.4 us  [on_device(): received = lax.all_to_all(send, 'sp', 0, 0, tiled=True)]
  transfers between devices with their start and end apart: 2 -> 2, of which waited for: 1 -> 1; matrix products, arithmetic and copies ran while one was open for 1% -> 1% of each run, Pallas kernels for 10% -> 9%
where the time goes in v2:
time: 131 us; the launch traced here: 130 us
  blocking collectives  72.4 us (55%)
  Pallas kernels  22.4 us (17%)
  waiting for transfers between devices  21.9 us (17%)
  starting transfers between devices  9.47 us (7%)
  local copies, waits for them, and re-layouts  3.3 us (3%)
    all_to_all x1, blocking collectives, on_device(): received = lax.all_to_all(send, 'sp', 0, 0, tiled=True)  72.4 us
    all_to_all x1, waiting for transfers between devices, on_device(): lax.all_to_all(send_back, 'sp', 0, 0, tiled=True, axis_index_groups=teams)  21.9 us
    pallas_call x1, Pallas kernels, on_device(): call(inner_kernel, (shaped(length, channels), shaped(length, channels), s...  6.68 us
    pallas_call x1, Pallas kernels, on_device(): call(local_kernel, (shaped(length, width, dtype=bf16), shaped(heads, leng...  5.92 us
    pallas_call x1, Pallas kernels, on_device(): call(project_kernel, (shaped(length, width, dtype=bf16), shaped(heads, le...  5.53 us
    all_to_all x1, starting transfers between devices, on_device(): lax.all_to_all(send_back, 'sp', 0, 0, tiled=True, axis_index_groups=teams)  4.77 us
    ppermute x1, starting transfers between devices, on_device(): lax.ppermute(tokens[length - HALO:], 'sp', [(i, i + 1) for i in range(seq...  4.7 us
  transfers between devices with their start and end apart: 2, of which 1 were waited for; matrix products, arithmetic and copies ran while one was open for 1% of the time, Pallas kernels for 9%

profile of v2, /device:TPU:40, one launch (start us, length us, event | category | flops | bytes accessed | tf_op | source)
XLA Modules:
  0.0 130.1 jit_solution(15965645022676570760)
XLA Ops:
  0.6 0.8 slice.3
  1.4 4.7 %collective-permute-start = (bf16[8,2048]{1,0:T(8,128)(2,1)S(1)}, bf16[8,2048]{1,0:T(8,128)(2,1)S(1)}, u32[]{:S(2)}, u32[]{:S(2)}) collective-permute-start(bf16[8,2048]{1,0:T(8,128)(2,1)S(1)} %slice.3), channel_id=1, source_target_pairs={{0,8},{8,16},{16,24},{24,32},{32,40},{40,48},{48,56},{56,64},{64,7... | collective-permute-start | bytes 98312 | tf_op jit(solution)/shard_map/ppermute | solution.py:365
  6.1 1.3 broadcast_in_dim.6.fresh_ref
  7.4 5.5 %project.1 = (bf16[512,512]{1,0:T(8,128)(2,1)}, f32[4,512]{1,0:T(4,128)}, f32[8,512]{1,0:T(8,128)}, f32[4,16]{1,0:T(4,128)}) custom-call(bf16[512,2048]{1,0:T(8,128)(2,1)} %tok_ref.3, bf16[1,2048]{1,0:T(2,128)(2,1)} %broadcast_in_dim.6.fresh_ref, bf16[2048,256]{1,0:T(8,128)(2,1)} %wv_ref.3, bf16[2048,128]{1,0:T(8,128)(2,1)} %ww_ref.3, ...), custom_call_target="tpu_custom_call" | custom-call | flops 1073741824 | bytes 1048576 | tf_op jit(solution)/shard_map/project/pallas_call | solution.py:371
  12.9 0.0 collective-permute-done.halo_ref
  12.9 0.0 copy-start.1
  12.9 0.6 copy-done.1
  13.5 5.9 %local.1 = (bf16[512,512]{1,0:T(8,128)(2,1)}, f32[4,512]{1,0:T(4,128)}, f32[4,512]{1,0:T(4,128)}, bf16[4,128,256]{2,1,0:T(8,128)(2,1)}, bf16[32,4,384]{2,1,0:T(4,128)(2,1)}) custom-call(bf16[512,512]{1,0:T(8,128)(2,1)} %get-tuple-element.20.rows_ref, bf16[8,2048]{1,0:T(8,128)(2,1)} %copy-done.1, bf16[2048,256]{1,0:T(8,128)(2,1)} %wv_ref.3, ...), custom_call_target="tpu_custom_call" | custom-call | flops 33554432 | bytes 1048576 | tf_op jit(solution)/shard_map/local/pallas_call | solution.py:405
  19.5 72.4 %all_to_all.10.recv_ref = bf16[32,4,384]{2,1,0:T(4,128)(2,1)} all-to-all(bf16[32,4,384]{2,1,0:T(4,128)(2,1)} %get-tuple-element.24), channel_id=1, replica_groups=mesh['grp'=2,'sp'=32,'tp'=8] {'sp'}, dimensions={0} | all-to-all | bytes 196608 | tf_op jit(solution)/shard_map/all_to_all | solution.py:425
  91.8 1.9 %prefix.1 = (bf16[32,4,512]{2,1,0:T(4,128)(2,1)}, bf16[4,256]{1,0:T(4,128)(2,1)}, f32[1,256]{1,0:T(1,128)}) custom-call(bf16[32,4,384]{2,1,0:T(4,128)(2,1)} %all_to_all.10.recv_ref, f32[4,16]{1,0:T(4,128)} %get-tuple-element.23.newstep_ref, f32[32]{0:T(128)} %decay_ref.3, f32[32]{0:T(128)} %bias_ref.3), custom_call_target="tpu_custom_call" | custom-call | bytes 1048576 | tf_op jit(solution)/shard_map/prefix/pallas_call | solution.py:451
  93.8 4.8 %all-to-all-start.1 = ((bf16[32,4,512]{2,1,0:T(4,128)(2,1)}), bf16[32,4,512]{2,1,0:T(4,128)(2,1)S(1)}, u32[]{:S(2)}, u32[]{:S(2)}) async-start(bf16[32,4,512]{2,1,0:T(4,128)(2,1)} %get-tuple-element.25), calls=%async_computation.1 | async-start | bytes 262144 | tf_op jit(solution)/shard_map/all_to_all | solution.py:466
  98.5 6.7 %inner.1 = (f32[512,256]{1,0:T(8,128)}, f32[512,256]{1,0:T(8,128)}, f32[8,256]{1,0:T(8,128)}) custom-call(bf16[512,2048]{1,0:T(8,128)(2,1)} %tok_ref.3, bf16[2048,256]{1,0:T(8,128)(2,1)} %wg_ref.1, bf16[1,2048]{1,0:T(2,128)(2,1)} %broadcast_in_dim.6.fresh_ref, bf16[512,512]{1,0:T(8,128)(2,1)} %get-tuple-element.26.vwr_ref.reads_ref, ...), custom_call_target="tpu_custom_call" | custom-call | flops 536870912 | bytes 1048576 | tf_op jit(solution)/shard_map/inner/pallas_call | solution.py:427
  105.2 21.9 %all-to-all-done.1.recv_ref = bf16[32,4,512]{2,1,0:T(4,128)(2,1)S(1)} async-done(((bf16[32,4,512]{2,1,0:T(4,128)(2,1)}), bf16[32,4,512]{2,1,0:T(4,128)(2,1)S(1)}, u32[]{:S(2)}, u32[]{:S(2)}) %all-to-all-start.1) | async-done | bytes 131104 | tf_op jit(solution)/shard_map/all_to_all | solution.py:466
  127.1 0.0 copy-start
  127.1 0.7 copy-done
  127.8 2.3 %finish.1 = (bf16[512,256]{1,0:T(8,128)(2,1)}, bf16[1,8]{1,0:T(2,128)(2,1)}) custom-call(bf16[32,4,512]{2,1,0:T(4,128)(2,1)} %copy-done, f32[512,256]{1,0:T(8,128)} %get-tuple-element.30.base_ref, f32[512,256]{1,0:T(8,128)} %get-tuple-element.31.lift_ref, bf16[512,512]{1,0:T(8,128)(2,1)} %get-tuple-element.26.vwr_ref.reads_ref, f32[1,2048]{1,0:T(1,128)} %bitcast.6, ...), custom_call_target="tpu_custom_call" | custom-call | bytes 1048576 | tf_op jit(solution)/shard_map/finish/pallas_call | solution.py:468
Async XLA Ops:
  1.4 11.5 %collective-permute-start = (bf16[8,2048]{1,0:T(8,128)(2,1)S(1)}, bf16[8,2048]{1,0:T(8,128)(2,1)S(1)}, u32[]{:S(2)}, u32[]{:S(2)}) collective-permute-start(bf16[8,2048]{1,0:T(8,128)(2,1)S(1)} %slice.3), channel_id=1, source_target_pairs={{0,8},{8,16},{16,24},{24,32},{32,40},{40,48},{48,56},{56,64},{64,7... | collective-permute-start | bytes 98312 | tf_op jit(solution)/shard_map/ppermute | solution.py:365
  12.9 0.6 copy-start.1
  93.8 33.4 %all-to-all-start.1 = ((bf16[32,4,512]{2,1,0:T(4,128)(2,1)}), bf16[32,4,512]{2,1,0:T(4,128)(2,1)S(1)}, u32[]{:S(2)}, u32[]{:S(2)}) async-start(bf16[32,4,512]{2,1,0:T(4,128)(2,1)} %get-tuple-element.25), calls=%async_computation.1 | async-start | bytes 262144 | tf_op jit(solution)/shard_map/all_to_all | solution.py:466
  127.1 0.7 copy-start

commit v3 on v1

--- a/solution.py
+++ b/solution.py
@@ -9,7 +9,7 @@
 STATE = 128
 CONV = 4
 BLOCK = 128
-SUB = 8
+TEAM = 8
 MISC = 128
 HALO = 8
 
@@ -17,7 +17,8 @@
 f32 = jnp.float32
 bf16 = jnp.bfloat16
 HIGHEST = lax.Precision.HIGHEST
-VMEM_LIMIT = 56 * 1024 * 1024
+VMEM_LIMIT = 24 * 1024 * 1024
+SPLIT = 4
 
 
 def dot(a, b, dims=((1,), (0,)), precision=None):
@@ -56,57 +57,64 @@
 
 
 def project_kernel(
-    tok_ref, fresh_ref, wv_ref, ww_ref, wr_ref, ws_ref, rows_ref, step_ref, new_ref, newstep_ref,
-    acc, accs, accn, accns,
+    tok_hbm, fresh_ref, wv_hbm, ww_hbm, wr_hbm, ws_ref,
+    rows_ref, weights, step_ref, new_ref, newstep_ref, tok, sems,
 ):
-    k = pl.program_id(0)
-    last = pl.num_programs(0) - 1
-    tok = tok_ref[...]
-    fresh = jnp.broadcast_to(fresh_ref[...], (16, fresh_ref.shape[1]))
-    weights = jnp.concatenate([wv_ref[...], ww_ref[...], wr_ref[...]], axis=1)
-    part = dot(tok, weights)
-    parts = dot(ws_ref[...], tok, ((1,), (1,)))
-    partn = dot(fresh, weights)
-    partns = dot(ws_ref[...], fresh, ((1,), (1,)))
-
-    @pl.when(k == 0)
-    def _():
-        acc[...] = part
-        accs[...] = parts
-        accn[...] = partn
-        accns[...] = partns
-
-    @pl.when(k > 0)
-    def _():
-        acc[...] += part
-        accs[...] += parts
-        accn[...] += partn
-        accns[...] += partns
-
-    @pl.when(k == last)
-    def _():
-        rank = lax.axis_index("tp")
-        heads = step_ref.shape[0]
-        rows_ref[...] = acc[...].astype(bf16)
-        step_ref[...] = own_rows(accs[...], rank, heads)
-        new_ref[...] = accn[...][0:8]
-        newstep_ref[...] = own_rows(accns[...], rank, heads)
+    depth = tok.shape[1]
+    channels = wv_hbm.shape[1]
+    state = ww_hbm.shape[1]
+    chunk = depth // SPLIT
+    copies = []
+    for k in range(SPLIT):
+        at = pl.ds(k * chunk, chunk)
+        moves = [
+            (tok_hbm.at[:, at], tok.at[:, at]),
+            (wv_hbm.at[at], weights.at[at, 0:channels]),
+            (ww_hbm.at[at], weights.at[at, channels : channels + state]),
+            (wr_hbm.at[at], weights.at[at, channels + state : channels + 2 * state]),
+        ]
+        copies.append(
+            [pltpu.make_async_copy(a, b, sems.at[k, i]) for i, (a, b) in enumerate(moves)]
+        )
+        for copy in copies[-1]:
+            copy.start()
+    rank = lax.axis_index("tp")
+    heads = step_ref.shape[0]
+    acc = accs = accn = accns = None
+    lines = fresh_ref[...].astype(f32)
+    for k in range(SPLIT):
+        at = slice(k * chunk, (k + 1) * chunk)
+        each = chunk // 128
+        fresh = jnp.concatenate([lines[k * each + i : k * each + i + 1] for i in range(each)], axis=1)
+        fresh = jnp.broadcast_to(fresh, (8, chunk)).astype(bf16)
+        for copy in copies[k]:
+            copy.wait()
+        part = dot(tok[:, at], weights[at])
+        parts = dot(ws_ref[:, at], tok[:, at], ((1,), (1,)))
+        partn = dot(fresh, weights[at])
+        partns = dot(ws_ref[:, at], fresh, ((1,), (1,)))
+        acc = part if k == 0 else acc + part
+        accs = parts if k == 0 else accs + parts
+        accn = partn if k == 0 else accn + partn
+        accns = partns if k == 0 else accns + partns
+    rows_ref[...] = acc.astype(bf16)
+    step_ref[...] = own_rows(accs, rank, heads)
+    new_ref[...] = accn
+    newstep_ref[...] = own_rows(accns, rank, heads)
 
 
 def local_kernel(
-    rows_ref, halo_ref, wv_ref, ww_ref, wr_ref, step_ref, new_ref, newstep_ref, spike_ref,
+    rows_ref, halo_ref, weights, step_ref, new_ref, newstep_ref, spike_ref,
     vtap_ref, wtap_ref, rtap_ref, decay_ref, bias_ref, skip_ref,
     vwr_ref, cum_ref, dt_ref, inside_ref, send_ref, ext,
 ):
     rank = lax.axis_index("tp")
     length = rows_ref.shape[0]
     heads = step_ref.shape[0]
-    channels = wv_ref.shape[1]
+    channels = rows_ref.shape[1] - 2 * STATE
     first = rank * heads
     halo = halo_ref[...]
-    before = jnp.concatenate(
-        [dot(halo, wv_ref[...]), dot(halo, ww_ref[...]), dot(halo, wr_ref[...])], axis=1
-    )
+    before = dot(halo, weights[...])
     ext[0:HALO] = before.astype(bf16).astype(f32)
     ext[HALO:] = rows_ref[...].astype(f32)
     taps = jnp.concatenate(
@@ -163,7 +171,8 @@
         misc = jnp.where(lanes == h, high[h : h + 1, 0:1], misc)
         misc = jnp.where(lanes == heads + h, low[h : h + 1, 0:1], misc)
     own = STATE // lax.axis_size("sp")
-    stretch = SUB * own
+    stretch = TEAM * own
+    teams = STATE // stretch
     diagonal = jnp.where(rows == lanes, jnp.broadcast_to(new_read, shape), 0.0)
     read_column = jnp.sum(diagonal, axis=1, keepdims=True)
     new_dt = softplus(newstep_ref[...][:, 0:1] + bias[:, 0:1])
@@ -173,20 +182,17 @@
     placed = jnp.where(iota((8, channels), 0) == iota((8, channels), 1) // HEAD, direct, 0.0)
     shift = (iota((channels, MISC), 0) % HEAD + (MISC - HEAD) == iota((channels, MISC), 1)).astype(f32)
     direct_rows = dot(placed, shift, precision=HIGHEST)[0:own]
-    for g in range(STATE // stretch):
+    for g in range(teams):
         at = slice(g * stretch, (g + 1) * stretch)
-        piece = running[at].reshape(SUB, own, channels).astype(bf16)
-        for copy in range(STATE // stretch):
-            send_ref[copy * SUB : (copy + 1) * SUB, :, g * channels : (g + 1) * channels] = piece
+        piece = running[at].reshape(TEAM, own, channels).astype(bf16)
+        send_ref[:, :, g * channels : (g + 1) * channels] = piece
     note = misc[0:stretch]
-    for g in range(STATE // stretch):
+    for g in range(teams):
         at = slice(g * stretch, (g + 1) * stretch)
         note = jnp.where(lanes[0:stretch] == 2 * heads + g, read_column[at], note)
-    note = note.reshape(SUB, own, MISC)
+    note = note.reshape(TEAM, own, MISC)
     note = jnp.where(iota(note.shape, 2) >= MISC - HEAD, direct_rows[None], note).astype(bf16)
-    wide = STATE // stretch * channels
-    for copy in range(STATE // stretch):
-        send_ref[copy * SUB : (copy + 1) * SUB, :, wide:] = note
+    send_ref[:, :, teams * channels :] = note
 
 
 def inner_kernel(
@@ -201,8 +207,10 @@
     @pl.when(b == 0)
     def _():
         before[...] = jnp.zeros_like(before)
-        fresh = jnp.broadcast_to(fresh_ref[...], (16, fresh_ref.shape[1]))
-        gate = dot(fresh, wg_ref[...])[0:8].astype(bf16).astype(f32)
+        lines = fresh_ref[...].astype(f32)
+        fresh = jnp.concatenate([lines[i : i + 1] for i in range(lines.shape[0])], axis=1)
+        fresh = jnp.broadcast_to(fresh, (8, fresh.shape[1])).astype(bf16)
+        gate = dot(fresh, wg_ref[...]).astype(bf16).astype(f32)
         newgate_ref[...] = silu(gate)
 
     expand = spread(heads, channels)
@@ -232,36 +240,72 @@
     before[...] += jnp.broadcast_to(cum[:, BLOCK - 1 :], before.shape)
 
 
-def prefix_kernel(recv_ref, newstep_ref, decay_ref, bias_ref, send_ref, cache_ref, direct_ref, states):
-    rank = lax.axis_index("tp")
-    place = lax.axis_index("sp")
-    count = recv_ref.shape[0]
-    own = recv_ref.shape[1]
-    wide = recv_ref.shape[2] - MISC
-    pieces = count // SUB
-    channels = wide // pieces
-    heads = channels // HEAD
-    group = place // SUB
-    notes = recv_ref[:, 0:1, wide:].astype(f32).reshape(count, MISC)
+def fades_of(notes, heads, channels):
     lane = iota((MISC, channels), 0)
     owner = iota((MISC, channels), 1) // HEAD
     pick = jnp.where((lane == owner) | (lane == owner + heads), 1.0, 0.0)
-    fades = dot(jnp.where(iota(notes.shape, 1) < 2 * heads, notes, 0.0), pick, precision=HIGHEST)
+    return dot(jnp.where(iota(notes.shape, 1) < 2 * heads, notes, 0.0), pick, precision=HIGHEST)
+
+
+def team_kernel(recv_ref, send_ref, local_ref, reach_ref):
+    count, own, width = recv_ref.shape
+    wide = width - MISC
+    teams = send_ref.shape[0]
+    channels = wide // teams
+    heads = channels // HEAD
+    notes = recv_ref[:, 0:1, wide:].astype(f32).reshape(count, MISC)
+    fades = fades_of(notes, heads, channels)
     state = jnp.zeros((own, wide), f32)
+    reach = jnp.ones((1, channels), f32)
     for k in range(count):
-        states[k] = state
-        fade = jnp.concatenate([fades[k : k + 1]] * pieces, axis=1)
+        local_ref[k] = state
+        reach_ref[k : k + 1] = reach
+        fade = jnp.concatenate([fades[k : k + 1]] * teams, axis=1)
         state = fade * state + recv_ref[k, :, 0:wide].astype(f32)
-    kept = state.astype(bf16)
+        reach = reach * fades[k : k + 1]
+    total = state.astype(bf16)
+    note = recv_ref[count - 1, :, wide:].astype(f32)
+    first = (iota((channels, MISC), 0) == iota((channels, MISC), 1) * HEAD).astype(f32)
+    high = reach.astype(bf16).astype(f32)
+    low = reach - high
+    packed = dot(jnp.concatenate([high, low, jnp.zeros((6, channels), f32)], axis=0), first, precision=HIGHEST)
+    shifted = (iota((MISC, MISC), 0) + heads == iota((MISC, MISC), 1)).astype(f32)
+    moved = dot(packed, shifted, precision=HIGHEST)
+    lanes = iota((own, MISC), 1)
+    note = jnp.where(lanes < heads, packed[0:1], jnp.where(lanes < 2 * heads, moved[1:2], note)).astype(bf16)
+    for t in range(teams):
+        send_ref[t, :, 0:wide] = total
+        send_ref[t, :, wide:] = note
+
+
+def prefix_kernel(recv_ref, local_ref, reach_ref, newstep_ref, decay_ref, bias_ref, send_ref, cache_ref, direct_ref):
+    rank = lax.axis_index("tp")
+    teams, own, width = recv_ref.shape
+    wide = width - MISC
+    channels = wide // teams
+    heads = channels // HEAD
+    group = lax.axis_index("sp") // TEAM
+    notes = recv_ref[:, 0:1, wide:].astype(f32).reshape(teams, MISC)
+    fades = fades_of(notes, heads, channels)
+    state = jnp.zeros((own, wide), f32)
+    entering = state
+    for t in range(teams):
+        entering = jnp.where(group == t, state, entering)
+        fade = jnp.concatenate([fades[t : t + 1]] * teams, axis=1)
+        state = fade * state + recv_ref[t, :, 0:wide].astype(f32)
+    for k in range(TEAM):
+        reach = jnp.concatenate([reach_ref[k : k + 1]] * teams, axis=1)
+        send_ref[k, :, 0:wide] = (local_ref[k] + reach * entering).astype(bf16)
+    kept = state.astype(bf16).astype(f32)
     mine = kept[:, 0:channels]
-    for g in range(1, pieces):
+    for g in range(1, teams):
         mine = jnp.where(group == g, kept[:, g * channels : (g + 1) * channels], mine)
-    cache_ref[...] = mine
-    note = recv_ref[count - 1, :, wide:].astype(f32)
+    cache_ref[...] = mine.astype(bf16)
+    note = recv_ref[teams - 1, :, wide:].astype(f32)
     reading = jnp.zeros((own, channels), f32)
-    for g in range(pieces):
+    for g in range(teams):
         column = note[:, 2 * heads + g : 2 * heads + g + 1]
-        reading = reading + column * kept[:, g * channels : (g + 1) * channels].astype(f32)
+        reading = reading + column * kept[:, g * channels : (g + 1) * channels]
     first = rank * heads
     bias = head_column(bias_ref, first, heads, 1)
     rate = jnp.exp(head_column(decay_ref, first, heads, 1))
@@ -272,9 +316,7 @@
     low = partial - high
     rows = iota((own, channels), 0)
     share = jnp.where(rows == 0, high, jnp.where(rows == 1, low, 0.0)).astype(bf16)
-    chosen = states[pl.ds(group * SUB, SUB)]
-    send_ref[:, :, 0:wide] = chosen.astype(bf16)
-    send_ref[:, :, wide:] = jnp.broadcast_to(share[None], (SUB, own, channels))
+    send_ref[:, :, wide:] = jnp.broadcast_to(share[None], (TEAM, own, channels))
     unshift = (iota((MISC, channels), 0) == iota((MISC, channels), 1) % HEAD + (MISC - HEAD)).astype(f32)
     laid = dot(note, unshift, precision=HIGHEST)
     direct_ref[...] = jnp.sum(jnp.where(rows == iota(rows.shape, 1) // HEAD, laid, 0.0), axis=0, keepdims=True)
@@ -289,13 +331,13 @@
     own = recv_ref.shape[1]
     earlier = jnp.concatenate(
         [
-            recv_ref[:, :, g * channels : (g + 1) * channels].astype(f32).reshape(SUB * own, channels)
+            recv_ref[:, :, g * channels : (g + 1) * channels].astype(f32).reshape(TEAM * own, channels)
             for g in range(pieces)
         ],
         axis=0,
     ).astype(bf16)
     gain = gain_ref[:, pl.ds(pl.multiple_of(rank * channels, 128), channels)]
-    gated = base_ref[...] + dot(reads_ref[...], earlier) * lift_ref[...]
+    gated = base_ref[...] + dot(reads_ref[:, channels + STATE :], earlier) * lift_ref[...]
     scale = lax.rsqrt(jnp.mean(gated * gated, axis=1, keepdims=True) + epsilon)
     out_ref[...] = (gated * scale * gain).astype(bf16)
     partial = jnp.sum(jnp.sum(recv_ref[:, :, wide:].astype(f32), axis=0), axis=0, keepdims=True)
@@ -331,6 +373,18 @@
 
 def shaped(*shape, dtype=f32):
     return jax.ShapeDtypeStruct(shape, dtype)
+
+
+def near(*shape, dtype=f32):
+    return pltpu.VMEM(shape, dtype)
+
+
+def held(array):
+    return pltpu.with_memory_space_constraint(array, pltpu.VMEM)
+
+
+def stored(array):
+    return pltpu.with_memory_space_constraint(array, pltpu.HBM)
 
 
 def on_device(
@@ -354,84 +408,85 @@
     length, depth = tokens.shape
     channels = value_matrix.shape[1]
     heads = channels // HEAD
-    all_heads = step_matrix.shape[1]
     own = STATE // sequence_count
-    pieces = sequence_count // SUB
+    teams = sequence_count // TEAM
     blocks = length // BLOCK
     width = channels + 2 * STATE
+    wide = teams * channels
     vm = pl.BlockSpec(memory_space=pltpu.VMEM)
     sm = pl.BlockSpec(memory_space=pltpu.SMEM)
+    far = pl.BlockSpec(memory_space=pltpu.HBM)
+    inside_team = [[TEAM * t + i for i in range(TEAM)] for t in range(teams)]
+    across_teams = [[TEAM * t + i for t in range(teams)] for i in range(TEAM)]
 
     halo = lax.ppermute(
         tokens[length - HALO :], "sp", [(i, i + 1) for i in range(sequence_count - 1)]
     )
-    fresh = fresh_token_input[None]
+    fresh = fresh_token_input.reshape(depth // 128, 128)
     spike = decay_spike.T
-    chunk = depth // 4
-    rows, step_raw, new_rows, new_step = call(
+    rows, weights, step_raw, new_rows, new_step = call(
         project_kernel,
         (
-            shaped(length, width, dtype=bf16),
-            shaped(heads, length),
-            shaped(8, width),
-            shaped(heads, 16),
-        ),
-        grid=(depth // chunk,),
-        in_specs=[
-            pl.BlockSpec((length, chunk), lambda k: (0, k)),
-            pl.BlockSpec((1, chunk), lambda k: (0, k)),
-            pl.BlockSpec((chunk, channels), lambda k: (k, 0)),
-            pl.BlockSpec((chunk, STATE), lambda k: (k, 0)),
-            pl.BlockSpec((chunk, STATE), lambda k: (k, 0)),
-            pl.BlockSpec((all_heads, chunk), lambda k: (0, k)),
-        ],
-        out_specs=[
-            pl.BlockSpec((length, width), lambda k: (0, 0)),
-            pl.BlockSpec((heads, length), lambda k: (0, 0)),
-            pl.BlockSpec((8, width), lambda k: (0, 0)),
-            pl.BlockSpec((heads, 16), lambda k: (0, 0)),
-        ],
-        scratch=[
-            pltpu.VMEM((length, width), f32),
-            pltpu.VMEM((all_heads, length), f32),
-            pltpu.VMEM((16, width), f32),
-            pltpu.VMEM((all_heads, 16), f32),
-        ],
+            near(length, width, dtype=bf16),
+            near(depth, width, dtype=bf16),
+            near(heads, length),
+            near(8, width),
+            near(heads, 8),
+        ),
+        in_specs=[far, vm, far, far, far, vm],
+        out_specs=[vm] * 5,
+        scratch=[pltpu.VMEM((length, depth), bf16), pltpu.SemaphoreType.DMA((SPLIT, 4))],
         flops=2 * length * depth * width,
         name="project",
-    )(tokens, fresh, value_matrix, write_matrix, read_matrix, step_matrix.T)
-
-    wide = pieces * channels
+    )(
+        stored(tokens), fresh, stored(value_matrix), stored(write_matrix), stored(read_matrix),
+        step_matrix.T,
+    )
+
     vwr, cum, dt, inside, send = call(
         local_kernel,
         (
-            shaped(length, width, dtype=bf16),
-            shaped(heads, length),
-            shaped(heads, length),
-            shaped(blocks, STATE, channels, dtype=bf16),
-            shaped(sequence_count, own, wide + MISC, dtype=bf16),
-        ),
-        in_specs=[vm] * 12 + [sm] * 3,
+            near(length, width, dtype=bf16),
+            near(heads, length),
+            near(heads, length),
+            near(blocks, STATE, channels, dtype=bf16),
+            near(TEAM, own, wide + MISC, dtype=bf16),
+        ),
+        in_specs=[vm] * 10 + [sm] * 3,
         out_specs=[vm] * 5,
         scratch=[pltpu.VMEM((length + HALO, width), f32)],
         flops=2 * length * STATE * channels,
         name="local",
     )(
-        rows, halo, value_matrix, write_matrix, read_matrix, step_raw, new_rows, new_step, spike,
+        held(rows), held(halo), held(weights), held(step_raw), held(new_rows), held(new_step), spike,
         value_filter_taps, write_filter_taps, read_filter_taps,
         head_log_decay, step_offset_bias, bypass_scale,
     )
 
-    received = lax.all_to_all(send, "sp", 0, 0, tiled=True)
+    received = lax.all_to_all(held(send), "sp", 0, 0, tiled=True, axis_index_groups=inside_team)
+
+    send, local_states, reach = call(
+        team_kernel,
+        (
+            near(teams, own, wide + MISC, dtype=bf16),
+            near(TEAM, own, wide),
+            near(TEAM, channels),
+        ),
+        in_specs=[vm],
+        out_specs=[vm] * 3,
+        name="team",
+    )(held(received))
+
+    received = lax.all_to_all(held(send), "sp", 0, 0, tiled=True, axis_index_groups=across_teams)
 
     base, lift, new_gate = call(
         inner_kernel,
-        (shaped(length, channels), shaped(length, channels), shaped(8, channels)),
+        (near(length, channels), near(length, channels), near(8, channels)),
         grid=(blocks,),
         in_specs=[
             pl.BlockSpec((BLOCK, depth), lambda b: (b, 0)),
             pl.BlockSpec((depth, channels), lambda b: (0, 0)),
-            pl.BlockSpec((1, depth), lambda b: (0, 0)),
+            pl.BlockSpec((depth // 128, 128), lambda b: (0, 0)),
             pl.BlockSpec((BLOCK, width), lambda b: (b, 0)),
             pl.BlockSpec((heads, BLOCK), lambda b: (0, b)),
             pl.BlockSpec((heads, BLOCK), lambda b: (0, b)),
@@ -446,23 +501,24 @@
         scratch=[pltpu.VMEM((heads, BLOCK), f32)],
         flops=2 * length * depth * channels,
         name="inner",
-    )(tokens, gate_matrix, fresh, vwr, cum, dt, inside, bypass_scale)
-
-    send_back, cache_rows, direct = call(
+    )(
+        stored(tokens), stored(gate_matrix), fresh, held(vwr), held(cum), held(dt), held(inside),
+        bypass_scale,
+    )
+
+    send, cache_rows, direct = call(
         prefix_kernel,
         (
-            shaped(SUB, own, wide + channels, dtype=bf16),
+            near(TEAM, own, wide + channels, dtype=bf16),
             shaped(own, channels, dtype=bf16),
-            shaped(1, channels),
-        ),
-        in_specs=[vm, vm, sm, sm],
+            near(1, channels),
+        ),
+        in_specs=[vm] * 4 + [sm] * 2,
         out_specs=[vm] * 3,
-        scratch=[pltpu.VMEM((sequence_count, own, wide), f32)],
         name="prefix",
-    )(received, new_step, head_log_decay, step_offset_bias)
-
-    teams = [[SUB * t + i for i in range(SUB)] for t in range(pieces)]
-    returned = lax.all_to_all(send_back, "sp", 0, 0, tiled=True, axis_index_groups=teams)
+    )(held(received), held(local_states), held(reach), held(new_step), head_log_decay, step_offset_bias)
+
+    received = lax.all_to_all(held(send), "sp", 0, 0, tiled=True, axis_index_groups=inside_team)
 
     prompt_out, step_row = call(
         finish_kernel,
@@ -470,22 +526,13 @@
             shaped(length, channels, dtype=bf16),
             shaped(1, channels // sequence_count, dtype=bf16),
         ),
-        grid=(1,),
-        in_specs=[
-            pl.BlockSpec(returned.shape, lambda i: (0, 0, 0)),
-            pl.BlockSpec((length, channels), lambda i: (0, 0)),
-            pl.BlockSpec((length, channels), lambda i: (0, 0)),
-            pl.BlockSpec((length, STATE), lambda i: (0, (channels + STATE) // STATE)),
-            pl.BlockSpec((1, group_norm_scale.shape[0]), lambda i: (0, 0)),
-            pl.BlockSpec((1, channels), lambda i: (0, 0)),
-            pl.BlockSpec((8, channels), lambda i: (0, 0)),
-        ],
-        out_specs=[
-            pl.BlockSpec((length, channels), lambda i: (0, 0)),
-            pl.BlockSpec((1, channels // sequence_count), lambda i: (0, 0)),
-        ],
+        in_specs=[vm] * 7,
+        out_specs=[vm] * 2,
         name="finish",
-    )(returned, base, lift, vwr, group_norm_scale[None], direct, new_gate)
+    )(
+        held(received), held(base), held(lift), held(vwr), group_norm_scale[None],
+        held(direct), held(new_gate),
+    )
     return (prompt_out, cache_rows, step_row.T)
 
 

time: 129 us -> 119 us (0.922)
  Pallas kernels: 22.6 us -> 16.7 us
  blocking collectives: 89.1 us -> 85.1 us
    pallas_call x4 -> x5, Pallas kernels: 20.3 us -> 15.6 us  [the longest x1 5.75 us: on_device(): call(inner_kernel, (near(length, channels), near(length, channels), near(...]
    all_to_all x1 -> x2, blocking collectives: 89.1 us -> 85.1 us  [the longest x1 54.6 us: on_device(): lax.all_to_all(held(send), 'sp', 0, 0, tiled=True, axis_index_groups=acro...]
  transfers between devices with their start and end apart: 2 -> 2, of which waited for: 1 -> 1; matrix products, arithmetic and copies ran while one was open for 1% -> 0% of each run, Pallas kernels for 10% -> 8%
where the time goes in v3:
time: 119 us; the launch traced here: 118 us
  blocking collectives  85.1 us (72%)
  Pallas kernels  16.7 us (14%)
  starting transfers between devices  8.39 us (7%)
  waiting for transfers between devices  5.09 us (4%)
  local copies, waits for them, and re-layouts  2.39 us (2%)
    all_to_all x1, blocking collectives, on_device(): lax.all_to_all(held(send), 'sp', 0, 0, tiled=True, axis_index_groups=acro...  54.6 us
    all_to_all x1, blocking collectives, on_device(): lax.all_to_all(held(send), 'sp', 0, 0, tiled=True, axis_index_groups=insi...  30.5 us
    pallas_call x1, Pallas kernels, on_device(): call(inner_kernel, (near(length, channels), near(length, channels), near(...  5.75 us
    all_to_all x1, waiting for transfers between devices, on_device(): lax.all_to_all(held(send), 'sp', 0, 0, tiled=True, axis_index_groups=insi...  5.09 us
    ppermute x1, starting transfers between devices, on_device(): lax.ppermute(tokens[length - HALO:], 'sp', [(i, i + 1) for i in range(seq...  4.7 us
    pallas_call x1, Pallas kernels, on_device(): call(local_kernel, (near(length, width, dtype=bf16), near(heads, length),...  4.03 us
    pallas_call x1, Pallas kernels, on_device(): call(project_kernel, (near(length, width, dtype=bf16), near(depth, width,...  3.79 us
    all_to_all x1, starting transfers between devices, on_device(): lax.all_to_all(held(send), 'sp', 0, 0, tiled=True, axis_index_groups=insi...  3.69 us
  transfers between devices with their start and end apart: 2, of which 1 were waited for; matrix products, arithmetic and copies ran while one was open for 0% of the time, Pallas kernels for 8%

profile of v3, /device:TPU:40, one launch (start us, length us, event | category | flops | bytes accessed | tf_op | source)
XLA Modules:
  0.0 118.5 jit_solution(12295502070391974113)
XLA Ops:
  0.6 0.8 slice.3
  1.4 4.7 %collective-permute-start = (bf16[8,2048]{1,0:T(8,128)(2,1)S(1)}, bf16[8,2048]{1,0:T(8,128)(2,1)S(1)}, u32[]{:S(2)}, u32[]{:S(2)}) collective-permute-start(bf16[8,2048]{1,0:T(8,128)(2,1)S(1)} %slice.3), channel_id=1, source_target_pairs={{0,8},{8,16},{16,24},{24,32},{32,40},{40,48},{48,56},{56,64},{64,7... | collective-permute-start | bytes 98312 | tf_op jit(solution)/shard_map/ppermute | solution.py:422
  6.1 0.0 copy-start
  6.1 0.9 copy-done
  7.0 0.0 copy-start.2
  7.0 0.7 copy-done.2
  7.7 0.0 copy-start.1
  7.7 0.0 copy-start.4
  7.7 0.0 copy-start.8
  7.7 0.0 copy-start.9
  7.7 0.0 copy-start.10
  7.7 3.8 %project.1 = (bf16[512,512]{1,0:T(8,128)(2,1)S(1)}, bf16[2048,512]{1,0:T(8,128)(2,1)S(1)}, f32[4,512]{1,0:T(4,128)S(1)}, f32[8,512]{1,0:T(8,128)S(1)}, f32[4,8]{1,0:T(4,128)S(1)}) custom-call(bf16[512,2048]{1,0:T(8,128)(2,1)} %tok_ref.1, bf16[16,128]{1,0:T(8,128)(2,1)S(1)} %bitcast.6, bf16[2048,256]{1,0:T(8,128)(2,1)} %wv_hbm.1, bf16[2048,128]{1,0:T(8,128)(2,1)} %ww_hbm.1, ...), custom_call_target="tpu_custom_call" | custom-call | flops 1073741824 | bytes 1048576 | tf_op jit(solution)/shard_map/project/pallas_call | solution.py:427
  11.5 0.0 copy-start.3
  11.6 0.0 collective-permute-done.halo_ref
  11.6 0.0 copy-done.1
  11.6 0.0 copy-done.4
  11.6 0.0 copy-done.5
  11.6 0.0 copy-done.6
  11.6 0.0 copy-done.8
  11.6 0.0 copy-done.9
  11.6 0.0 copy-done.10
  11.6 4.0 %local.1 = (bf16[512,512]{1,0:T(8,128)(2,1)S(1)}, f32[4,512]{1,0:T(4,128)S(1)}, f32[4,512]{1,0:T(4,128)S(1)}, bf16[4,128,256]{2,1,0:T(8,128)(2,1)S(1)}, bf16[8,4,1152]{2,1,0:T(4,128)(2,1)S(1)}) custom-call(bf16[512,512]{1,0:T(8,128)(2,1)S(1)} %get-tuple-element.24.rows_ref, bf16[8,2048]{1,0:T(8,128)(2,1)S(1)} %collective-permute-done.halo_ref, ...), custom_call_target="tpu_custom_call" | custom-call | flops 33554432 | bytes 1048576 | tf_op jit(solution)/shard_map/local/pallas_call | solution.py:446
  15.7 30.5 %all_to_all.15.recv_ref = bf16[8,4,1152]{2,1,0:T(4,128)(2,1)S(1)} all-to-all(bf16[8,4,1152]{2,1,0:T(4,128)(2,1)S(1)} %get-tuple-element.29), channel_id=1, replica_groups={{0,8,16,24,32,40,48,56},{64,72,80,88,96,104,112,120},{128,136,144,152,1..., dimensions={0} | all-to-all | bytes 147456 | tf_op jit(solution)/shard_map/all_to_all | solution.py:466
  46.2 0.6 team.1
  46.8 54.6 %all_to_all.16.recv_ref = bf16[4,4,1152]{2,1,0:T(4,128)(2,1)S(1)} all-to-all(bf16[4,4,1152]{2,1,0:T(4,128)(2,1)S(1)} %get-tuple-element.30), channel_id=1, replica_groups={{0,64,128,192},{8,72,136,200},{16,80,144,208},{24,88,152,216},{32,96,16..., dimensions={0} | all-to-all | bytes 73728 | tf_op jit(solution)/shard_map/all_to_all | solution.py:480
  101.4 1.5 %prefix.1 = (bf16[8,4,1280]{2,1,0:T(4,128)(2,1)}, bf16[4,256]{1,0:T(4,128)(2,1)}, f32[1,256]{1,0:T(1,128)S(1)}) custom-call(bf16[4,4,1152]{2,1,0:T(4,128)(2,1)S(1)} %all_to_all.16.recv_ref, f32[8,4,1024]{2,1,0:T(4,128)S(1)} %get-tuple-element.31.local_ref, f32[8,256]{1,0:T(8,128)S(1)} %get-tuple-element.32.reach_ref, ...), custom_call_target="tpu_custom_call" | custom-call | bytes 1048576 | tf_op jit(solution)/shard_map/prefix/pallas_call | solution.py:509
  102.9 3.7 %all-to-all-start.2 = ((bf16[8,4,1280]{2,1,0:T(4,128)(2,1)}), bf16[8,4,1280]{2,1,0:T(4,128)(2,1)S(1)}, u32[]{:S(2)}, u32[]{:S(2)}) async-start(bf16[8,4,1280]{2,1,0:T(4,128)(2,1)} %get-tuple-element.33), calls=%async_computation.2 | async-start | bytes 163840 | tf_op jit(solution)/shard_map/all_to_all | solution.py:521
  106.6 0.0 copy-done.3
  106.6 5.7 %inner.1 = (f32[512,256]{1,0:T(8,128)S(1)}, f32[512,256]{1,0:T(8,128)S(1)}, f32[8,256]{1,0:T(8,128)S(1)}) custom-call(bf16[512,2048]{1,0:T(8,128)(2,1)} %tok_ref.1, bf16[2048,256]{1,0:T(8,128)(2,1)} %wg_ref.1, bf16[16,128]{1,0:T(8,128)(2,1)S(1)} %bitcast.7, bf16[512,512]{1,0:T(8,128)(2,1)S(1)} %get-tuple-element.34.vwr_ref.reads_ref, ...), custom_call_target="tpu_custom_call" | custom-call | flops 536870912 | bytes 1048576 | tf_op jit(solution)/shard_map/inner/pallas_call | solution.py:482
  112.3 5.1 %all-to-all-done.2.recv_ref = bf16[8,4,1280]{2,1,0:T(4,128)(2,1)S(1)} async-done(((bf16[8,4,1280]{2,1,0:T(4,128)(2,1)}), bf16[8,4,1280]{2,1,0:T(4,128)(2,1)S(1)}, u32[]{:S(2)}, u32[]{:S(2)}) %all-to-all-start.2) | async-done | bytes 81952 | tf_op jit(solution)/shard_map/all_to_all | solution.py:521
  117.4 0.0 copy-done.7
  117.4 1.0 finish.1
  (3 shorter events, 0.0 us)
Async XLA Ops:
  1.4 10.2 %collective-permute-start = (bf16[8,2048]{1,0:T(8,128)(2,1)S(1)}, bf16[8,2048]{1,0:T(8,128)(2,1)S(1)}, u32[]{:S(2)}, u32[]{:S(2)}) collective-permute-start(bf16[8,2048]{1,0:T(8,128)(2,1)S(1)} %slice.3), channel_id=1, source_target_pairs={{0,8},{8,16},{16,24},{24,32},{32,40},{40,48},{48,56},{56,64},{64,7... | collective-permute-start | bytes 98312 | tf_op jit(solution)/shard_map/ppermute | solution.py:422
  6.1 0.9 copy-start
  7.0 0.7 copy-start.2
  7.7 3.9 %copy-start.1 = (bf16[4,2048]{1,0:T(4,128)(2,1)S(1)}, bf16[4,2048]{1,0:T(4,128)(2,1)}, u32[]{:S(2)}) copy-start(bf16[4,2048]{1,0:T(4,128)(2,1)} %vtap_ref.1) | copy-start | bytes 49156
  7.7 3.9 %copy-start.4 = (f32[512,4]{0,1:T(4,128)S(1)}, f32[512,4]{0,1:T(4,128)}, u32[]{:S(2)}) copy-start(f32[512,4]{0,1:T(4,128)} %param.27) | copy-start | bytes 24580
  7.7 3.9 %copy-start.5 = (bf16[4,1024]{1,0:T(4,128)(2,1)S(1)}, bf16[4,1024]{1,0:T(4,128)(2,1)}, u32[]{:S(2)}) copy-start(bf16[4,1024]{1,0:T(4,128)(2,1)} %wtap_ref.1) | copy-start | bytes 24580
  7.7 3.9 %copy-start.6 = (bf16[4,1024]{1,0:T(4,128)(2,1)S(1)}, bf16[4,1024]{1,0:T(4,128)(2,1)}, u32[]{:S(2)}) copy-start(bf16[4,1024]{1,0:T(4,128)(2,1)} %rtap_ref.1) | copy-start | bytes 24580
  7.7 3.9 %copy-start.8 = (f32[32]{0:T(128)S(1)}, f32[32]{0:T(128)}, u32[]{:S(2)}) copy-start(f32[32]{0:T(128)} %decay_ref.3) | copy-start | bytes 388
  7.7 3.9 %copy-start.9 = (f32[32]{0:T(128)S(1)}, f32[32]{0:T(128)}, u32[]{:S(2)}) copy-start(f32[32]{0:T(128)} %bias_ref.3) | copy-start | bytes 388
  7.7 3.9 %copy-start.10 = (f32[32]{0:T(128)S(1)}, f32[32]{0:T(128)}, u32[]{:S(2)}) copy-start(f32[32]{0:T(128)} %skip_ref.3) | copy-start | bytes 388
  11.5 95.0 %copy-start.3 = (bf16[2048]{0:T(1024)(128)(2,1)S(1)}, bf16[2048]{0:T(1024)(128)(2,1)}, u32[]{:S(2)}) copy-start(bf16[2048]{0:T(1024)(128)(2,1)} %param.16) | copy-start | bytes 12292
  102.9 14.6 %copy-start.7 = (f32[2048]{0:T(1024)S(1)}, f32[2048]{0:T(1024)}, u32[]{:S(2)}) copy-start(f32[2048]{0:T(1024)} %param.29) | copy-start | bytes 24580
  102.9 14.6 %all-to-all-start.2 = ((bf16[8,4,1280]{2,1,0:T(4,128)(2,1)}), bf16[8,4,1280]{2,1,0:T(4,128)(2,1)S(1)}, u32[]{:S(2)}, u32[]{:S(2)}) async-start(bf16[8,4,1280]{2,1,0:T(4,128)(2,1)} %get-tuple-element.33), calls=%async_computation.2 | async-start | bytes 163840 | tf_op jit(solution)/shard_map/all_to_all | solution.py:521

commit v4 on v3

--- a/solution.py
+++ b/solution.py
@@ -9,7 +9,7 @@
 STATE = 128
 CONV = 4
 BLOCK = 128
-TEAM = 8
+TEAM = 4
 MISC = 128
 HALO = 8
 
@@ -48,30 +48,34 @@
     return picked
 
 
-def head_column(ref, first, count, width):
-    rows = iota((count, width), 0)
-    column = jnp.full((count, width), ref[first], f32)
-    for h in range(1, count):
-        column = jnp.where(rows == h, ref[first + h], column)
-    return column
+def head_column(ref, first, count):
+    row = ref[...]
+    shape = (count, row.shape[1])
+    return jnp.sum(jnp.where(iota(shape, 1) == iota(shape, 0) + first, row, 0.0), axis=1, keepdims=True)
 
 
 def project_kernel(
-    tok_hbm, fresh_ref, wv_hbm, ww_hbm, wr_hbm, ws_ref,
-    rows_ref, weights, step_ref, new_ref, newstep_ref, tok, sems,
+    tok_hbm, fresh_hbm, wv_hbm, ww_hbm, wr_hbm, ws_hbm,
+    rows_ref, weights, step_ref, new_ref, newstep_ref, tok, lines, steps, sems, small,
 ):
-    depth = tok.shape[1]
+    length, depth = tok_hbm.shape
     channels = wv_hbm.shape[1]
     state = ww_hbm.shape[1]
     chunk = depth // SPLIT
+    first = [
+        pltpu.make_async_copy(fresh_hbm, lines, small.at[0]),
+        pltpu.make_async_copy(ws_hbm, steps, small.at[1]),
+    ]
+    for copy in first:
+        copy.start()
     copies = []
     for k in range(SPLIT):
         at = pl.ds(k * chunk, chunk)
         moves = [
-            (tok_hbm.at[:, at], tok.at[:, at]),
-            (wv_hbm.at[at], weights.at[at, 0:channels]),
-            (ww_hbm.at[at], weights.at[at, channels : channels + state]),
-            (wr_hbm.at[at], weights.at[at, channels + state : channels + 2 * state]),
+            (tok_hbm.at[:, at], tok.at[pl.ds(0, length), at]),
+            (wv_hbm.at[at], weights.at[at, pl.ds(0, channels)]),
+            (ww_hbm.at[at], weights.at[at, pl.ds(channels, state)]),
+            (wr_hbm.at[at], weights.at[at, pl.ds(channels + state, state)]),
         ]
         copies.append(
             [pltpu.make_async_copy(a, b, sems.at[k, i]) for i, (a, b) in enumerate(moves)]
@@ -80,33 +84,32 @@
             copy.start()
     rank = lax.axis_index("tp")
     heads = step_ref.shape[0]
-    acc = accs = accn = accns = None
-    lines = fresh_ref[...].astype(f32)
+    extra = tok.shape[0] - length
+    for copy in first:
+        copy.wait()
+    rows = lines[...].astype(f32)
+    fresh = jnp.concatenate([rows[i : i + 1] for i in range(depth // 128)], axis=1)
+    tok[length:] = jnp.broadcast_to(fresh, (extra, depth)).astype(bf16)
+    acc = accs = None
     for k in range(SPLIT):
         at = slice(k * chunk, (k + 1) * chunk)
-        each = chunk // 128
-        fresh = jnp.concatenate([lines[k * each + i : k * each + i + 1] for i in range(each)], axis=1)
-        fresh = jnp.broadcast_to(fresh, (8, chunk)).astype(bf16)
         for copy in copies[k]:
             copy.wait()
         part = dot(tok[:, at], weights[at])
-        parts = dot(ws_ref[:, at], tok[:, at], ((1,), (1,)))
-        partn = dot(fresh, weights[at])
-        partns = dot(ws_ref[:, at], fresh, ((1,), (1,)))
+        parts = dot(steps[:, at], tok[:, at], ((1,), (1,)))
         acc = part if k == 0 else acc + part
         accs = parts if k == 0 else accs + parts
-        accn = partn if k == 0 else accn + partn
-        accns = partns if k == 0 else accns + partns
-    rows_ref[...] = acc.astype(bf16)
-    step_ref[...] = own_rows(accs, rank, heads)
-    new_ref[...] = accn
-    newstep_ref[...] = own_rows(accns, rank, heads)
+    rows_ref[...] = acc[0:length].astype(bf16)
+    new_ref[...] = acc[length : length + 8]
+    accs = own_rows(accs, rank, heads)
+    step_ref[...] = accs[:, 0:length]
+    newstep_ref[...] = accs[:, length : length + 8]
 
 
 def local_kernel(
     rows_ref, halo_ref, weights, step_ref, new_ref, newstep_ref, spike_ref,
     vtap_ref, wtap_ref, rtap_ref, decay_ref, bias_ref, skip_ref,
-    vwr_ref, cum_ref, dt_ref, inside_ref, send_ref, ext,
+    vw_ref, edge_ref, cum_ref, dt_ref, inside_ref, newdecay_ref, send_ref, ext,
 ):
     rank = lax.axis_index("tp")
     length = rows_ref.shape[0]
@@ -115,8 +118,11 @@
     first = rank * heads
     halo = halo_ref[...]
     before = dot(halo, weights[...])
-    ext[0:HALO] = before.astype(bf16).astype(f32)
-    ext[HALO:] = rows_ref[...].astype(f32)
+    before = before.astype(bf16).astype(f32)
+    used = channels + STATE
+    edge_ref[...] = before[:, used:]
+    ext[0:HALO] = before[:, 0:used]
+    ext[HALO:] = rows_ref[:, 0:used].astype(f32)
     taps = jnp.concatenate(
         [
             vtap_ref[:, pl.ds(pl.multiple_of(rank * channels, 128), channels)].astype(f32),
@@ -126,21 +132,22 @@
         axis=1,
     )
     off = HALO - (CONV - 1)
-    summed = taps[0:1] * ext[off : off + length]
+    summed = taps[0:1, 0:used] * ext[off : off + length]
     for k in range(1, CONV):
-        summed = summed + taps[k : k + 1] * ext[off + k : off + k + length]
+        summed = summed + taps[k : k + 1, 0:used] * ext[off + k : off + k + length]
     vwr = silu(summed).astype(bf16)
-    vwr_ref[...] = vwr
+    vw_ref[...] = vwr
     newest = taps[CONV - 1 : CONV] * new_ref[0:1].astype(bf16).astype(f32)
+    ending = rows_ref[length - 16 :].astype(f32)
     for k in range(CONV - 1):
-        row = length + off + k
-        newest = newest + taps[k : k + 1] * ext[row : row + 1]
+        row = 16 - (CONV - 1) + k
+        newest = newest + taps[k : k + 1] * ending[row : row + 1]
     newest = silu(newest).astype(bf16).astype(f32)
     new_value = newest[:, 0:channels]
     new_write = newest[:, channels : channels + STATE]
     new_read = newest[:, channels + STATE :]
-    bias = head_column(bias_ref, first, heads, 128)
-    rate = jnp.exp(head_column(decay_ref, first, heads, 128))
+    bias = head_column(bias_ref, first, heads)
+    rate = jnp.exp(head_column(decay_ref, first, heads))
     upper = (iota((BLOCK, BLOCK), 0) <= iota((BLOCK, BLOCK), 1)).astype(f32)
     expand = spread(heads, channels)
     running = jnp.zeros((STATE, channels), f32)
@@ -175,8 +182,9 @@
     teams = STATE // stretch
     diagonal = jnp.where(rows == lanes, jnp.broadcast_to(new_read, shape), 0.0)
     read_column = jnp.sum(diagonal, axis=1, keepdims=True)
-    new_dt = softplus(newstep_ref[...][:, 0:1] + bias[:, 0:1])
-    skip = head_column(skip_ref, first, heads, 128)[:, 0:1]
+    new_dt = softplus(newstep_ref[...][:, 0:1] + bias)
+    newdecay_ref[...] = jnp.sum(expand * jnp.exp(-new_dt * rate), axis=0, keepdims=True)
+    skip = head_column(skip_ref, first, heads)
     weight = new_dt * jnp.sum(new_read * new_write, axis=1, keepdims=True) + skip
     direct = jnp.sum(expand * weight, axis=0, keepdims=True) * new_value
     placed = jnp.where(iota((8, channels), 0) == iota((8, channels), 1) // HEAD, direct, 0.0)
@@ -196,13 +204,15 @@
 
 
 def inner_kernel(
-    tok_ref, wg_ref, fresh_ref, vwr_ref, cum_ref, dt_ref, inside_ref, skip_ref,
-    base_ref, lift_ref, newgate_ref, before,
+    tok_ref, wg_ref, fresh_ref, rows_ref, edge_ref, rtap_ref, vw_ref, cum_ref, dt_ref, inside_ref,
+    skip_ref, after_ref, base_ref, lift_ref, newgate_ref, reads_ref, before, ext,
 ):
+    del after_ref
     b = pl.program_id(0)
     rank = lax.axis_index("tp")
     heads = cum_ref.shape[0]
     channels = wg_ref.shape[1]
+    length = rows_ref.shape[0]
 
     @pl.when(b == 0)
     def _():
@@ -212,16 +222,22 @@
         fresh = jnp.broadcast_to(fresh, (8, fresh.shape[1])).astype(bf16)
         gate = dot(fresh, wg_ref[...]).astype(bf16).astype(f32)
         newgate_ref[...] = silu(gate)
+        ext[0:HALO] = edge_ref[...]
+        ext[HALO:] = rows_ref[:, channels + STATE :].astype(f32)
+        taps = rtap_ref[:, pl.ds(pl.multiple_of(rank * STATE, 128), STATE)].astype(f32)
+        off = HALO - (CONV - 1)
+        summed = taps[0:1] * ext[off : off + length]
+        for k in range(1, CONV):
+            summed = summed + taps[k : k + 1] * ext[off + k : off + k + length]
+        reads_ref[...] = silu(summed).astype(bf16)
 
     expand = spread(heads, channels)
-    skip = jnp.sum(
-        expand * head_column(skip_ref, rank * heads, heads, channels), axis=0, keepdims=True
-    )
+    skip = jnp.sum(expand * head_column(skip_ref, rank * heads, heads), axis=0, keepdims=True)
     cum = cum_ref[...]
     dt = dt_ref[...]
-    values = vwr_ref[:, 0:channels]
-    writes = vwr_ref[:, channels : channels + STATE]
-    reads = vwr_ref[:, channels + STATE :]
+    values = vw_ref[:, 0:channels]
+    writes = vw_ref[:, channels:]
+    reads = reads_ref[pl.ds(pl.multiple_of(b * BLOCK, BLOCK), BLOCK)]
     gate = silu(dot(tok_ref[...], wg_ref[...]).astype(bf16).astype(f32))
     scores = dot(reads, writes, ((1,), (1,)))
     causal = iota((BLOCK, BLOCK), 0) >= iota((BLOCK, BLOCK), 1)
@@ -278,8 +294,8 @@
         send_ref[t, :, wide:] = note
 
 
-def prefix_kernel(recv_ref, local_ref, reach_ref, newstep_ref, decay_ref, bias_ref, send_ref, cache_ref, direct_ref):
-    rank = lax.axis_index("tp")
+def prefix_kernel(recv_ref, local_ref, reach_ref, newdecay_ref, after_ref, send_ref, cache_ref, direct_ref):
+    del after_ref
     teams, own, width = recv_ref.shape
     wide = width - MISC
     channels = wide // teams
@@ -306,12 +322,7 @@
     for g in range(teams):
         column = note[:, 2 * heads + g : 2 * heads + g + 1]
         reading = reading + column * kept[:, g * channels : (g + 1) * channels]
-    first = rank * heads
-    bias = head_column(bias_ref, first, heads, 1)
-    rate = jnp.exp(head_column(decay_ref, first, heads, 1))
-    decay = jnp.exp(-softplus(newstep_ref[...][:, 0:1] + bias) * rate)
-    decay = jnp.sum(spread(heads, channels) * decay, axis=0, keepdims=True)
-    partial = jnp.sum(reading, axis=0, keepdims=True) * decay
+    partial = jnp.sum(reading, axis=0, keepdims=True) * newdecay_ref[...]
     high = partial.astype(bf16).astype(f32)
     low = partial - high
     rows = iota((own, channels), 0)
@@ -337,7 +348,7 @@
         axis=0,
     ).astype(bf16)
     gain = gain_ref[:, pl.ds(pl.multiple_of(rank * channels, 128), channels)]
-    gated = base_ref[...] + dot(reads_ref[:, channels + STATE :], earlier) * lift_ref[...]
+    gated = base_ref[...] + dot(reads_ref[...], earlier) * lift_ref[...]
     scale = lax.rsqrt(jnp.mean(gated * gated, axis=1, keepdims=True) + epsilon)
     out_ref[...] = (gated * scale * gain).astype(bf16)
     partial = jnp.sum(jnp.sum(recv_ref[:, :, wide:].astype(f32), axis=0), axis=0, keepdims=True)
@@ -414,7 +425,6 @@
     width = channels + 2 * STATE
     wide = teams * channels
     vm = pl.BlockSpec(memory_space=pltpu.VMEM)
-    sm = pl.BlockSpec(memory_space=pltpu.SMEM)
     far = pl.BlockSpec(memory_space=pltpu.HBM)
     inside_team = [[TEAM * t + i for i in range(TEAM)] for t in range(teams)]
     across_teams = [[TEAM * t + i for t in range(teams)] for i in range(TEAM)]
@@ -433,34 +443,43 @@
             near(8, width),
             near(heads, 8),
         ),
-        in_specs=[far, vm, far, far, far, vm],
+        in_specs=[far] * 6,
         out_specs=[vm] * 5,
-        scratch=[pltpu.VMEM((length, depth), bf16), pltpu.SemaphoreType.DMA((SPLIT, 4))],
+        scratch=[
+            pltpu.VMEM((length + 16, depth), bf16),
+            pltpu.VMEM((depth // 128, 128), bf16),
+            pltpu.VMEM((step_matrix.shape[1], depth), bf16),
+            pltpu.SemaphoreType.DMA((SPLIT, 4)),
+            pltpu.SemaphoreType.DMA((2,)),
+        ],
         flops=2 * length * depth * width,
         name="project",
     )(
-        stored(tokens), fresh, stored(value_matrix), stored(write_matrix), stored(read_matrix),
-        step_matrix.T,
-    )
-
-    vwr, cum, dt, inside, send = call(
+        stored(tokens), stored(fresh), stored(value_matrix), stored(write_matrix),
+        stored(read_matrix), stored(step_matrix.T),
+    )
+
+    decay_row, bias_row, skip_row = head_log_decay[None], step_offset_bias[None], bypass_scale[None]
+    vw, edge, cum, dt, inside, new_decay, send = call(
         local_kernel,
         (
-            near(length, width, dtype=bf16),
+            near(length, channels + STATE, dtype=bf16),
+            near(HALO, STATE),
             near(heads, length),
             near(heads, length),
             near(blocks, STATE, channels, dtype=bf16),
+            near(1, channels),
             near(TEAM, own, wide + MISC, dtype=bf16),
         ),
-        in_specs=[vm] * 10 + [sm] * 3,
-        out_specs=[vm] * 5,
-        scratch=[pltpu.VMEM((length + HALO, width), f32)],
+        in_specs=[vm] * 13,
+        out_specs=[vm] * 7,
+        scratch=[pltpu.VMEM((length + HALO, channels + STATE), f32)],
         flops=2 * length * STATE * channels,
         name="local",
     )(
         held(rows), held(halo), held(weights), held(step_raw), held(new_rows), held(new_step), spike,
         value_filter_taps, write_filter_taps, read_filter_taps,
-        head_log_decay, step_offset_bias, bypass_scale,
+        decay_row, bias_row, skip_row,
     )
 
     received = lax.all_to_all(held(send), "sp", 0, 0, tiled=True, axis_index_groups=inside_team)
@@ -479,31 +498,41 @@
 
     received = lax.all_to_all(held(send), "sp", 0, 0, tiled=True, axis_index_groups=across_teams)
 
-    base, lift, new_gate = call(
+    base, lift, new_gate, reads = call(
         inner_kernel,
-        (near(length, channels), near(length, channels), near(8, channels)),
+        (
+            near(length, channels),
+            near(length, channels),
+            near(8, channels),
+            near(length, STATE, dtype=bf16),
+        ),
         grid=(blocks,),
         in_specs=[
             pl.BlockSpec((BLOCK, depth), lambda b: (b, 0)),
             pl.BlockSpec((depth, channels), lambda b: (0, 0)),
             pl.BlockSpec((depth // 128, 128), lambda b: (0, 0)),
-            pl.BlockSpec((BLOCK, width), lambda b: (b, 0)),
+            pl.BlockSpec((length, width), lambda b: (0, 0)),
+            pl.BlockSpec((HALO, STATE), lambda b: (0, 0)),
+            pl.BlockSpec(read_filter_taps.shape, lambda b: (0, 0)),
+            pl.BlockSpec((BLOCK, channels + STATE), lambda b: (b, 0)),
             pl.BlockSpec((heads, BLOCK), lambda b: (0, b)),
             pl.BlockSpec((heads, BLOCK), lambda b: (0, b)),
             pl.BlockSpec((1, STATE, channels), lambda b: (b, 0, 0)),
-            sm,
+            pl.BlockSpec(skip_row.shape, lambda b: (0, 0)),
+            pl.BlockSpec(reach.shape, lambda b: (0, 0)),
         ],
         out_specs=[
             pl.BlockSpec((BLOCK, channels), lambda b: (b, 0)),
             pl.BlockSpec((BLOCK, channels), lambda b: (b, 0)),
             pl.BlockSpec((8, channels), lambda b: (0, 0)),
+            pl.BlockSpec((length, STATE), lambda b: (0, 0)),
         ],
-        scratch=[pltpu.VMEM((heads, BLOCK), f32)],
+        scratch=[pltpu.VMEM((heads, BLOCK), f32), pltpu.VMEM((length + HALO, STATE), f32)],
         flops=2 * length * depth * channels,
         name="inner",
     )(
-        stored(tokens), stored(gate_matrix), fresh, held(vwr), held(cum), held(dt), held(inside),
-        bypass_scale,
+        stored(tokens), stored(gate_matrix), fresh, held(rows), held(edge), read_filter_taps,
+        held(vw), held(cum), held(dt), held(inside), skip_row, held(reach),
     )
 
     send, cache_rows, direct = call(
@@ -513,10 +542,10 @@
             shaped(own, channels, dtype=bf16),
             near(1, channels),
         ),
-        in_specs=[vm] * 4 + [sm] * 2,
+        in_specs=[vm] * 5,
         out_specs=[vm] * 3,
         name="prefix",
-    )(held(received), held(local_states), held(reach), held(new_step), head_log_decay, step_offset_bias)
+    )(held(received), held(local_states), held(reach), held(new_decay), held(new_gate))
 
     received = lax.all_to_all(held(send), "sp", 0, 0, tiled=True, axis_index_groups=inside_team)
 
@@ -530,7 +559,7 @@
         out_specs=[vm] * 2,
         name="finish",
     )(
-        held(received), held(base), held(lift), held(vwr), group_norm_scale[None],
+        held(received), held(base), held(lift), held(reads), group_norm_scale[None],
         held(direct), held(new_gate),
     )
     return (prompt_out, cache_rows, step_row.T)

time: 119 us -> 108 us (0.908)
  blocking collectives: 85.1 us -> 24 us
  starting transfers between devices: 8.39 us -> 42.9 us
  waiting for transfers between devices: 5.09 us -> 22.7 us
  local copies, waits for them, and re-layouts: 2.39 us -> 0.82 us
    all_to_all x1 -> x0, blocking collectives: 54.6 us -> none  [on_device(): lax.all_to_all(held(send), 'sp', 0, 0, tiled=True, axis_index_groups=acro...]
    all_to_all x1, starting transfers between devices: 3.69 us -> 38.2 us  [on_device(): lax.all_to_all(held(send), 'sp', 0, 0, tiled=True, axis_index_groups=acro...]
    all_to_all x1, waiting for transfers between devices: 5.09 us -> 22.7 us  [on_device(): lax.all_to_all(held(send), 'sp', 0, 0, tiled=True, axis_index_groups=acro...]
    all_to_all x1 -> x2, blocking collectives: 30.5 us -> 24 us  [on_device(): lax.all_to_all(held(send), 'sp', 0, 0, tiled=True, axis_index_groups=insi...]
    unnamed x22 -> x18, local copies, waits for them, and re-layouts: 1.63 us -> 0.06 us
  transfers between devices with their start and end apart: 2 -> 2, of which waited for: 1 -> 1; matrix products, arithmetic and copies ran while one was open for 0% -> 0% of each run, Pallas kernels for 8% -> 9%
where the time goes in v4:
time: 108 us
  starting transfers between devices  42.9 us (40%)
  blocking collectives  24 us (22%)
  waiting for transfers between devices  22.7 us (21%)
  Pallas kernels  16.7 us (15%)
    all_to_all x1, starting transfers between devices, on_device(): lax.all_to_all(held(send), 'sp', 0, 0, tiled=True, axis_index_groups=acro...  38.2 us
    all_to_all x2, blocking collectives, on_device(): lax.all_to_all(held(send), 'sp', 0, 0, tiled=True, axis_index_groups=insi...  24 us
    all_to_all x1, waiting for transfers between devices, on_device(): lax.all_to_all(held(send), 'sp', 0, 0, tiled=True, axis_index_groups=acro...  22.7 us
    pallas_call x1, Pallas kernels, on_device(): call(inner_kernel, (near(length, channels), near(length, channels), near(...  5.78 us
    ppermute x1, starting transfers between devices, on_device(): lax.ppermute(tokens[length - HALO:], 'sp', [(i, i + 1) for i in range(seq...  4.7 us
    pallas_call x1, Pallas kernels, on_device(): call(project_kernel, (near(length, width, dtype=bf16), near(depth, width,...  4.26 us
    pallas_call x1, Pallas kernels, on_device(): call(local_kernel, (near(length, channels + STATE, dtype=bf16), near(HALO...  3.44 us
  transfers between devices with their start and end apart: 2, of which 1 were waited for; matrix products, arithmetic and copies ran while one was open for 0% of the time, Pallas kernels for 9%

profile of v4, /device:TPU:40, one launch (start us, length us, event | category | flops | bytes accessed | tf_op | source)
XLA Modules:
  0.0 107.9 jit_solution(8877909291796836001)
XLA Ops:
  0.6 0.8 slice.3
  1.4 4.7 %collective-permute-start = (bf16[8,2048]{1,0:T(8,128)(2,1)S(1)}, bf16[8,2048]{1,0:T(8,128)(2,1)S(1)}, u32[]{:S(2)}, u32[]{:S(2)}) collective-permute-start(bf16[8,2048]{1,0:T(8,128)(2,1)S(1)} %slice.3), channel_id=1, source_target_pairs={{0,8},{8,16},{16,24},{24,32},{32,40},{40,48},{48,56},{56,64},{64,7... | collective-permute-start | bytes 98312 | tf_op jit(solution)/shard_map/ppermute | solution.py:432
  6.1 0.0 copy-start
  6.1 0.0 copy-start.1
  6.1 0.0 copy-start.3
  6.1 0.0 copy-start.4
  6.2 0.0 copy-start.6
  6.2 0.0 copy-start.7
  6.2 0.0 copy-start.8
  6.2 4.3 %project.1 = (bf16[512,512]{1,0:T(8,128)(2,1)S(1)}, bf16[2048,512]{1,0:T(8,128)(2,1)S(1)}, f32[4,512]{1,0:T(4,128)S(1)}, f32[8,512]{1,0:T(8,128)S(1)}, f32[4,8]{1,0:T(4,128)S(1)}) custom-call(bf16[512,2048]{1,0:T(8,128)(2,1)} %tok_ref.1, bf16[16,128]{1,0:T(8,128)(2,1)} %bitcast.8, bf16[2048,256]{1,0:T(8,128)(2,1)} %wv_hbm.1, bf16[2048,128]{1,0:T(8,128)(2,1)} %ww_hbm.1, ...), custom_call_target="tpu_custom_call" | custom-call | flops 1073741824 | bytes 1048576 | tf_op jit(solution)/shard_map/project/pallas_call | solution.py:437
  10.5 0.0 copy-start.2
  10.5 0.0 collective-permute-done.halo_ref
  10.5 0.0 copy-done
  10.5 0.0 copy-done.1
  10.5 0.0 copy-done.3
  10.5 0.0 copy-done.4
  10.5 0.0 copy-done.6
  10.5 0.0 copy-done.7
  10.5 0.0 copy-done.8
  10.6 3.4 %local.1 = (bf16[512,384]{1,0:T(8,128)(2,1)S(1)}, f32[8,128]{1,0:T(8,128)S(1)}, f32[4,512]{1,0:T(4,128)S(1)}, f32[4,512]{1,0:T(4,128)S(1)}, bf16[4,128,256]{2,1,...) custom-call(bf16[512,512]{1,0:T(8,128)(2,1)S(1)} %get-tuple-element.27.rows_ref, ...), custom_call_target="tpu_custom_call" | custom-call | flops 33554432 | bytes 1048576 | tf_op jit(solution)/shard_map/local/pallas_call | solution.py:463
  14.0 15.3 %all_to_all.15.recv_ref = bf16[4,4,2176]{2,1,0:T(4,128)(2,1)S(1)} all-to-all(bf16[4,4,2176]{2,1,0:T(4,128)(2,1)S(1)} %get-tuple-element.32), channel_id=1, replica_groups={{0,8,16,24},{32,40,48,56},{64,72,80,88},{96,104,112,120},{128,136,144,1..., dimensions={0} | all-to-all | bytes 139264 | tf_op jit(solution)/shard_map/all_to_all | solution.py:485
  29.3 1.3 %team.1 = (bf16[8,4,2176]{2,1,0:T(4,128)(2,1)}, f32[4,4,2048]{2,1,0:T(4,128)S(1)}, f32[4,256]{1,0:T(4,128)S(1)}) custom-call(bf16[4,4,2176]{2,1,0:T(4,128)(2,1)S(1)} %all_to_all.15.recv_ref), custom_call_target="tpu_custom_call" | custom-call | bytes 1048576 | tf_op jit(solution)/shard_map/team/pallas_call | solution.py:487
  30.5 38.2 %all-to-all-start.1 = ((bf16[8,4,2176]{2,1,0:T(4,128)(2,1)}), bf16[8,4,2176]{2,1,0:T(4,128)(2,1)S(1)}, u32[]{:S(2)}, u32[]{:S(2)}) async-start(bf16[8,4,2176]{2,1,0:T(4,128)(2,1)} %get-tuple-element.33), calls=%async_computation.1 | async-start | bytes 278528 | tf_op jit(solution)/shard_map/all_to_all | solution.py:499
  68.7 0.0 copy-done.2
  68.7 0.0 copy-start.5
  68.8 5.8 %inner.1 = (f32[512,256]{1,0:T(8,128)S(1)}, f32[512,256]{1,0:T(8,128)S(1)}, f32[8,256]{1,0:T(8,128)S(1)}, bf16[512,128]{1,0:T(8,128)(2,1)S(1)}) custom-call(bf16[512,2048]{1,0:T(8,128)(2,1)} %tok_ref.1, bf16[2048,256]{1,0:T(8,128)(2,1)} %wg_ref.1, bf16[16,128]{1,0:T(8,128)(2,1)S(1)} %bitcast.9, bf16[512,512]{1,0:T(8,128)(2,1)S(1)} %get-tuple-element.27.rows_ref, ...), custom_call_target="tpu_custom_call" | custom-call | flops 536870912 | bytes 1048576 | tf_op jit(solution)/shard_map/inner/pallas_call | solution.py:501
  74.5 22.7 %all-to-all-done.1.recv_ref = bf16[8,4,2176]{2,1,0:T(4,128)(2,1)S(1)} async-done(((bf16[8,4,2176]{2,1,0:T(4,128)(2,1)}), bf16[8,4,2176]{2,1,0:T(4,128)(2,1)S(1)}, u32[]{:S(2)}, u32[]{:S(2)}) %all-to-all-start.1) | async-done | bytes 139296 | tf_op jit(solution)/shard_map/all_to_all | solution.py:499
  97.2 0.9 prefix.1
  98.2 8.7 %all_to_all.16.recv_ref = bf16[4,4,2304]{2,1,0:T(4,128)(2,1)S(1)} all-to-all(bf16[4,4,2304]{2,1,0:T(4,128)(2,1)S(1)} %get-tuple-element.43), channel_id=1, replica_groups={{0,8,16,24},{32,40,48,56},{64,72,80,88},{96,104,112,120},{128,136,144,1..., dimensions={0} | all-to-all | bytes 147456 | tf_op jit(solution)/shard_map/all_to_all | solution.py:550
  106.9 0.0 copy-done.5
  106.9 1.0 finish.1
Async XLA Ops:
  1.4 9.1 %collective-permute-start = (bf16[8,2048]{1,0:T(8,128)(2,1)S(1)}, bf16[8,2048]{1,0:T(8,128)(2,1)S(1)}, u32[]{:S(2)}, u32[]{:S(2)}) collective-permute-start(bf16[8,2048]{1,0:T(8,128)(2,1)S(1)} %slice.3), channel_id=1, source_target_pairs={{0,8},{8,16},{16,24},{24,32},{32,40},{40,48},{48,56},{56,64},{64,7... | collective-permute-start | bytes 98312 | tf_op jit(solution)/shard_map/ppermute | solution.py:432
  6.1 4.4 %copy-start = (bf16[4,1024]{1,0:T(4,128)(2,1)S(1)}, bf16[4,1024]{1,0:T(4,128)(2,1)}, u32[]{:S(2)}) copy-start(bf16[4,1024]{1,0:T(4,128)(2,1)} %rtap_ref.3) | copy-start | bytes 24580
  6.1 4.4 %copy-start.1 = (bf16[4,2048]{1,0:T(4,128)(2,1)S(1)}, bf16[4,2048]{1,0:T(4,128)(2,1)}, u32[]{:S(2)}) copy-start(bf16[4,2048]{1,0:T(4,128)(2,1)} %vtap_ref.1) | copy-start | bytes 49156
  6.1 4.4 %copy-start.3 = (f32[512,4]{0,1:T(4,128)S(1)}, f32[512,4]{0,1:T(4,128)}, u32[]{:S(2)}) copy-start(f32[512,4]{0,1:T(4,128)} %param.27) | copy-start | bytes 24580
  6.1 4.4 %copy-start.4 = (bf16[4,1024]{1,0:T(4,128)(2,1)S(1)}, bf16[4,1024]{1,0:T(4,128)(2,1)}, u32[]{:S(2)}) copy-start(bf16[4,1024]{1,0:T(4,128)(2,1)} %wtap_ref.1) | copy-start | bytes 24580
  6.2 4.4 %copy-start.6 = (f32[32]{0:T(128)S(1)}, f32[32]{0:T(128)}, u32[]{:S(2)}) copy-start(f32[32]{0:T(128)} %param.28) | copy-start | bytes 388
  6.2 4.4 %copy-start.7 = (f32[32]{0:T(128)S(1)}, f32[32]{0:T(128)}, u32[]{:S(2)}) copy-start(f32[32]{0:T(128)} %param.25) | copy-start | bytes 388
  6.2 4.4 %copy-start.8 = (f32[32]{0:T(128)S(1)}, f32[32]{0:T(128)}, u32[]{:S(2)}) copy-start(f32[32]{0:T(128)} %param.26) | copy-start | bytes 388
  10.5 58.3 %copy-start.2 = (bf16[2048]{0:T(1024)(128)(2,1)S(1)}, bf16[2048]{0:T(1024)(128)(2,1)}, u32[]{:S(2)}) copy-start(bf16[2048]{0:T(1024)(128)(2,1)} %param.16) | copy-start | bytes 12292
  30.5 66.7 %all-to-all-start.1 = ((bf16[8,4,2176]{2,1,0:T(4,128)(2,1)}), bf16[8,4,2176]{2,1,0:T(4,128)(2,1)S(1)}, u32[]{:S(2)}, u32[]{:S(2)}) async-start(bf16[8,4,2176]{2,1,0:T(4,128)(2,1)} %get-tuple-element.33), calls=%async_computation.1 | async-start | bytes 278528 | tf_op jit(solution)/shard_map/all_to_all | solution.py:499
  68.7 38.1 %copy-start.5 = (f32[2048]{0:T(1024)S(1)}, f32[2048]{0:T(1024)}, u32[]{:S(2)}) copy-start(f32[2048]{0:T(1024)} %param.29) | copy-start | bytes 24580

commit v5 on v4

--- a/solution.py
+++ b/solution.py
@@ -18,7 +18,8 @@
 bf16 = jnp.bfloat16
 HIGHEST = lax.Precision.HIGHEST
 VMEM_LIMIT = 24 * 1024 * 1024
-SPLIT = 4
+SPLIT = 8
+AHEAD = 8
 
 
 def dot(a, b, dims=((1,), (0,)), precision=None):
@@ -26,7 +27,8 @@
 
 
 def silu(x):
-    return x / (1.0 + jnp.exp(-x))
+    half = 0.5 * x
+    return half * jnp.tanh(half) + half
 
 
 def softplus(x):
@@ -39,6 +41,27 @@
 
 def spread(heads, channels):
     return (iota((heads, channels), 0) == iota((heads, channels), 1) // HEAD).astype(f32)
+
+
+def thirds(x):
+    high = x.astype(bf16)
+    rest = x - high.astype(f32)
+    middle = rest.astype(bf16)
+    low = (rest - middle.astype(f32)).astype(bf16)
+    return jnp.concatenate([high.astype(f32), middle.astype(f32), low.astype(f32)], axis=0).astype(bf16)
+
+
+def over_channels(x, channels):
+    heads = x.shape[0]
+    shape = (3 * heads, channels)
+    mask = iota(shape, 0) % heads == iota(shape, 1) // HEAD
+    return dot(thirds(x), mask.astype(bf16), ((0,), (0,)))
+
+
+def summed_up(x, upper):
+    heads = x.shape[0]
+    parts = dot(thirds(x), upper)
+    return parts[0:heads] + parts[heads : 2 * heads] + parts[2 * heads :]
 
 
 def own_rows(table, rank, count):
@@ -56,9 +79,9 @@
 
 def project_kernel(
     tok_hbm, fresh_hbm, wv_hbm, ww_hbm, wr_hbm, ws_hbm,
-    rows_ref, weights, step_ref, new_ref, newstep_ref, tok, lines, steps, sems, small,
+    rows_ref, weights, step_ref, fresh_ref, newstep_ref, tok, lines, steps, sems, small,
 ):
-    length, depth = tok_hbm.shape
+    depth = tok_hbm.shape[1]
     channels = wv_hbm.shape[1]
     state = ww_hbm.shape[1]
     chunk = depth // SPLIT
@@ -72,7 +95,7 @@
     for k in range(SPLIT):
         at = pl.ds(k * chunk, chunk)
         moves = [
-            (tok_hbm.at[:, at], tok.at[pl.ds(0, length), at]),
+            (tok_hbm.at[:, at], tok.at[:, at]),
             (wv_hbm.at[at], weights.at[at, pl.ds(0, channels)]),
             (ww_hbm.at[at], weights.at[at, pl.ds(channels, state)]),
             (wr_hbm.at[at], weights.at[at, pl.ds(channels + state, state)]),
@@ -80,34 +103,36 @@
         copies.append(
             [pltpu.make_async_copy(a, b, sems.at[k, i]) for i, (a, b) in enumerate(moves)]
         )
-        for copy in copies[-1]:
+    for k in range(min(AHEAD, SPLIT)):
+        for copy in copies[k]:
             copy.start()
     rank = lax.axis_index("tp")
     heads = step_ref.shape[0]
-    extra = tok.shape[0] - length
     for copy in first:
         copy.wait()
     rows = lines[...].astype(f32)
     fresh = jnp.concatenate([rows[i : i + 1] for i in range(depth // 128)], axis=1)
-    tok[length:] = jnp.broadcast_to(fresh, (extra, depth)).astype(bf16)
+    fresh_ref[...] = jnp.broadcast_to(fresh, fresh_ref.shape).astype(bf16)
+    newstep = jnp.sum(own_rows(steps[...].astype(f32), rank, heads) * fresh, axis=1, keepdims=True)
+    newstep_ref[...] = jnp.broadcast_to(newstep, newstep_ref.shape)
     acc = accs = None
     for k in range(SPLIT):
         at = slice(k * chunk, (k + 1) * chunk)
         for copy in copies[k]:
             copy.wait()
+        if k + AHEAD < SPLIT:
+            for copy in copies[k + AHEAD]:
+                copy.start()
         part = dot(tok[:, at], weights[at])
         parts = dot(steps[:, at], tok[:, at], ((1,), (1,)))
         acc = part if k == 0 else acc + part
         accs = parts if k == 0 else accs + parts
-    rows_ref[...] = acc[0:length].astype(bf16)
-    new_ref[...] = acc[length : length + 8]
-    accs = own_rows(accs, rank, heads)
-    step_ref[...] = accs[:, 0:length]
-    newstep_ref[...] = accs[:, length : length + 8]
+    rows_ref[...] = acc.astype(bf16)
+    step_ref[...] = own_rows(accs, rank, heads)
 
 
 def local_kernel(
-    rows_ref, halo_ref, weights, step_ref, new_ref, newstep_ref, spike_ref,
+    rows_ref, halo_ref, weights, step_ref, fresh_ref, newstep_ref, spike_ref,
     vtap_ref, wtap_ref, rtap_ref, decay_ref, bias_ref, skip_ref,
     vw_ref, edge_ref, cum_ref, dt_ref, inside_ref, newdecay_ref, send_ref, ext,
 ):
@@ -116,9 +141,9 @@
     heads = step_ref.shape[0]
     channels = rows_ref.shape[1] - 2 * STATE
     first = rank * heads
-    halo = halo_ref[...]
-    before = dot(halo, weights[...])
-    before = before.astype(bf16).astype(f32)
+    few = dot(jnp.concatenate([halo_ref[...], fresh_ref[...]], axis=0), weights[...])
+    few = few.astype(bf16).astype(f32)
+    before = few[0:HALO]
     used = channels + STATE
     edge_ref[...] = before[:, used:]
     ext[0:HALO] = before[:, 0:used]
@@ -137,7 +162,7 @@
         summed = summed + taps[k : k + 1, 0:used] * ext[off + k : off + k + length]
     vwr = silu(summed).astype(bf16)
     vw_ref[...] = vwr
-    newest = taps[CONV - 1 : CONV] * new_ref[0:1].astype(bf16).astype(f32)
+    newest = taps[CONV - 1 : CONV] * few[HALO : HALO + 1]
     ending = rows_ref[length - 16 :].astype(f32)
     for k in range(CONV - 1):
         row = 16 - (CONV - 1) + k
@@ -148,7 +173,7 @@
     new_read = newest[:, channels + STATE :]
     bias = head_column(bias_ref, first, heads)
     rate = jnp.exp(head_column(decay_ref, first, heads))
-    upper = (iota((BLOCK, BLOCK), 0) <= iota((BLOCK, BLOCK), 1)).astype(f32)
+    upper = (iota((BLOCK, BLOCK), 0) <= iota((BLOCK, BLOCK), 1)).astype(bf16)
     expand = spread(heads, channels)
     running = jnp.zeros((STATE, channels), f32)
     total = jnp.zeros((heads, 128), f32)
@@ -156,14 +181,14 @@
         at = slice(b * BLOCK, (b + 1) * BLOCK)
         dt = softplus(step_ref[:, at] + bias)
         log_decay = spike_ref[:, at] - dt * rate
-        cum = dot(log_decay, upper, precision=HIGHEST)
+        cum = summed_up(log_decay, upper)
         dt_ref[:, at] = dt
         cum_ref[:, at] = cum
         end = jnp.broadcast_to(cum[:, BLOCK - 1 :], (heads, BLOCK))
-        factor = dot(jnp.exp(end - cum) * dt, expand, ((0,), (0,)), HIGHEST)
+        factor = over_channels(jnp.exp(end - cum) * dt, channels)
         scaled = (factor * vwr[at, 0:channels].astype(f32)).astype(bf16)
         states = dot(vwr[at, channels : channels + STATE], scaled, ((0,), (0,)))
-        fade = dot(jnp.exp(end), expand, ((0,), (0,)), HIGHEST)
+        fade = jnp.sum(expand * jnp.exp(end[:, 0:1]), axis=0, keepdims=True)
         inside_ref[b] = running.astype(bf16)
         running = fade * running + states
         total = total + end
@@ -217,10 +242,7 @@
     @pl.when(b == 0)
     def _():
         before[...] = jnp.zeros_like(before)
-        lines = fresh_ref[...].astype(f32)
-        fresh = jnp.concatenate([lines[i : i + 1] for i in range(lines.shape[0])], axis=1)
-        fresh = jnp.broadcast_to(fresh, (8, fresh.shape[1])).astype(bf16)
-        gate = dot(fresh, wg_ref[...]).astype(bf16).astype(f32)
+        gate = dot(fresh_ref[...], wg_ref[...]).astype(bf16).astype(f32)
         newgate_ref[...] = silu(gate)
         ext[0:HALO] = edge_ref[...]
         ext[HALO:] = rows_ref[:, channels + STATE :].astype(f32)
@@ -248,11 +270,11 @@
         mixing = scores * jnp.exp(jnp.where(causal, gap, -jnp.inf)) * dt[h : h + 1]
         parts.append(dot(mixing.astype(bf16), values[:, h * HEAD : (h + 1) * HEAD]))
     inner = jnp.concatenate(parts, axis=1)
-    fade = dot(jnp.exp(cum), expand, ((0,), (0,)), HIGHEST)
+    fade = over_channels(jnp.exp(cum), channels)
     carried = fade * dot(reads, inside_ref[0])
     base_ref[...] = (inner + carried + skip * values.astype(f32)) * gate
     far = jnp.exp(cum + before[...])
-    lift_ref[...] = dot(far, expand, ((0,), (0,)), HIGHEST) * gate
+    lift_ref[...] = over_channels(far, channels) * gate
     before[...] += jnp.broadcast_to(cum[:, BLOCK - 1 :], before.shape)
 
 
@@ -434,19 +456,19 @@
     )
     fresh = fresh_token_input.reshape(depth // 128, 128)
     spike = decay_spike.T
-    rows, weights, step_raw, new_rows, new_step = call(
+    rows, weights, step_raw, fresh_rows, new_step = call(
         project_kernel,
         (
             near(length, width, dtype=bf16),
             near(depth, width, dtype=bf16),
             near(heads, length),
-            near(8, width),
+            near(8, depth, dtype=bf16),
             near(heads, 8),
         ),
         in_specs=[far] * 6,
         out_specs=[vm] * 5,
         scratch=[
-            pltpu.VMEM((length + 16, depth), bf16),
+            pltpu.VMEM((length, depth), bf16),
             pltpu.VMEM((depth // 128, 128), bf16),
             pltpu.VMEM((step_matrix.shape[1], depth), bf16),
             pltpu.SemaphoreType.DMA((SPLIT, 4)),
@@ -477,7 +499,7 @@
         flops=2 * length * STATE * channels,
         name="local",
     )(
-        held(rows), held(halo), held(weights), held(step_raw), held(new_rows), held(new_step), spike,
+        held(rows), held(halo), held(weights), held(step_raw), held(fresh_rows), held(new_step), spike,
         value_filter_taps, write_filter_taps, read_filter_taps,
         decay_row, bias_row, skip_row,
     )
@@ -510,7 +532,7 @@
         in_specs=[
             pl.BlockSpec((BLOCK, depth), lambda b: (b, 0)),
             pl.BlockSpec((depth, channels), lambda b: (0, 0)),
-            pl.BlockSpec((depth // 128, 128), lambda b: (0, 0)),
+            pl.BlockSpec(fresh_rows.shape, lambda b: (0, 0)),
             pl.BlockSpec((length, width), lambda b: (0, 0)),
             pl.BlockSpec((HALO, STATE), lambda b: (0, 0)),
             pl.BlockSpec(read_filter_taps.shape, lambda b: (0, 0)),
@@ -531,7 +553,7 @@
         flops=2 * length * depth * channels,
         name="inner",
     )(
-        stored(tokens), stored(gate_matrix), fresh, held(rows), held(edge), read_filter_taps,
+        stored(tokens), stored(gate_matrix), held(fresh_rows), held(rows), held(edge), read_filter_taps,
         held(vw), held(cum), held(dt), held(inside), skip_row, held(reach),
     )
 

time: 108 us -> 107 us (level)
  Pallas kernels: 16.7 us -> 14.2 us
  waiting for transfers between devices: 22.7 us -> 24 us
    pallas_call x1, Pallas kernels: 3.44 us -> 1.99 us  [on_device(): call(local_kernel, (near(length, channels + STATE, dtype=bf16), near(HALO...]
    all_to_all x1, waiting for transfers between devices: 22.7 us -> 24 us  [on_device(): lax.all_to_all(held(send), 'sp', 0, 0, tiled=True, axis_index_groups=acro...]
    pallas_call x1, Pallas kernels: 5.78 us -> 4.51 us  [on_device(): call(inner_kernel, (near(length, channels), near(length, channels), near(...]
  transfers between devices with their start and end apart: 2 -> 2, of which waited for: 1 -> 1; matrix products, arithmetic and copies ran while one was open for 0% -> 0% of each run, Pallas kernels for 9% -> 8%
where the time goes in v5:
time: 107 us
  starting transfers between devices  42.9 us (40%)
  waiting for transfers between devices  24 us (22%)
  blocking collectives  24 us (22%)
  Pallas kernels  14.2 us (13%)
    all_to_all x1, starting transfers between devices, on_device(): lax.all_to_all(held(send), 'sp', 0, 0, tiled=True, axis_index_groups=acro...  38.2 us
    all_to_all x1, waiting for transfers between devices, on_device(): lax.all_to_all(held(send), 'sp', 0, 0, tiled=True, axis_index_groups=acro...  24 us
    all_to_all x2, blocking collectives, on_device(): lax.all_to_all(held(send), 'sp', 0, 0, tiled=True, axis_index_groups=insi...  24 us
    ppermute x1, starting transfers between devices, on_device(): lax.ppermute(tokens[length - HALO:], 'sp', [(i, i + 1) for i in range(seq...  4.7 us
    pallas_call x1, Pallas kernels, on_device(): call(inner_kernel, (near(length, channels), near(length, channels), near(...  4.51 us
    pallas_call x1, Pallas kernels, on_device(): call(project_kernel, (near(length, width, dtype=bf16), near(depth, width,...  4.42 us
  transfers between devices with their start and end apart: 2, of which 1 were waited for; matrix products, arithmetic and copies ran while one was open for 0% of the time, Pallas kernels for 8%

profile of v5, /device:TPU:40, one launch (start us, length us, event | category | flops | bytes accessed | tf_op | source)
XLA Modules:
  0.0 106.6 jit_solution(1303912719612587524)
XLA Ops:
  0.6 0.8 slice.3
  1.4 4.7 %collective-permute-start = (bf16[8,2048]{1,0:T(8,128)(2,1)S(1)}, bf16[8,2048]{1,0:T(8,128)(2,1)S(1)}, u32[]{:S(2)}, u32[]{:S(2)}) collective-permute-start(bf16[8,2048]{1,0:T(8,128)(2,1)S(1)} %slice.3), channel_id=1, source_target_pairs={{0,8},{8,16},{16,24},{24,32},{32,40},{40,48},{48,56},{56,64},{64,7... | collective-permute-start | bytes 98312 | tf_op jit(solution)/shard_map/ppermute | solution.py:454
  6.1 0.0 copy-start
  6.1 0.0 copy-start.1
  6.1 0.0 copy-start.2
  6.1 0.0 copy-start.3
  6.2 0.0 copy-start.5
  6.2 0.0 copy-start.6
  6.2 0.0 copy-start.7
  6.2 4.4 %project.1 = (bf16[512,512]{1,0:T(8,128)(2,1)S(1)}, bf16[2048,512]{1,0:T(8,128)(2,1)S(1)}, f32[4,512]{1,0:T(4,128)S(1)}, bf16[8,2048]{1,0:T(8,128)(2,1)S(1)}, f32[4,8]{1,0:T(4,128)S(1)}) custom-call(bf16[512,2048]{1,0:T(8,128)(2,1)} %tok_ref.1, bf16[16,128]{1,0:T(8,128)(2,1)} %bitcast.15, bf16[2048,256]{1,0:T(8,128)(2,1)} %wv_hbm.1, ...), custom_call_target="tpu_custom_call" | custom-call | flops 1073741824 | bytes 1048576 | tf_op jit(solution)/shard_map/project/pallas_call | solution.py:459
  10.6 0.0 collective-permute-done.halo_ref
  10.6 0.0 copy-done
  10.6 0.0 copy-done.1
  10.6 0.0 copy-done.2
  10.7 0.0 copy-done.3
  10.7 0.0 copy-done.5
  10.7 0.0 copy-done.6
  10.7 0.0 copy-done.7
  10.7 2.0 %local.1 = (bf16[512,384]{1,0:T(8,128)(2,1)S(1)}, f32[8,128]{1,0:T(8,128)S(1)}, f32[4,512]{1,0:T(4,128)S(1)}, f32[4,512]{1,0:T(4,128)S(1)}, bf16[4,128,256]{2,1,...) custom-call(bf16[512,512]{1,0:T(8,128)(2,1)S(1)} %get-tuple-element.27.rows_ref, ...), custom_call_target="tpu_custom_call" | custom-call | flops 33554432 | bytes 1048576 | tf_op jit(solution)/shard_map/local/pallas_call | solution.py:485
  12.7 15.2 %all_to_all.15.recv_ref = bf16[4,4,2176]{2,1,0:T(4,128)(2,1)S(1)} all-to-all(bf16[4,4,2176]{2,1,0:T(4,128)(2,1)S(1)} %get-tuple-element.32), channel_id=1, replica_groups={{0,8,16,24},{32,40,48,56},{64,72,80,88},{96,104,112,120},{128,136,144,1..., dimensions={0} | all-to-all | bytes 139264 | tf_op jit(solution)/shard_map/all_to_all | solution.py:507
  27.9 1.3 %team.1 = (bf16[8,4,2176]{2,1,0:T(4,128)(2,1)}, f32[4,4,2048]{2,1,0:T(4,128)S(1)}, f32[4,256]{1,0:T(4,128)S(1)}) custom-call(bf16[4,4,2176]{2,1,0:T(4,128)(2,1)S(1)} %all_to_all.15.recv_ref), custom_call_target="tpu_custom_call" | custom-call | bytes 1048576 | tf_op jit(solution)/shard_map/team/pallas_call | solution.py:509
  29.2 38.2 %all-to-all-start.1 = ((bf16[8,4,2176]{2,1,0:T(4,128)(2,1)}), bf16[8,4,2176]{2,1,0:T(4,128)(2,1)S(1)}, u32[]{:S(2)}, u32[]{:S(2)}) async-start(bf16[8,4,2176]{2,1,0:T(4,128)(2,1)} %get-tuple-element.33), calls=%async_computation.1 | async-start | bytes 278528 | tf_op jit(solution)/shard_map/all_to_all | solution.py:521
  67.4 0.0 copy-start.4
  67.4 4.5 %inner.1 = (f32[512,256]{1,0:T(8,128)S(1)}, f32[512,256]{1,0:T(8,128)S(1)}, f32[8,256]{1,0:T(8,128)S(1)}, bf16[512,128]{1,0:T(8,128)(2,1)S(1)}) custom-call(bf16[512,2048]{1,0:T(8,128)(2,1)} %tok_ref.1, bf16[2048,256]{1,0:T(8,128)(2,1)} %wg_ref.1, bf16[8,2048]{1,0:T(8,128)(2,1)S(1)} %get-tuple-element.30.fresh_ref, ...), custom_call_target="tpu_custom_call" | custom-call | flops 536870912 | bytes 1048576 | tf_op jit(solution)/shard_map/inner/pallas_call | solution.py:523
  71.9 24.0 %all-to-all-done.1.recv_ref = bf16[8,4,2176]{2,1,0:T(4,128)(2,1)S(1)} async-done(((bf16[8,4,2176]{2,1,0:T(4,128)(2,1)}), bf16[8,4,2176]{2,1,0:T(4,128)(2,1)S(1)}, u32[]{:S(2)}, u32[]{:S(2)}) %all-to-all-start.1) | async-done | bytes 139296 | tf_op jit(solution)/shard_map/all_to_all | solution.py:521
  95.9 0.9 prefix.1
  96.8 8.7 %all_to_all.16.recv_ref = bf16[4,4,2304]{2,1,0:T(4,128)(2,1)S(1)} all-to-all(bf16[4,4,2304]{2,1,0:T(4,128)(2,1)S(1)} %get-tuple-element.43), channel_id=1, replica_groups={{0,8,16,24},{32,40,48,56},{64,72,80,88},{96,104,112,120},{128,136,144,1..., dimensions={0} | all-to-all | bytes 147456 | tf_op jit(solution)/shard_map/all_to_all | solution.py:572
  105.6 0.0 copy-done.4
  105.6 1.0 finish.1
Async XLA Ops:
  1.4 9.2 %collective-permute-start = (bf16[8,2048]{1,0:T(8,128)(2,1)S(1)}, bf16[8,2048]{1,0:T(8,128)(2,1)S(1)}, u32[]{:S(2)}, u32[]{:S(2)}) collective-permute-start(bf16[8,2048]{1,0:T(8,128)(2,1)S(1)} %slice.3), channel_id=1, source_target_pairs={{0,8},{8,16},{16,24},{24,32},{32,40},{40,48},{48,56},{56,64},{64,7... | collective-permute-start | bytes 98312 | tf_op jit(solution)/shard_map/ppermute | solution.py:454
  6.1 4.5 %copy-start = (bf16[4,1024]{1,0:T(4,128)(2,1)S(1)}, bf16[4,1024]{1,0:T(4,128)(2,1)}, u32[]{:S(2)}) copy-start(bf16[4,1024]{1,0:T(4,128)(2,1)} %rtap_ref.3) | copy-start | bytes 24580
  6.1 4.5 %copy-start.1 = (bf16[4,2048]{1,0:T(4,128)(2,1)S(1)}, bf16[4,2048]{1,0:T(4,128)(2,1)}, u32[]{:S(2)}) copy-start(bf16[4,2048]{1,0:T(4,128)(2,1)} %vtap_ref.1) | copy-start | bytes 49156
  6.1 4.5 %copy-start.2 = (f32[512,4]{0,1:T(4,128)S(1)}, f32[512,4]{0,1:T(4,128)}, u32[]{:S(2)}) copy-start(f32[512,4]{0,1:T(4,128)} %param.27) | copy-start | bytes 24580
  6.1 4.5 %copy-start.3 = (bf16[4,1024]{1,0:T(4,128)(2,1)S(1)}, bf16[4,1024]{1,0:T(4,128)(2,1)}, u32[]{:S(2)}) copy-start(bf16[4,1024]{1,0:T(4,128)(2,1)} %wtap_ref.1) | copy-start | bytes 24580
  6.2 4.5 %copy-start.5 = (f32[32]{0:T(128)S(1)}, f32[32]{0:T(128)}, u32[]{:S(2)}) copy-start(f32[32]{0:T(128)} %param.28) | copy-start | bytes 388
  6.2 4.5 %copy-start.6 = (f32[32]{0:T(128)S(1)}, f32[32]{0:T(128)}, u32[]{:S(2)}) copy-start(f32[32]{0:T(128)} %param.25) | copy-start | bytes 388
  6.2 4.5 %copy-start.7 = (f32[32]{0:T(128)S(1)}, f32[32]{0:T(128)}, u32[]{:S(2)}) copy-start(f32[32]{0:T(128)} %param.26) | copy-start | bytes 388
  29.2 66.7 %all-to-all-start.1 = ((bf16[8,4,2176]{2,1,0:T(4,128)(2,1)}), bf16[8,4,2176]{2,1,0:T(4,128)(2,1)S(1)}, u32[]{:S(2)}, u32[]{:S(2)}) async-start(bf16[8,4,2176]{2,1,0:T(4,128)(2,1)} %get-tuple-element.33), calls=%async_computation.1 | async-start | bytes 278528 | tf_op jit(solution)/shard_map/all_to_all | solution.py:521
  67.4 38.2 %copy-start.4 = (f32[2048]{0:T(1024)S(1)}, f32[2048]{0:T(1024)}, u32[]{:S(2)}) copy-start(f32[2048]{0:T(1024)} %param.29) | copy-start | bytes 24580

commit v6 on v5

--- a/solution.py
+++ b/solution.py
@@ -19,7 +19,6 @@
 HIGHEST = lax.Precision.HIGHEST
 VMEM_LIMIT = 24 * 1024 * 1024
 SPLIT = 8
-AHEAD = 8
 
 
 def dot(a, b, dims=((1,), (0,)), precision=None):
@@ -85,12 +84,9 @@
     channels = wv_hbm.shape[1]
     state = ww_hbm.shape[1]
     chunk = depth // SPLIT
-    first = [
-        pltpu.make_async_copy(fresh_hbm, lines, small.at[0]),
-        pltpu.make_async_copy(ws_hbm, steps, small.at[1]),
-    ]
-    for copy in first:
-        copy.start()
+    get_fresh = pltpu.make_async_copy(fresh_hbm, lines, small.at[0])
+    get_steps = pltpu.make_async_copy(ws_hbm, steps, small.at[1])
+    get_steps.start()
     copies = []
     for k in range(SPLIT):
         at = pl.ds(k * chunk, chunk)
@@ -103,30 +99,30 @@
         copies.append(
             [pltpu.make_async_copy(a, b, sems.at[k, i]) for i, (a, b) in enumerate(moves)]
         )
-    for k in range(min(AHEAD, SPLIT)):
+    for k in range(SPLIT):
         for copy in copies[k]:
             copy.start()
+    get_fresh.start()
     rank = lax.axis_index("tp")
     heads = step_ref.shape[0]
-    for copy in first:
-        copy.wait()
-    rows = lines[...].astype(f32)
-    fresh = jnp.concatenate([rows[i : i + 1] for i in range(depth // 128)], axis=1)
-    fresh_ref[...] = jnp.broadcast_to(fresh, fresh_ref.shape).astype(bf16)
-    newstep = jnp.sum(own_rows(steps[...].astype(f32), rank, heads) * fresh, axis=1, keepdims=True)
-    newstep_ref[...] = jnp.broadcast_to(newstep, newstep_ref.shape)
     acc = accs = None
+    get_steps.wait()
     for k in range(SPLIT):
         at = slice(k * chunk, (k + 1) * chunk)
         for copy in copies[k]:
             copy.wait()
-        if k + AHEAD < SPLIT:
-            for copy in copies[k + AHEAD]:
-                copy.start()
         part = dot(tok[:, at], weights[at])
         parts = dot(steps[:, at], tok[:, at], ((1,), (1,)))
         acc = part if k == 0 else acc + part
         accs = parts if k == 0 else accs + parts
+        if k == SPLIT - 1:
+            get_fresh.wait()
+            rows = lines[...].astype(f32)
+            fresh = jnp.concatenate([rows[i : i + 1] for i in range(depth // 128)], axis=1)
+            fresh_ref[...] = jnp.broadcast_to(fresh, fresh_ref.shape).astype(bf16)
+            table = own_rows(steps[...].astype(f32), rank, heads)
+            newstep = jnp.sum(table * fresh, axis=1, keepdims=True)
+            newstep_ref[...] = jnp.broadcast_to(newstep, newstep_ref.shape)
     rows_ref[...] = acc.astype(bf16)
     step_ref[...] = own_rows(accs, rank, heads)
 
@@ -316,8 +312,7 @@
         send_ref[t, :, wide:] = note
 
 
-def prefix_kernel(recv_ref, local_ref, reach_ref, newdecay_ref, after_ref, send_ref, cache_ref, direct_ref):
-    del after_ref
+def prefix_kernel(recv_ref, local_ref, reach_ref, newdecay_ref, send_ref, cache_ref, direct_ref):
     teams, own, width = recv_ref.shape
     wide = width - MISC
     channels = wide // teams
@@ -520,6 +515,20 @@
 
     received = lax.all_to_all(held(send), "sp", 0, 0, tiled=True, axis_index_groups=across_teams)
 
+    send, cache_rows, direct = call(
+        prefix_kernel,
+        (
+            near(TEAM, own, wide + channels, dtype=bf16),
+            shaped(own, channels, dtype=bf16),
+            near(1, channels),
+        ),
+        in_specs=[vm] * 4,
+        out_specs=[vm] * 3,
+        name="prefix",
+    )(held(received), held(local_states), held(reach), held(new_decay))
+
+    received = lax.all_to_all(held(send), "sp", 0, 0, tiled=True, axis_index_groups=inside_team)
+
     base, lift, new_gate, reads = call(
         inner_kernel,
         (
@@ -541,7 +550,7 @@
             pl.BlockSpec((heads, BLOCK), lambda b: (0, b)),
             pl.BlockSpec((1, STATE, channels), lambda b: (b, 0, 0)),
             pl.BlockSpec(skip_row.shape, lambda b: (0, 0)),
-            pl.BlockSpec(reach.shape, lambda b: (0, 0)),
+            pl.BlockSpec(direct.shape, lambda b: (0, 0)),
         ],
         out_specs=[
             pl.BlockSpec((BLOCK, channels), lambda b: (b, 0)),
@@ -554,22 +563,8 @@
         name="inner",
     )(
         stored(tokens), stored(gate_matrix), held(fresh_rows), held(rows), held(edge), read_filter_taps,
-        held(vw), held(cum), held(dt), held(inside), skip_row, held(reach),
-    )
-
-    send, cache_rows, direct = call(
-        prefix_kernel,
-        (
-            near(TEAM, own, wide + channels, dtype=bf16),
-            shaped(own, channels, dtype=bf16),
-            near(1, channels),
-        ),
-        in_specs=[vm] * 5,
-        out_specs=[vm] * 3,
-        name="prefix",
-    )(held(received), held(local_states), held(reach), held(new_decay), held(new_gate))
-
-    received = lax.all_to_all(held(send), "sp", 0, 0, tiled=True, axis_index_groups=inside_team)
+        held(vw), held(cum), held(dt), held(inside), skip_row, held(direct),
+    )
 
     prompt_out, step_row = call(
         finish_kernel,

time: 107 us -> 107 us (level)
  blocking collectives: 24 us -> 81.7 us
  starting transfers between devices: 42.9 us -> 8.08 us
  waiting for transfers between devices: 24 us -> 1.16 us
    all_to_all x0 -> x1, blocking collectives: none -> 66.5 us  [on_device(): lax.all_to_all(held(send), 'sp', 0, 0, tiled=True, axis_index_groups=acro...]
    all_to_all x1, starting transfers between devices: 38.2 us -> 3.38 us  [on_device(): lax.all_to_all(held(send), 'sp', 0, 0, tiled=True, axis_index_groups=insi...]
    all_to_all x1, waiting for transfers between devices: 24 us -> 1.16 us  [on_device(): lax.all_to_all(held(send), 'sp', 0, 0, tiled=True, axis_index_groups=insi...]
    all_to_all x2 -> x1, blocking collectives: 24 us -> 15.3 us  [on_device(): lax.all_to_all(held(send), 'sp', 0, 0, tiled=True, axis_index_groups=insi...]
where the time goes in v6:
time: 107 us; the launch traced here: 106 us
  blocking collectives  81.7 us (76%)
  Pallas kernels  13.5 us (13%)
  starting transfers between devices  8.08 us (8%)
  waiting for transfers between devices  1.16 us (1%)
    all_to_all x1, blocking collectives, on_device(): lax.all_to_all(held(send), 'sp', 0, 0, tiled=True, axis_index_groups=acro...  66.5 us
    all_to_all x1, blocking collectives, on_device(): lax.all_to_all(held(send), 'sp', 0, 0, tiled=True, axis_index_groups=insi...  15.3 us
    ppermute x1, starting transfers between devices, on_device(): lax.ppermute(tokens[length - HALO:], 'sp', [(i, i + 1) for i in range(seq...  4.7 us
    pallas_call x1, Pallas kernels, on_device(): call(inner_kernel, (near(length, channels), near(length, channels), near(...  4.51 us
    pallas_call x1, Pallas kernels, on_device(): call(project_kernel, (near(length, width, dtype=bf16), near(depth, width,...  4.39 us
    all_to_all x1, starting transfers between devices, on_device(): lax.all_to_all(held(send), 'sp', 0, 0, tiled=True, axis_index_groups=insi...  3.38 us
  transfers between devices with their start and end apart: 2, of which 1 were waited for; matrix products, arithmetic and copies ran while one was open for 0% of the time, Pallas kernels for 8%

profile of v6, /device:TPU:40, one launch (start us, length us, event | category | flops | bytes accessed | tf_op | source)
XLA Modules:
  0.0 106.1 jit_solution(16845792570591500451)
XLA Ops:
  0.6 0.8 slice.3
  1.4 4.7 %collective-permute-start = (bf16[8,2048]{1,0:T(8,128)(2,1)S(1)}, bf16[8,2048]{1,0:T(8,128)(2,1)S(1)}, u32[]{:S(2)}, u32[]{:S(2)}) collective-permute-start(bf16[8,2048]{1,0:T(8,128)(2,1)S(1)} %slice.3), channel_id=1, source_target_pairs={{0,8},{8,16},{16,24},{24,32},{32,40},{40,48},{48,56},{56,64},{64,7... | collective-permute-start | bytes 98312 | tf_op jit(solution)/shard_map/ppermute | solution.py:449
  6.1 0.0 copy-start
  6.1 0.0 copy-start.1
  6.1 0.0 copy-start.2
  6.1 0.0 copy-start.3
  6.2 0.0 copy-start.5
  6.2 0.0 copy-start.6
  6.2 0.0 copy-start.7
  6.2 4.4 %project.1 = (bf16[512,512]{1,0:T(8,128)(2,1)S(1)}, bf16[2048,512]{1,0:T(8,128)(2,1)S(1)}, f32[4,512]{1,0:T(4,128)S(1)}, bf16[8,2048]{1,0:T(8,128)(2,1)S(1)}, f32[4,8]{1,0:T(4,128)S(1)}) custom-call(bf16[512,2048]{1,0:T(8,128)(2,1)} %tok_ref.1, bf16[16,128]{1,0:T(8,128)(2,1)} %bitcast.15, bf16[2048,256]{1,0:T(8,128)(2,1)} %wv_hbm.1, ...), custom_call_target="tpu_custom_call" | custom-call | flops 1073741824 | bytes 1048576 | tf_op jit(solution)/shard_map/project/pallas_call | solution.py:454
  10.6 0.0 collective-permute-done.halo_ref
  10.6 0.0 copy-done
  10.6 0.0 copy-done.1
  10.6 0.0 copy-done.2
  10.6 0.0 copy-done.3
  10.6 0.0 copy-done.5
  10.6 0.0 copy-done.6
  10.7 0.0 copy-done.7
  10.7 2.0 %local.1 = (bf16[512,384]{1,0:T(8,128)(2,1)S(1)}, f32[8,128]{1,0:T(8,128)S(1)}, f32[4,512]{1,0:T(4,128)S(1)}, f32[4,512]{1,0:T(4,128)S(1)}, bf16[4,128,256]{2,1,...) custom-call(bf16[512,512]{1,0:T(8,128)(2,1)S(1)} %get-tuple-element.27.rows_ref, ...), custom_call_target="tpu_custom_call" | custom-call | flops 33554432 | bytes 1048576 | tf_op jit(solution)/shard_map/local/pallas_call | solution.py:480
  12.7 15.3 %all_to_all.15.recv_ref = bf16[4,4,2176]{2,1,0:T(4,128)(2,1)S(1)} all-to-all(bf16[4,4,2176]{2,1,0:T(4,128)(2,1)S(1)} %get-tuple-element.32), channel_id=1, replica_groups={{0,8,16,24},{32,40,48,56},{64,72,80,88},{96,104,112,120},{128,136,144,1..., dimensions={0} | all-to-all | bytes 139264 | tf_op jit(solution)/shard_map/all_to_all | solution.py:502
  27.9 0.6 team.1
  28.5 66.5 %all_to_all.16.recv_ref = bf16[8,4,2176]{2,1,0:T(4,128)(2,1)S(1)} all-to-all(bf16[8,4,2176]{2,1,0:T(4,128)(2,1)S(1)} %get-tuple-element.33), channel_id=1, replica_groups={{0,32,64,96,128,160,192,224},{8,40,72,104,136,168,200,232},{16,48,80,11..., dimensions={0} | all-to-all | bytes 278528 | tf_op jit(solution)/shard_map/all_to_all | solution.py:516
  95.0 1.0 prefix.1
  96.0 3.4 %all-to-all-start.2 = ((bf16[4,4,2304]{2,1,0:T(4,128)(2,1)}), bf16[4,4,2304]{2,1,0:T(4,128)(2,1)S(1)}, u32[]{:S(2)}, u32[]{:S(2)}) async-start(bf16[4,4,2304]{2,1,0:T(4,128)(2,1)} %get-tuple-element.37), calls=%async_computation.2 | async-start | bytes 147456 | tf_op jit(solution)/shard_map/all_to_all | solution.py:530
  99.4 0.0 copy-start.4
  99.4 4.5 %inner.1 = (f32[512,256]{1,0:T(8,128)S(1)}, f32[512,256]{1,0:T(8,128)S(1)}, f32[8,256]{1,0:T(8,128)S(1)}, bf16[512,128]{1,0:T(8,128)(2,1)S(1)}) custom-call(bf16[512,2048]{1,0:T(8,128)(2,1)} %tok_ref.1, bf16[2048,256]{1,0:T(8,128)(2,1)} %wg_ref.1, bf16[8,2048]{1,0:T(8,128)(2,1)S(1)} %get-tuple-element.30.fresh_ref, ...), custom_call_target="tpu_custom_call" | custom-call | flops 536870912 | bytes 1048576 | tf_op jit(solution)/shard_map/inner/pallas_call | solution.py:532
  103.9 1.2 %all-to-all-done.2.recv_ref = bf16[4,4,2304]{2,1,0:T(4,128)(2,1)S(1)} async-done(((bf16[4,4,2304]{2,1,0:T(4,128)(2,1)}), bf16[4,4,2304]{2,1,0:T(4,128)(2,1)S(1)}, u32[]{:S(2)}, u32[]{:S(2)}) %all-to-all-start.2) | async-done | bytes 73760 | tf_op jit(solution)/shard_map/all_to_all | solution.py:530
  105.1 0.0 copy-done.4
  105.1 1.0 finish.1
Async XLA Ops:
  1.4 9.2 %collective-permute-start = (bf16[8,2048]{1,0:T(8,128)(2,1)S(1)}, bf16[8,2048]{1,0:T(8,128)(2,1)S(1)}, u32[]{:S(2)}, u32[]{:S(2)}) collective-permute-start(bf16[8,2048]{1,0:T(8,128)(2,1)S(1)} %slice.3), channel_id=1, source_target_pairs={{0,8},{8,16},{16,24},{24,32},{32,40},{40,48},{48,56},{56,64},{64,7... | collective-permute-start | bytes 98312 | tf_op jit(solution)/shard_map/ppermute | solution.py:449
  6.1 4.5 %copy-start = (bf16[4,1024]{1,0:T(4,128)(2,1)S(1)}, bf16[4,1024]{1,0:T(4,128)(2,1)}, u32[]{:S(2)}) copy-start(bf16[4,1024]{1,0:T(4,128)(2,1)} %rtap_ref.3) | copy-start | bytes 24580
  6.1 4.5 %copy-start.1 = (bf16[4,2048]{1,0:T(4,128)(2,1)S(1)}, bf16[4,2048]{1,0:T(4,128)(2,1)}, u32[]{:S(2)}) copy-start(bf16[4,2048]{1,0:T(4,128)(2,1)} %vtap_ref.1) | copy-start | bytes 49156
  6.1 4.5 %copy-start.2 = (f32[512,4]{0,1:T(4,128)S(1)}, f32[512,4]{0,1:T(4,128)}, u32[]{:S(2)}) copy-start(f32[512,4]{0,1:T(4,128)} %param.27) | copy-start | bytes 24580
  6.1 4.5 %copy-start.3 = (bf16[4,1024]{1,0:T(4,128)(2,1)S(1)}, bf16[4,1024]{1,0:T(4,128)(2,1)}, u32[]{:S(2)}) copy-start(bf16[4,1024]{1,0:T(4,128)(2,1)} %wtap_ref.1) | copy-start | bytes 24580
  6.2 4.5 %copy-start.5 = (f32[32]{0:T(128)S(1)}, f32[32]{0:T(128)}, u32[]{:S(2)}) copy-start(f32[32]{0:T(128)} %param.28) | copy-start | bytes 388
  6.2 4.5 %copy-start.6 = (f32[32]{0:T(128)S(1)}, f32[32]{0:T(128)}, u32[]{:S(2)}) copy-start(f32[32]{0:T(128)} %param.25) | copy-start | bytes 388
  6.2 4.5 %copy-start.7 = (f32[32]{0:T(128)S(1)}, f32[32]{0:T(128)}, u32[]{:S(2)}) copy-start(f32[32]{0:T(128)} %param.26) | copy-start | bytes 388
  96.0 9.1 %all-to-all-start.2 = ((bf16[4,4,2304]{2,1,0:T(4,128)(2,1)}), bf16[4,4,2304]{2,1,0:T(4,128)(2,1)S(1)}, u32[]{:S(2)}, u32[]{:S(2)}) async-start(bf16[4,4,2304]{2,1,0:T(4,128)(2,1)} %get-tuple-element.37), calls=%async_computation.2 | async-start | bytes 147456 | tf_op jit(solution)/shard_map/all_to_all | solution.py:530
  99.4 5.7 %copy-start.4 = (f32[2048]{0:T(1024)S(1)}, f32[2048]{0:T(1024)}, u32[]{:S(2)}) copy-start(f32[2048]{0:T(1024)} %param.29) | copy-start | bytes 24580

commit v7 on v6

--- a/solution.py
+++ b/solution.py
@@ -18,7 +18,7 @@
 bf16 = jnp.bfloat16
 HIGHEST = lax.Precision.HIGHEST
 VMEM_LIMIT = 24 * 1024 * 1024
-SPLIT = 8
+SPLIT = 4
 
 
 def dot(a, b, dims=((1,), (0,)), precision=None):
@@ -274,6 +274,10 @@
     before[...] += jnp.broadcast_to(cum[:, BLOCK - 1 :], before.shape)
 
 
+def places(teams):
+    return [*reversed(range(teams))]
+
+
 def fades_of(notes, heads, channels):
     lane = iota((MISC, channels), 0)
     owner = iota((MISC, channels), 1) // HEAD
@@ -322,10 +326,12 @@
     fades = fades_of(notes, heads, channels)
     state = jnp.zeros((own, wide), f32)
     entering = state
+    place = {t: p for p, t in enumerate(places(teams))}
     for t in range(teams):
+        at = place[t]
         entering = jnp.where(group == t, state, entering)
-        fade = jnp.concatenate([fades[t : t + 1]] * teams, axis=1)
-        state = fade * state + recv_ref[t, :, 0:wide].astype(f32)
+        fade = jnp.concatenate([fades[at : at + 1]] * teams, axis=1)
+        state = fade * state + recv_ref[at, :, 0:wide].astype(f32)
     for k in range(TEAM):
         reach = jnp.concatenate([reach_ref[k : k + 1]] * teams, axis=1)
         send_ref[k, :, 0:wide] = (local_ref[k] + reach * entering).astype(bf16)
@@ -334,7 +340,7 @@
     for g in range(1, teams):
         mine = jnp.where(group == g, kept[:, g * channels : (g + 1) * channels], mine)
     cache_ref[...] = mine.astype(bf16)
-    note = recv_ref[teams - 1, :, wide:].astype(f32)
+    note = recv_ref[place[teams - 1], :, wide:].astype(f32)
     reading = jnp.zeros((own, channels), f32)
     for g in range(teams):
         column = note[:, 2 * heads + g : 2 * heads + g + 1]
@@ -444,7 +450,7 @@
     vm = pl.BlockSpec(memory_space=pltpu.VMEM)
     far = pl.BlockSpec(memory_space=pltpu.HBM)
     inside_team = [[TEAM * t + i for i in range(TEAM)] for t in range(teams)]
-    across_teams = [[TEAM * t + i for t in range(teams)] for i in range(TEAM)]
+    across_teams = [[TEAM * t + i for t in places(teams)] for i in range(TEAM)]
 
     halo = lax.ppermute(
         tokens[length - HALO :], "sp", [(i, i + 1) for i in range(sequence_count - 1)]

time: 107 us -> 103 us (0.963)
  blocking collectives: 81.7 us -> 76.8 us
  starting transfers between devices: 8.08 us -> 9.22 us
    all_to_all x1, blocking collectives: 66.5 us -> 61.6 us  [on_device(): lax.all_to_all(held(send), 'sp', 0, 0, tiled=True, axis_index_groups=acro...]
    all_to_all x1, starting transfers between devices: 3.38 us -> 4.52 us  [on_device(): lax.all_to_all(held(send), 'sp', 0, 0, tiled=True, axis_index_groups=insi...]
  transfers between devices with their start and end apart: 2 -> 2, of which waited for: 1 -> 1; matrix products, arithmetic and copies ran while one was open for 0% -> 0% of each run, Pallas kernels for 8% -> 9%
where the time goes in v7:
time: 103 us; the launch traced here: 102 us
  blocking collectives  76.8 us (75%)
  Pallas kernels  13.4 us (13%)
  starting transfers between devices  9.22 us (9%)
  waiting for transfers between devices  1.27 us (1%)
    all_to_all x1, blocking collectives, on_device(): lax.all_to_all(held(send), 'sp', 0, 0, tiled=True, axis_index_groups=acro...  61.6 us
    all_to_all x1, blocking collectives, on_device(): lax.all_to_all(held(send), 'sp', 0, 0, tiled=True, axis_index_groups=insi...  15.2 us
    ppermute x1, starting transfers between devices, on_device(): lax.ppermute(tokens[length - HALO:], 'sp', [(i, i + 1) for i in range(seq...  4.7 us
    all_to_all x1, starting transfers between devices, on_device(): lax.all_to_all(held(send), 'sp', 0, 0, tiled=True, axis_index_groups=insi...  4.52 us
    pallas_call x1, Pallas kernels, on_device(): call(inner_kernel, (near(length, channels), near(length, channels), near(...  4.49 us
    pallas_call x1, Pallas kernels, on_device(): call(project_kernel, (near(length, width, dtype=bf16), near(depth, width,...  4.26 us
  transfers between devices with their start and end apart: 2, of which 1 were waited for; matrix products, arithmetic and copies ran while one was open for 0% of the time, Pallas kernels for 9%

profile of v7, /device:TPU:40, one launch (start us, length us, event | category | flops | bytes accessed | tf_op | source)
XLA Modules:
  0.0 102.3 jit_solution(18129855209952996794)
XLA Ops:
  0.6 0.8 slice.3
  1.4 4.7 %collective-permute-start = (bf16[8,2048]{1,0:T(8,128)(2,1)S(1)}, bf16[8,2048]{1,0:T(8,128)(2,1)S(1)}, u32[]{:S(2)}, u32[]{:S(2)}) collective-permute-start(bf16[8,2048]{1,0:T(8,128)(2,1)S(1)} %slice.3), channel_id=1, source_target_pairs={{0,8},{8,16},{16,24},{24,32},{32,40},{40,48},{48,56},{56,64},{64,7... | collective-permute-start | bytes 98312 | tf_op jit(solution)/shard_map/ppermute | solution.py:455
  6.1 0.0 copy-start
  6.1 0.0 copy-start.1
  6.1 0.0 copy-start.2
  6.1 0.0 copy-start.3
  6.2 0.0 copy-start.5
  6.2 0.0 copy-start.6
  6.2 0.0 copy-start.7
  6.2 4.3 %project.1 = (bf16[512,512]{1,0:T(8,128)(2,1)S(1)}, bf16[2048,512]{1,0:T(8,128)(2,1)S(1)}, f32[4,512]{1,0:T(4,128)S(1)}, bf16[8,2048]{1,0:T(8,128)(2,1)S(1)}, f32[4,8]{1,0:T(4,128)S(1)}) custom-call(bf16[512,2048]{1,0:T(8,128)(2,1)} %tok_ref.1, bf16[16,128]{1,0:T(8,128)(2,1)} %bitcast.15, bf16[2048,256]{1,0:T(8,128)(2,1)} %wv_hbm.1, ...), custom_call_target="tpu_custom_call" | custom-call | flops 1073741824 | bytes 1048576 | tf_op jit(solution)/shard_map/project/pallas_call | solution.py:460
  10.5 0.0 collective-permute-done.halo_ref
  10.5 0.0 copy-done
  10.5 0.0 copy-done.1
  10.5 0.0 copy-done.2
  10.5 0.0 copy-done.3
  10.5 0.0 copy-done.5
  10.5 0.0 copy-done.6
  10.5 0.0 copy-done.7
  10.5 2.0 %local.1 = (bf16[512,384]{1,0:T(8,128)(2,1)S(1)}, f32[8,128]{1,0:T(8,128)S(1)}, f32[4,512]{1,0:T(4,128)S(1)}, f32[4,512]{1,0:T(4,128)S(1)}, bf16[4,128,256]{2,1,...) custom-call(bf16[512,512]{1,0:T(8,128)(2,1)S(1)} %get-tuple-element.27.rows_ref, ...), custom_call_target="tpu_custom_call" | custom-call | flops 33554432 | bytes 1048576 | tf_op jit(solution)/shard_map/local/pallas_call | solution.py:486
  12.5 15.2 %all_to_all.15.recv_ref = bf16[4,4,2176]{2,1,0:T(4,128)(2,1)S(1)} all-to-all(bf16[4,4,2176]{2,1,0:T(4,128)(2,1)S(1)} %get-tuple-element.32), channel_id=1, replica_groups={{0,8,16,24},{32,40,48,56},{64,72,80,88},{96,104,112,120},{128,136,144,1..., dimensions={0} | all-to-all | bytes 139264 | tf_op jit(solution)/shard_map/all_to_all | solution.py:508
  27.8 0.6 team.1
  28.4 61.6 %all_to_all.16.recv_ref = bf16[8,4,2176]{2,1,0:T(4,128)(2,1)S(1)} all-to-all(bf16[8,4,2176]{2,1,0:T(4,128)(2,1)S(1)} %get-tuple-element.33), channel_id=1, replica_groups={{224,192,160,128,96,64,32,0},{232,200,168,136,104,72,40,8},{240,208,176..., dimensions={0} | all-to-all | bytes 278528 | tf_op jit(solution)/shard_map/all_to_all | solution.py:522
  90.0 1.0 prefix.1
  91.0 4.5 %all-to-all-start.2 = ((bf16[4,4,2304]{2,1,0:T(4,128)(2,1)}), bf16[4,4,2304]{2,1,0:T(4,128)(2,1)S(1)}, u32[]{:S(2)}, u32[]{:S(2)}) async-start(bf16[4,4,2304]{2,1,0:T(4,128)(2,1)} %get-tuple-element.37), calls=%async_computation.2 | async-start | bytes 147456 | tf_op jit(solution)/shard_map/all_to_all | solution.py:536
  95.5 0.0 copy-start.4
  95.5 4.5 %inner.1 = (f32[512,256]{1,0:T(8,128)S(1)}, f32[512,256]{1,0:T(8,128)S(1)}, f32[8,256]{1,0:T(8,128)S(1)}, bf16[512,128]{1,0:T(8,128)(2,1)S(1)}) custom-call(bf16[512,2048]{1,0:T(8,128)(2,1)} %tok_ref.1, bf16[2048,256]{1,0:T(8,128)(2,1)} %wg_ref.1, bf16[8,2048]{1,0:T(8,128)(2,1)S(1)} %get-tuple-element.30.fresh_ref, ...), custom_call_target="tpu_custom_call" | custom-call | flops 536870912 | bytes 1048576 | tf_op jit(solution)/shard_map/inner/pallas_call | solution.py:538
  100.0 1.3 %all-to-all-done.2.recv_ref = bf16[4,4,2304]{2,1,0:T(4,128)(2,1)S(1)} async-done(((bf16[4,4,2304]{2,1,0:T(4,128)(2,1)}), bf16[4,4,2304]{2,1,0:T(4,128)(2,1)S(1)}, u32[]{:S(2)}, u32[]{:S(2)}) %all-to-all-start.2) | async-done | bytes 73760 | tf_op jit(solution)/shard_map/all_to_all | solution.py:536
  101.3 0.0 copy-done.4
  101.3 1.0 %finish.1 = (bf16[512,256]{1,0:T(8,128)(2,1)}, bf16[1,8]{1,0:T(2,128)(2,1)}) custom-call(bf16[4,4,2304]{2,1,0:T(4,128)(2,1)S(1)} %all-to-all-done.2.recv_ref, f32[512,256]{1,0:T(8,128)S(1)} %get-tuple-element.44.base_ref, f32[512,256]{1,0:T(8,128)S(1)} %get-tuple-element.45.lift_ref, bf16[512,128]{1,0:T(8,128)(2,1)S(1)} %get-tuple-element.46.reads_ref, ...), custom_call_target="tpu_custom_call" | custom-call | bytes 1048576 | tf_op jit(solution)/shard_map/finish/pallas_call | solution.py:575
Async XLA Ops:
  1.4 9.1 %collective-permute-start = (bf16[8,2048]{1,0:T(8,128)(2,1)S(1)}, bf16[8,2048]{1,0:T(8,128)(2,1)S(1)}, u32[]{:S(2)}, u32[]{:S(2)}) collective-permute-start(bf16[8,2048]{1,0:T(8,128)(2,1)S(1)} %slice.3), channel_id=1, source_target_pairs={{0,8},{8,16},{16,24},{24,32},{32,40},{40,48},{48,56},{56,64},{64,7... | collective-permute-start | bytes 98312 | tf_op jit(solution)/shard_map/ppermute | solution.py:455
  6.1 4.4 %copy-start = (bf16[4,1024]{1,0:T(4,128)(2,1)S(1)}, bf16[4,1024]{1,0:T(4,128)(2,1)}, u32[]{:S(2)}) copy-start(bf16[4,1024]{1,0:T(4,128)(2,1)} %rtap_ref.3) | copy-start | bytes 24580
  6.1 4.4 %copy-start.1 = (bf16[4,2048]{1,0:T(4,128)(2,1)S(1)}, bf16[4,2048]{1,0:T(4,128)(2,1)}, u32[]{:S(2)}) copy-start(bf16[4,2048]{1,0:T(4,128)(2,1)} %vtap_ref.1) | copy-start | bytes 49156
  6.1 4.4 %copy-start.2 = (f32[512,4]{0,1:T(4,128)S(1)}, f32[512,4]{0,1:T(4,128)}, u32[]{:S(2)}) copy-start(f32[512,4]{0,1:T(4,128)} %param.27) | copy-start | bytes 24580
  6.1 4.4 %copy-start.3 = (bf16[4,1024]{1,0:T(4,128)(2,1)S(1)}, bf16[4,1024]{1,0:T(4,128)(2,1)}, u32[]{:S(2)}) copy-start(bf16[4,1024]{1,0:T(4,128)(2,1)} %wtap_ref.1) | copy-start | bytes 24580
  6.2 4.4 %copy-start.5 = (f32[32]{0:T(128)S(1)}, f32[32]{0:T(128)}, u32[]{:S(2)}) copy-start(f32[32]{0:T(128)} %param.28) | copy-start | bytes 388
  6.2 4.4 %copy-start.6 = (f32[32]{0:T(128)S(1)}, f32[32]{0:T(128)}, u32[]{:S(2)}) copy-start(f32[32]{0:T(128)} %param.25) | copy-start | bytes 388
  6.2 4.4 %copy-start.7 = (f32[32]{0:T(128)S(1)}, f32[32]{0:T(128)}, u32[]{:S(2)}) copy-start(f32[32]{0:T(128)} %param.26) | copy-start | bytes 388
  91.0 10.3 %all-to-all-start.2 = ((bf16[4,4,2304]{2,1,0:T(4,128)(2,1)}), bf16[4,4,2304]{2,1,0:T(4,128)(2,1)S(1)}, u32[]{:S(2)}, u32[]{:S(2)}) async-start(bf16[4,4,2304]{2,1,0:T(4,128)(2,1)} %get-tuple-element.37), calls=%async_computation.2 | async-start | bytes 147456 | tf_op jit(solution)/shard_map/all_to_all | solution.py:536
  95.5 5.8 %copy-start.4 = (f32[2048]{0:T(1024)S(1)}, f32[2048]{0:T(1024)}, u32[]{:S(2)}) copy-start(f32[2048]{0:T(1024)} %param.29) | copy-start | bytes 24580

commit v8 on v7

--- a/solution.py
+++ b/solution.py
@@ -214,14 +214,16 @@
     for g in range(teams):
         at = slice(g * stretch, (g + 1) * stretch)
         piece = running[at].reshape(TEAM, own, channels).astype(bf16)
-        send_ref[:, :, g * channels : (g + 1) * channels] = piece
+        for p, member in enumerate(places(TEAM)):
+            send_ref[p, :, g * channels : (g + 1) * channels] = piece[member]
     note = misc[0:stretch]
     for g in range(teams):
         at = slice(g * stretch, (g + 1) * stretch)
         note = jnp.where(lanes[0:stretch] == 2 * heads + g, read_column[at], note)
     note = note.reshape(TEAM, own, MISC)
     note = jnp.where(iota(note.shape, 2) >= MISC - HEAD, direct_rows[None], note).astype(bf16)
-    send_ref[:, :, teams * channels :] = note
+    for p, member in enumerate(places(TEAM)):
+        send_ref[p, :, teams * channels :] = note[member]
 
 
 def inner_kernel(
@@ -274,8 +276,8 @@
     before[...] += jnp.broadcast_to(cum[:, BLOCK - 1 :], before.shape)
 
 
-def places(teams):
-    return [*reversed(range(teams))]
+def places(count):
+    return [*reversed(range(count))]
 
 
 def fades_of(notes, heads, channels):
@@ -295,14 +297,16 @@
     fades = fades_of(notes, heads, channels)
     state = jnp.zeros((own, wide), f32)
     reach = jnp.ones((1, channels), f32)
+    place = {member: p for p, member in enumerate(places(count))}
     for k in range(count):
         local_ref[k] = state
         reach_ref[k : k + 1] = reach
-        fade = jnp.concatenate([fades[k : k + 1]] * teams, axis=1)
-        state = fade * state + recv_ref[k, :, 0:wide].astype(f32)
-        reach = reach * fades[k : k + 1]
+        at = place[k]
+        fade = jnp.concatenate([fades[at : at + 1]] * teams, axis=1)
+        state = fade * state + recv_ref[at, :, 0:wide].astype(f32)
+        reach = reach * fades[at : at + 1]
     total = state.astype(bf16)
-    note = recv_ref[count - 1, :, wide:].astype(f32)
+    note = recv_ref[place[count - 1], :, wide:].astype(f32)
     first = (iota((channels, MISC), 0) == iota((channels, MISC), 1) * HEAD).astype(f32)
     high = reach.astype(bf16).astype(f32)
     low = reach - high
@@ -332,9 +336,9 @@
         entering = jnp.where(group == t, state, entering)
         fade = jnp.concatenate([fades[at : at + 1]] * teams, axis=1)
         state = fade * state + recv_ref[at, :, 0:wide].astype(f32)
-    for k in range(TEAM):
+    for p, k in enumerate(places(TEAM)):
         reach = jnp.concatenate([reach_ref[k : k + 1]] * teams, axis=1)
-        send_ref[k, :, 0:wide] = (local_ref[k] + reach * entering).astype(bf16)
+        send_ref[p, :, 0:wide] = (local_ref[k] + reach * entering).astype(bf16)
     kept = state.astype(bf16).astype(f32)
     mine = kept[:, 0:channels]
     for g in range(1, teams):
@@ -363,10 +367,12 @@
     wide = recv_ref.shape[2] - channels
     pieces = wide // channels
     own = recv_ref.shape[1]
+    spot = {member: p for p, member in enumerate(places(TEAM))}
     earlier = jnp.concatenate(
         [
-            recv_ref[:, :, g * channels : (g + 1) * channels].astype(f32).reshape(TEAM * own, channels)
+            recv_ref[spot[i], :, g * channels : (g + 1) * channels].astype(f32)
             for g in range(pieces)
+            for i in range(TEAM)
         ],
         axis=0,
     ).astype(bf16)
@@ -449,7 +455,7 @@
     wide = teams * channels
     vm = pl.BlockSpec(memory_space=pltpu.VMEM)
     far = pl.BlockSpec(memory_space=pltpu.HBM)
-    inside_team = [[TEAM * t + i for i in range(TEAM)] for t in range(teams)]
+    inside_team = [[TEAM * t + i for i in places(TEAM)] for t in range(teams)]
     across_teams = [[TEAM * t + i for t in places(teams)] for i in range(TEAM)]
 
     halo = lax.ppermute(

time: 103 us -> 102 us (level)
  starting transfers between devices: 9.22 us -> 15.1 us
  blocking collectives: 76.8 us -> 71.7 us
  waiting for transfers between devices: 1.27 us -> 0.01 us
    all_to_all x1, starting transfers between devices: 4.52 us -> 10.4 us  [on_device(): lax.all_to_all(held(send), 'sp', 0, 0, tiled=True, axis_index_groups=insi...]
    all_to_all x1, blocking collectives: 61.6 us -> 58.1 us  [on_device(): lax.all_to_all(held(send), 'sp', 0, 0, tiled=True, axis_index_groups=acro...]
    all_to_all x1, blocking collectives: 15.2 us -> 13.5 us  [on_device(): lax.all_to_all(held(send), 'sp', 0, 0, tiled=True, axis_index_groups=insi...]
    all_to_all x1, waiting for transfers between devices: 1.27 us -> 0.01 us  [on_device(): lax.all_to_all(held(send), 'sp', 0, 0, tiled=True, axis_index_groups=insi...]
  transfers between devices with their start and end apart: 2 -> 2, of which waited for: 1 -> 0; matrix products, arithmetic and copies ran while one was open for 0% -> 0% of each run, Pallas kernels for 9% -> 9%
where the time goes in v8:
time: 102 us
  blocking collectives  71.7 us (70%)
  starting transfers between devices  15.1 us (15%)
  Pallas kernels  13.4 us (13%)
    all_to_all x1, blocking collectives, on_device(): lax.all_to_all(held(send), 'sp', 0, 0, tiled=True, axis_index_groups=acro...  58.1 us
    all_to_all x1, blocking collectives, on_device(): lax.all_to_all(held(send), 'sp', 0, 0, tiled=True, axis_index_groups=insi...  13.5 us
    all_to_all x1, starting transfers between devices, on_device(): lax.all_to_all(held(send), 'sp', 0, 0, tiled=True, axis_index_groups=insi...  10.4 us
    ppermute x1, starting transfers between devices, on_device(): lax.ppermute(tokens[length - HALO:], 'sp', [(i, i + 1) for i in range(seq...  4.7 us
    pallas_call x1, Pallas kernels, on_device(): call(inner_kernel, (near(length, channels), near(length, channels), near(...  4.49 us
    pallas_call x1, Pallas kernels, on_device(): call(project_kernel, (near(length, width, dtype=bf16), near(depth, width,...  4.26 us
  transfers between devices with their start and end apart: 2, of which 0 were waited for; matrix products, arithmetic and copies ran while one was open for 0% of the time, Pallas kernels for 9%

profile of v8, /device:TPU:40, one launch (start us, length us, event | category | flops | bytes accessed | tf_op | source)
XLA Modules:
  0.0 101.8 jit_solution(5403124137379502874)
XLA Ops:
  0.6 0.8 slice.3
  1.4 4.7 %collective-permute-start = (bf16[8,2048]{1,0:T(8,128)(2,1)S(1)}, bf16[8,2048]{1,0:T(8,128)(2,1)S(1)}, u32[]{:S(2)}, u32[]{:S(2)}) collective-permute-start(bf16[8,2048]{1,0:T(8,128)(2,1)S(1)} %slice.3), channel_id=1, source_target_pairs={{0,8},{8,16},{16,24},{24,32},{32,40},{40,48},{48,56},{56,64},{64,7... | collective-permute-start | bytes 98312 | tf_op jit(solution)/shard_map/ppermute | solution.py:461
  6.1 0.0 copy-start
  6.1 0.0 copy-start.1
  6.1 0.0 copy-start.2
  6.1 0.0 copy-start.3
  6.2 0.0 copy-start.5
  6.2 0.0 copy-start.6
  6.2 0.0 copy-start.7
  6.2 4.3 %project.1 = (bf16[512,512]{1,0:T(8,128)(2,1)S(1)}, bf16[2048,512]{1,0:T(8,128)(2,1)S(1)}, f32[4,512]{1,0:T(4,128)S(1)}, bf16[8,2048]{1,0:T(8,128)(2,1)S(1)}, f32[4,8]{1,0:T(4,128)S(1)}) custom-call(bf16[512,2048]{1,0:T(8,128)(2,1)} %tok_ref.1, bf16[16,128]{1,0:T(8,128)(2,1)} %bitcast.15, bf16[2048,256]{1,0:T(8,128)(2,1)} %wv_hbm.1, ...), custom_call_target="tpu_custom_call" | custom-call | flops 1073741824 | bytes 1048576 | tf_op jit(solution)/shard_map/project/pallas_call | solution.py:466
  10.5 0.0 collective-permute-done.halo_ref
  10.5 0.0 copy-done
  10.5 0.0 copy-done.1
  10.5 0.0 copy-done.2
  10.5 0.0 copy-done.3
  10.5 0.0 copy-done.5
  10.5 0.0 copy-done.6
  10.5 0.0 copy-done.7
  10.5 2.0 %local.1 = (bf16[512,384]{1,0:T(8,128)(2,1)S(1)}, f32[8,128]{1,0:T(8,128)S(1)}, f32[4,512]{1,0:T(4,128)S(1)}, f32[4,512]{1,0:T(4,128)S(1)}, bf16[4,128,256]{2,1,...) custom-call(bf16[512,512]{1,0:T(8,128)(2,1)S(1)} %get-tuple-element.27.rows_ref, ...), custom_call_target="tpu_custom_call" | custom-call | flops 33554432 | bytes 1048576 | tf_op jit(solution)/shard_map/local/pallas_call | solution.py:492
  12.5 13.5 %all_to_all.15.recv_ref = bf16[4,4,2176]{2,1,0:T(4,128)(2,1)S(1)} all-to-all(bf16[4,4,2176]{2,1,0:T(4,128)(2,1)S(1)} %get-tuple-element.32), channel_id=1, replica_groups={{24,16,8,0},{56,48,40,32},{88,80,72,64},{120,112,104,96},{152,144,136,1..., dimensions={0} | all-to-all | bytes 139264 | tf_op jit(solution)/shard_map/all_to_all | solution.py:514
  26.1 0.6 team.1
  26.7 58.1 %all_to_all.16.recv_ref = bf16[8,4,2176]{2,1,0:T(4,128)(2,1)S(1)} all-to-all(bf16[8,4,2176]{2,1,0:T(4,128)(2,1)S(1)} %get-tuple-element.33), channel_id=1, replica_groups={{224,192,160,128,96,64,32,0},{232,200,168,136,104,72,40,8},{240,208,176..., dimensions={0} | all-to-all | bytes 278528 | tf_op jit(solution)/shard_map/all_to_all | solution.py:528
  84.8 1.0 prefix.1
  85.8 10.4 %all-to-all-start.2 = ((bf16[4,4,2304]{2,1,0:T(4,128)(2,1)}), bf16[4,4,2304]{2,1,0:T(4,128)(2,1)S(1)}, u32[]{:S(2)}, u32[]{:S(2)}) async-start(bf16[4,4,2304]{2,1,0:T(4,128)(2,1)} %get-tuple-element.37), calls=%async_computation.2 | async-start | bytes 147456 | tf_op jit(solution)/shard_map/all_to_all | solution.py:542
  96.2 0.0 copy-start.4
  96.2 4.5 %inner.1 = (f32[512,256]{1,0:T(8,128)S(1)}, f32[512,256]{1,0:T(8,128)S(1)}, f32[8,256]{1,0:T(8,128)S(1)}, bf16[512,128]{1,0:T(8,128)(2,1)S(1)}) custom-call(bf16[512,2048]{1,0:T(8,128)(2,1)} %tok_ref.1, bf16[2048,256]{1,0:T(8,128)(2,1)} %wg_ref.1, bf16[8,2048]{1,0:T(8,128)(2,1)S(1)} %get-tuple-element.30.fresh_ref, ...), custom_call_target="tpu_custom_call" | custom-call | flops 536870912 | bytes 1048576 | tf_op jit(solution)/shard_map/inner/pallas_call | solution.py:544
  100.7 0.0 all-to-all-done.2.recv_ref
  100.8 0.0 copy-done.4
  100.8 1.0 %finish.1 = (bf16[512,256]{1,0:T(8,128)(2,1)}, bf16[1,8]{1,0:T(2,128)(2,1)}) custom-call(bf16[4,4,2304]{2,1,0:T(4,128)(2,1)S(1)} %all-to-all-done.2.recv_ref, f32[512,256]{1,0:T(8,128)S(1)} %get-tuple-element.44.base_ref, f32[512,256]{1,0:T(8,128)S(1)} %get-tuple-element.45.lift_ref, bf16[512,128]{1,0:T(8,128)(2,1)S(1)} %get-tuple-element.46.reads_ref, ...), custom_call_target="tpu_custom_call" | custom-call | bytes 1048576 | tf_op jit(solution)/shard_map/finish/pallas_call | solution.py:581
Async XLA Ops:
  1.4 9.1 %collective-permute-start = (bf16[8,2048]{1,0:T(8,128)(2,1)S(1)}, bf16[8,2048]{1,0:T(8,128)(2,1)S(1)}, u32[]{:S(2)}, u32[]{:S(2)}) collective-permute-start(bf16[8,2048]{1,0:T(8,128)(2,1)S(1)} %slice.3), channel_id=1, source_target_pairs={{0,8},{8,16},{16,24},{24,32},{32,40},{40,48},{48,56},{56,64},{64,7... | collective-permute-start | bytes 98312 | tf_op jit(solution)/shard_map/ppermute | solution.py:461
  6.1 4.4 %copy-start = (bf16[4,1024]{1,0:T(4,128)(2,1)S(1)}, bf16[4,1024]{1,0:T(4,128)(2,1)}, u32[]{:S(2)}) copy-start(bf16[4,1024]{1,0:T(4,128)(2,1)} %rtap_ref.3) | copy-start | bytes 24580
  6.1 4.4 %copy-start.1 = (bf16[4,2048]{1,0:T(4,128)(2,1)S(1)}, bf16[4,2048]{1,0:T(4,128)(2,1)}, u32[]{:S(2)}) copy-start(bf16[4,2048]{1,0:T(4,128)(2,1)} %vtap_ref.1) | copy-start | bytes 49156
  6.1 4.4 %copy-start.2 = (f32[512,4]{0,1:T(4,128)S(1)}, f32[512,4]{0,1:T(4,128)}, u32[]{:S(2)}) copy-start(f32[512,4]{0,1:T(4,128)} %param.27) | copy-start | bytes 24580
  6.1 4.4 %copy-start.3 = (bf16[4,1024]{1,0:T(4,128)(2,1)S(1)}, bf16[4,1024]{1,0:T(4,128)(2,1)}, u32[]{:S(2)}) copy-start(bf16[4,1024]{1,0:T(4,128)(2,1)} %wtap_ref.1) | copy-start | bytes 24580
  6.2 4.4 %copy-start.5 = (f32[32]{0:T(128)S(1)}, f32[32]{0:T(128)}, u32[]{:S(2)}) copy-start(f32[32]{0:T(128)} %param.28) | copy-start | bytes 388
  6.2 4.4 %copy-start.6 = (f32[32]{0:T(128)S(1)}, f32[32]{0:T(128)}, u32[]{:S(2)}) copy-start(f32[32]{0:T(128)} %param.25) | copy-start | bytes 388
  6.2 4.4 %copy-start.7 = (f32[32]{0:T(128)S(1)}, f32[32]{0:T(128)}, u32[]{:S(2)}) copy-start(f32[32]{0:T(128)} %param.26) | copy-start | bytes 388
  85.8 14.9 %all-to-all-start.2 = ((bf16[4,4,2304]{2,1,0:T(4,128)(2,1)}), bf16[4,4,2304]{2,1,0:T(4,128)(2,1)S(1)}, u32[]{:S(2)}, u32[]{:S(2)}) async-start(bf16[4,4,2304]{2,1,0:T(4,128)(2,1)} %get-tuple-element.37), calls=%async_computation.2 | async-start | bytes 147456 | tf_op jit(solution)/shard_map/all_to_all | solution.py:542
  96.2 4.5 %copy-start.4 = (f32[2048]{0:T(1024)S(1)}, f32[2048]{0:T(1024)}, u32[]{:S(2)}) copy-start(f32[2048]{0:T(1024)} %param.29) | copy-start | bytes 24580

commit v9 on v8

--- a/solution.py
+++ b/solution.py
@@ -74,6 +74,13 @@
     row = ref[...]
     shape = (count, row.shape[1])
     return jnp.sum(jnp.where(iota(shape, 1) == iota(shape, 0) + first, row, 0.0), axis=1, keepdims=True)
+
+
+def tail_kernel(tok_hbm, tail_ref, sem):
+    rows = tok_hbm.at[pl.ds(tok_hbm.shape[0] - HALO, HALO)]
+    copy = pltpu.make_async_copy(rows, tail_ref, sem)
+    copy.start()
+    copy.wait()
 
 
 def project_kernel(
@@ -458,9 +465,15 @@
     inside_team = [[TEAM * t + i for i in places(TEAM)] for t in range(teams)]
     across_teams = [[TEAM * t + i for t in places(teams)] for i in range(TEAM)]
 
-    halo = lax.ppermute(
-        tokens[length - HALO :], "sp", [(i, i + 1) for i in range(sequence_count - 1)]
-    )
+    tail = call(
+        tail_kernel,
+        near(HALO, depth, dtype=bf16),
+        in_specs=[far],
+        out_specs=vm,
+        scratch=[pltpu.SemaphoreType.DMA],
+        name="tail",
+    )(stored(tokens))
+    halo = lax.ppermute(held(tail), "sp", [(i, i + 1) for i in range(sequence_count - 1)])
     fresh = fresh_token_input.reshape(depth // 128, 128)
     spike = decay_spike.T
     rows, weights, step_raw, fresh_rows, new_step = call(

time: 102 us -> 102 us (level)
  no operation moved by 1% of the time
where the time goes in v9:
time: 102 us
  blocking collectives  71.7 us (70%)
  starting transfers between devices  15.1 us (15%)
  Pallas kernels  14.1 us (14%)
    all_to_all x1, blocking collectives, on_device(): lax.all_to_all(held(send), 'sp', 0, 0, tiled=True, axis_index_groups=acro...  58.1 us
    all_to_all x1, blocking collectives, on_device(): lax.all_to_all(held(send), 'sp', 0, 0, tiled=True, axis_index_groups=insi...  13.5 us
    all_to_all x1, starting transfers between devices, on_device(): lax.all_to_all(held(send), 'sp', 0, 0, tiled=True, axis_index_groups=insi...  10.4 us
    ppermute x1, starting transfers between devices, on_device(): lax.ppermute(held(tail), 'sp', [(i, i + 1) for i in range(sequence_count...  4.71 us
    pallas_call x1, Pallas kernels, on_device(): call(inner_kernel, (near(length, channels), near(length, channels), near(...  4.49 us
    pallas_call x1, Pallas kernels, on_device(): call(project_kernel, (near(length, width, dtype=bf16), near(depth, width,...  4.26 us
  transfers between devices with their start and end apart: 2, of which 0 were waited for; matrix products, arithmetic and copies ran while one was open for 0% of the time, Pallas kernels for 9%

profile of v9, /device:TPU:40, one launch (start us, length us, event | category | flops | bytes accessed | tf_op | source)
XLA Modules:
  0.0 101.8 jit_solution(615816817030950301)
XLA Ops:
  0.6 0.8 tail.1
  1.4 4.7 %collective-permute-start = (bf16[8,2048]{1,0:T(8,128)(2,1)S(1)}, bf16[8,2048]{1,0:T(8,128)(2,1)S(1)}, u32[]{:S(2)}, u32[]{:S(2)}) collective-permute-start(bf16[8,2048]{1,0:T(8,128)(2,1)S(1)} %tail.1), channel_id=1, source_target_pairs={{0,8},{8,16},{16,24},{24,32},{32,40},{40,48},{48,56},{56,64},{64,7... | collective-permute-start | bytes 98312 | tf_op jit(solution)/shard_map/ppermute | solution.py:476
  6.1 0.0 copy-start
  6.1 0.0 copy-start.1
  6.2 0.0 copy-start.2
  6.2 0.0 copy-start.3
  6.2 0.0 copy-start.5
  6.2 0.0 copy-start.6
  6.2 0.0 copy-start.7
  6.2 4.3 %project.1 = (bf16[512,512]{1,0:T(8,128)(2,1)S(1)}, bf16[2048,512]{1,0:T(8,128)(2,1)S(1)}, f32[4,512]{1,0:T(4,128)S(1)}, bf16[8,2048]{1,0:T(8,128)(2,1)S(1)}, f32[4,8]{1,0:T(4,128)S(1)}) custom-call(bf16[512,2048]{1,0:T(8,128)(2,1)} %tok_ref.1, bf16[16,128]{1,0:T(8,128)(2,1)} %bitcast.15, bf16[2048,256]{1,0:T(8,128)(2,1)} %wv_hbm.1, ...), custom_call_target="tpu_custom_call" | custom-call | flops 1073741824 | bytes 1048576 | tf_op jit(solution)/shard_map/project/pallas_call | solution.py:479
  10.5 0.0 collective-permute-done.halo_ref
  10.5 0.0 copy-done
  10.5 0.0 copy-done.1
  10.5 0.0 copy-done.2
  10.5 0.0 copy-done.3
  10.5 0.0 copy-done.5
  10.5 0.0 copy-done.6
  10.5 0.0 copy-done.7
  10.6 2.0 %local.1 = (bf16[512,384]{1,0:T(8,128)(2,1)S(1)}, f32[8,128]{1,0:T(8,128)S(1)}, f32[4,512]{1,0:T(4,128)S(1)}, f32[4,512]{1,0:T(4,128)S(1)}, bf16[4,128,256]{2,1,...) custom-call(bf16[512,512]{1,0:T(8,128)(2,1)S(1)} %get-tuple-element.27.rows_ref, ...), custom_call_target="tpu_custom_call" | custom-call | flops 33554432 | bytes 1048576 | tf_op jit(solution)/shard_map/local/pallas_call | solution.py:505
  12.6 13.5 %all_to_all.15.recv_ref = bf16[4,4,2176]{2,1,0:T(4,128)(2,1)S(1)} all-to-all(bf16[4,4,2176]{2,1,0:T(4,128)(2,1)S(1)} %get-tuple-element.32), channel_id=1, replica_groups={{24,16,8,0},{56,48,40,32},{88,80,72,64},{120,112,104,96},{152,144,136,1..., dimensions={0} | all-to-all | bytes 139264 | tf_op jit(solution)/shard_map/all_to_all | solution.py:527
  26.1 0.6 team.1
  26.7 58.1 %all_to_all.16.recv_ref = bf16[8,4,2176]{2,1,0:T(4,128)(2,1)S(1)} all-to-all(bf16[8,4,2176]{2,1,0:T(4,128)(2,1)S(1)} %get-tuple-element.33), channel_id=1, replica_groups={{224,192,160,128,96,64,32,0},{232,200,168,136,104,72,40,8},{240,208,176..., dimensions={0} | all-to-all | bytes 278528 | tf_op jit(solution)/shard_map/all_to_all | solution.py:541
  84.8 1.0 prefix.1
  85.8 10.4 %all-to-all-start.2 = ((bf16[4,4,2304]{2,1,0:T(4,128)(2,1)}), bf16[4,4,2304]{2,1,0:T(4,128)(2,1)S(1)}, u32[]{:S(2)}, u32[]{:S(2)}) async-start(bf16[4,4,2304]{2,1,0:T(4,128)(2,1)} %get-tuple-element.37), calls=%async_computation.2 | async-start | bytes 147456 | tf_op jit(solution)/shard_map/all_to_all | solution.py:555
  96.3 0.0 copy-start.4
  96.3 4.5 %inner.1 = (f32[512,256]{1,0:T(8,128)S(1)}, f32[512,256]{1,0:T(8,128)S(1)}, f32[8,256]{1,0:T(8,128)S(1)}, bf16[512,128]{1,0:T(8,128)(2,1)S(1)}) custom-call(bf16[512,2048]{1,0:T(8,128)(2,1)} %tok_ref.1, bf16[2048,256]{1,0:T(8,128)(2,1)} %wg_ref.1, bf16[8,2048]{1,0:T(8,128)(2,1)S(1)} %get-tuple-element.30.fresh_ref, ...), custom_call_target="tpu_custom_call" | custom-call | flops 536870912 | bytes 1048576 | tf_op jit(solution)/shard_map/inner/pallas_call | solution.py:557
  100.8 0.0 all-to-all-done.2.recv_ref
  100.8 0.0 copy-done.4
  100.8 1.0 %finish.1 = (bf16[512,256]{1,0:T(8,128)(2,1)}, bf16[1,8]{1,0:T(2,128)(2,1)}) custom-call(bf16[4,4,2304]{2,1,0:T(4,128)(2,1)S(1)} %all-to-all-done.2.recv_ref, f32[512,256]{1,0:T(8,128)S(1)} %get-tuple-element.44.base_ref, f32[512,256]{1,0:T(8,128)S(1)} %get-tuple-element.45.lift_ref, bf16[512,128]{1,0:T(8,128)(2,1)S(1)} %get-tuple-element.46.reads_ref, ...), custom_call_target="tpu_custom_call" | custom-call | bytes 1048576 | tf_op jit(solution)/shard_map/finish/pallas_call | solution.py:594
Async XLA Ops:
  1.4 9.1 %collective-permute-start = (bf16[8,2048]{1,0:T(8,128)(2,1)S(1)}, bf16[8,2048]{1,0:T(8,128)(2,1)S(1)}, u32[]{:S(2)}, u32[]{:S(2)}) collective-permute-start(bf16[8,2048]{1,0:T(8,128)(2,1)S(1)} %tail.1), channel_id=1, source_target_pairs={{0,8},{8,16},{16,24},{24,32},{32,40},{40,48},{48,56},{56,64},{64,7... | collective-permute-start | bytes 98312 | tf_op jit(solution)/shard_map/ppermute | solution.py:476
  6.1 4.4 %copy-start = (bf16[4,1024]{1,0:T(4,128)(2,1)S(1)}, bf16[4,1024]{1,0:T(4,128)(2,1)}, u32[]{:S(2)}) copy-start(bf16[4,1024]{1,0:T(4,128)(2,1)} %rtap_ref.3) | copy-start | bytes 24580
  6.1 4.4 %copy-start.1 = (bf16[4,2048]{1,0:T(4,128)(2,1)S(1)}, bf16[4,2048]{1,0:T(4,128)(2,1)}, u32[]{:S(2)}) copy-start(bf16[4,2048]{1,0:T(4,128)(2,1)} %vtap_ref.1) | copy-start | bytes 49156
  6.2 4.4 %copy-start.2 = (f32[512,4]{0,1:T(4,128)S(1)}, f32[512,4]{0,1:T(4,128)}, u32[]{:S(2)}) copy-start(f32[512,4]{0,1:T(4,128)} %param.27) | copy-start | bytes 24580
  6.2 4.4 %copy-start.3 = (bf16[4,1024]{1,0:T(4,128)(2,1)S(1)}, bf16[4,1024]{1,0:T(4,128)(2,1)}, u32[]{:S(2)}) copy-start(bf16[4,1024]{1,0:T(4,128)(2,1)} %wtap_ref.1) | copy-start | bytes 24580
  6.2 4.4 %copy-start.5 = (f32[32]{0:T(128)S(1)}, f32[32]{0:T(128)}, u32[]{:S(2)}) copy-start(f32[32]{0:T(128)} %param.28) | copy-start | bytes 388
  6.2 4.4 %copy-start.6 = (f32[32]{0:T(128)S(1)}, f32[32]{0:T(128)}, u32[]{:S(2)}) copy-start(f32[32]{0:T(128)} %param.25) | copy-start | bytes 388
  6.2 4.4 %copy-start.7 = (f32[32]{0:T(128)S(1)}, f32[32]{0:T(128)}, u32[]{:S(2)}) copy-start(f32[32]{0:T(128)} %param.26) | copy-start | bytes 388
  85.8 14.9 %all-to-all-start.2 = ((bf16[4,4,2304]{2,1,0:T(4,128)(2,1)}), bf16[4,4,2304]{2,1,0:T(4,128)(2,1)S(1)}, u32[]{:S(2)}, u32[]{:S(2)}) async-start(bf16[4,4,2304]{2,1,0:T(4,128)(2,1)} %get-tuple-element.37), calls=%async_computation.2 | async-start | bytes 147456 | tf_op jit(solution)/shard_map/all_to_all | solution.py:555
  96.3 4.5 %copy-start.4 = (f32[2048]{0:T(1024)S(1)}, f32[2048]{0:T(1024)}, u32[]{:S(2)}) copy-start(f32[2048]{0:T(1024)} %param.29) | copy-start | bytes 24580
